TPU v7x, 128 devices: a whole 4x4x4 slice. The times are simulated.
128 devices in a mesh: ep: 128 (over z, y, x, core).
Axes of the slice: x: 4, y: 4, z: 4, core: 2. Of those that a mesh axis runs over, the one named last changes fastest.
Arguments:
- tokens: bfloat16 [2048, 2048], P('ep'), may hold values from -6 to 6
- state: float32 [2, 2048, 2048], P(None, 'ep'), may hold values from -4 to 4
- norm_mix: float32 [2048], replicated, may hold values from 0.1 to 1.9
- w_drive: bfloat16 [2048, 512], replicated, may hold values from -0.125 to 0.125
- lam_real: float32 [32, 64], replicated, may hold values from -1 to -0.05
- lam_imag: float32 [32, 64], replicated, may hold values from -3 to 3
- log_step: float32 [32], replicated, may hold values from -2.5 to 0.5
- b_real: float32 [32, 64, 16], replicated, may hold values from -1 to 1
- b_imag: float32 [32, 64, 16], replicated, may hold values from -1 to 1
- readout_real: float32 [32, 16, 64], replicated, may hold values from -0.5 to 0.5
- readout_imaginary: float32 [32, 16, 64], replicated, may hold values from -0.5 to 0.5
- d_skip: float32 [512], replicated, may hold values from -4 to 4
- w_value: bfloat16 [512, 512], replicated, may hold values from -0.25 to 0.25
- w_glugate: bfloat16 [512, 512], replicated, may hold values from -0.25 to 0.25
- w_output: bfloat16 [512, 2048], replicated, may hold values from -0.25 to 0.25
- norm_ffn: float32 [2048], replicated, may hold values from 0.1 to 1.9
- w_group: bfloat16 [2048, 4], replicated, may hold values from -0.125 to 0.125
- w_expert: bfloat16 [2048, 128], replicated, may hold values from -0.125 to 0.125
- route_ids: int32 [2048, 6], P('ep'), may hold values from 0 to 127, all different within a row; in each aligned block of 16 rows (0 to 15, 16 to 31, ...) at most 2 rows name the same one
- expert_gate: bfloat16 [128, 2048, 512], P('ep'), may hold values from -0.125 to 0.125
- expert_up: bfloat16 [128, 2048, 512], P('ep'), may hold values from -0.125 to 0.125
- expert_down: bfloat16 [128, 512, 2048], P('ep'), may hold values from -1 to 1
- dense_vector: float32 [2048], replicated, may hold values from -0.125 to 0.125
- dense_gate: bfloat16 [2048, 8192], P(None, 'ep'), may hold values from -0.125 to 0.125
- dense_up: bfloat16 [2048, 8192], P(None, 'ep'), may hold values from -0.125 to 0.125
- dense_down: bfloat16 [8192, 2048], P('ep'), may hold values from -0.25 to 0.25
Outputs:
- layer_out: bfloat16 [2048, 2048], P('ep')
- new_state: float32 [2, 2048, 2048], P(None, 'ep')
Inputs may be any that keep to these rules, and one draw needn't show every extreme that they name: `route_ids`: each row names 6 different experts. Among the rows of one device no expert is named more than 2 times, a bound that some block reaches.
All inputs are finite; a program needn't handle non-finite values.
Results may differ from a plain program's by a relative error of at most 0.018.
Values may be sent and summed in bfloat16 or wider, within the bound.
A program may use at most 128 MiB of HBM per device.

v0:
```python
import jax
import jax.numpy as jnp
from jax import lax
from jax.sharding import PartitionSpec as P

EPS = 1e-05


def from_partner(array, axis, bit):
    return lax.ppermute(array, axis, [(i, i ^ 1 << bit) for i in range(lax.axis_size(axis))])


def rms_scale(values, gain):
    widened = values.astype(jnp.float32)
    scaled = widened * lax.rsqrt(jnp.mean(widened * widened, axis=-1, keepdims=True) + EPS)
    return (scaled * gain).astype(jnp.bfloat16)


def state_mixer(
    tokens,
    state,
    norm_mix,
    w_drive,
    lam_real,
    lam_imag,
    log_step,
    b_real,
    b_imag,
    readout_real,
    readout_imaginary,
    d_skip,
    w_value,
    w_glugate,
    w_output,
):
    row_count = tokens.shape[0]
    group_count, state_dimension = lam_real.shape
    channels = b_real.shape[2]
    normed_in = rms_scale(tokens, norm_mix)
    drive = jnp.dot(normed_in, w_drive, preferred_element_type=jnp.float32).astype(jnp.bfloat16)
    time_step = jnp.exp(log_step)[:, None]
    magnitude = jnp.exp(lam_real * time_step)
    decay_re = magnitude * jnp.cos(lam_imag * time_step)
    decay_im = magnitude * jnp.sin(lam_imag * time_step)
    modulus = lam_real * lam_real + lam_imag * lam_imag
    factor_re = ((decay_re - 1.0) * lam_real + decay_im * lam_imag) / modulus
    factor_im = (decay_im * lam_real - (decay_re - 1.0) * lam_imag) / modulus
    map_re = factor_re[:, :, None] * b_real - factor_im[:, :, None] * b_imag
    map_im = factor_re[:, :, None] * b_imag + factor_im[:, :, None] * b_real
    drive_wide = drive.astype(jnp.float32)
    grouped = drive_wide.reshape(row_count, group_count, channels)
    input_re = jnp.einsum("gpc,sgc->sgp", map_re, grouped)
    input_im = jnp.einsum("gpc,sgc->sgp", map_im, grouped)
    old_re = state[0].reshape(row_count, group_count, state_dimension)
    old_im = state[1].reshape(row_count, group_count, state_dimension)
    incoming_real = decay_re * old_re - decay_im * old_im + input_re
    incoming_imaginary = decay_re * old_im + decay_im * old_re + input_im
    projected_output = jnp.einsum("xej,fxj->fxe", readout_real, incoming_real) - jnp.einsum(
        "xej,fxj->fxe", readout_imaginary, incoming_imaginary
    )
    readout = jax.nn.gelu(
        projected_output.reshape(row_count, group_count * channels) + d_skip * drive_wide
    ).astype(jnp.bfloat16)
    value_part = jnp.dot(readout, w_value, preferred_element_type=jnp.float32)
    gate_part = jnp.dot(readout, w_glugate, preferred_element_type=jnp.float32)
    mixed = (value_part * jax.nn.sigmoid(gate_part)).astype(jnp.bfloat16)
    resid = (
        tokens.astype(jnp.float32) + jnp.dot(mixed, w_output, preferred_element_type=jnp.float32)
    ).astype(jnp.bfloat16)
    new_state = jnp.stack(
        [incoming_real.reshape(row_count, -1), incoming_imaginary.reshape(row_count, -1)]
    )
    return (resid, new_state)


def route_gates(normed, w_group, w_expert, route_ids):
    row_count = normed.shape[0]
    group_count = w_group.shape[1]
    expert_count = w_expert.shape[1]
    per_group = expert_count // group_count
    group_exp = jnp.exp(jnp.dot(normed, w_group, preferred_element_type=jnp.float32))
    group_prob = group_exp / jnp.sum(group_exp, axis=1, keepdims=True)
    inner_exp = jnp.exp(jnp.dot(normed, w_expert, preferred_element_type=jnp.float32)).reshape(
        row_count, group_count, per_group
    )
    inner_prob = inner_exp / jnp.sum(inner_exp, axis=2, keepdims=True)
    joint = (group_prob[:, :, None] * inner_prob).reshape(row_count, expert_count)
    inner_flat = inner_prob.reshape(row_count, expert_count)
    matched = route_ids[:, :, None] == jnp.arange(expert_count, dtype=jnp.int32)[None, None, :]
    picked_joint = jnp.sum(jnp.where(matched, joint[:, None, :], 0.0), axis=2)
    picked_inner = jnp.sum(jnp.where(matched, inner_flat[:, None, :], 0.0), axis=2)
    return picked_joint / jnp.sum(picked_inner, axis=1, keepdims=True)


def expert_rows(rows_in, w_gate, w_up, w_down):
    gate_part = jnp.dot(rows_in, w_gate, preferred_element_type=jnp.float32)
    up_part = jnp.dot(rows_in, w_up, preferred_element_type=jnp.float32)
    hidden = (jax.nn.silu(gate_part) * up_part).astype(jnp.bfloat16)
    return jnp.dot(hidden, w_down, preferred_element_type=jnp.float32).astype(jnp.bfloat16)


def on_device(
    tokens,
    state,
    norm_mix,
    w_drive,
    lam_real,
    lam_imag,
    log_step,
    b_real,
    b_imag,
    readout_real,
    readout_imaginary,
    d_skip,
    w_value,
    w_glugate,
    w_output,
    norm_ffn,
    w_group,
    w_expert,
    route_ids,
    expert_gate,
    expert_up,
    expert_down,
    dense_vector,
    dense_gate,
    dense_up,
    dense_down,
):
    resid, new_state = state_mixer(
        tokens,
        state,
        norm_mix,
        w_drive,
        lam_real,
        lam_imag,
        log_step,
        b_real,
        b_imag,
        readout_real,
        readout_imaginary,
        d_skip,
        w_value,
        w_glugate,
        w_output,
    )
    normed = rms_scale(resid, norm_ffn)
    seq_count, width = normed.shape
    topk = route_ids.shape[1]
    expert_count = w_expert.shape[1]
    capacity = max(2, 5 * seq_count * topk // (2 * expert_count))
    own_gate = expert_gate[0]
    own_up = expert_up[0]
    own_down = expert_down[0]
    my_index = lax.axis_index("ep")
    low_bits = lax.axis_size("ep").bit_length() - 3
    block = normed
    for bit in range(low_bits):
        other = from_partner(block, "ep", bit)
        upper = my_index >> bit & 1 == 1
        block = jnp.where(
            upper, jnp.concatenate([other, block], 0), jnp.concatenate([block, other], 0)
        )
    packed = jnp.stack([dense_gate, dense_up, jnp.transpose(dense_down)])
    for bit in (low_bits, low_bits + 1):
        packed = jnp.concatenate([packed, from_partner(packed, "ep", bit)], 2)
    branch_gate = jax.nn.sigmoid(jnp.dot(block.astype(jnp.float32), dense_vector))
    dense_g = jnp.dot(block, packed[0], preferred_element_type=jnp.float32)
    dense_u = jnp.dot(block, packed[1], preferred_element_type=jnp.float32)
    block_hidden = (branch_gate[:, None] * jax.nn.silu(dense_g) * dense_u).astype(jnp.bfloat16)
    partial_sum = lax.dot_general(
        block_hidden, packed[2], (((1,), (1,)), ((), ())), preferred_element_type=jnp.float32
    )
    for bit in reversed(range(low_bits)):
        half = partial_sum.shape[0] // 2
        lower_part = partial_sum[:half]
        upper_part = partial_sum[half:]
        upper = my_index >> bit & 1 == 1
        outgoing_half = jnp.where(upper, lower_part, upper_part)
        kept_half = jnp.where(upper, upper_part, lower_part)
        partial_sum = kept_half + from_partner(
            outgoing_half.astype(jnp.bfloat16), "ep", bit
        ).astype(outgoing_half.dtype)
    gates = route_gates(normed, w_group, w_expert, route_ids)
    flat_ids = route_ids.reshape(-1)
    onehot = (flat_ids[:, None] == jnp.arange(expert_count, dtype=jnp.int32)[None, :]).astype(
        jnp.int32
    )
    ordinal = jnp.sum((jnp.cumsum(onehot, axis=0) - 1) * onehot, axis=1)
    target = flat_ids * capacity + ordinal
    source_rows = jnp.repeat(normed, topk, axis=0)
    outgoing = jnp.zeros((expert_count * capacity, width), jnp.bfloat16).at[target].set(source_rows)
    outgoing = outgoing.reshape(expert_count, capacity, width)
    received = lax.all_to_all(outgoing, "ep", split_axis=0, concat_axis=0, tiled=True)
    senders, items, inner_width = received.shape
    result = expert_rows(received.reshape(senders * items, inner_width), own_gate, own_up, own_down)
    returned = lax.all_to_all(
        result.reshape(senders, items, inner_width), "ep", split_axis=0, concat_axis=0, tiled=True
    )
    picked = returned.reshape(expert_count * capacity, width)[target]
    weighted = picked.astype(jnp.float32).reshape(seq_count, topk, width) * gates[:, :, None]
    local_moe = jnp.sum(weighted, axis=1)
    layer_out = (resid.astype(jnp.float32) + partial_sum + local_moe).astype(jnp.bfloat16)
    return (layer_out, new_state)


def solution(mesh):
    placed = (
        P("ep", None),
        P(None, "ep", None),
        P(),
        P(),
        P(),
        P(),
        P(),
        P(),
        P(),
        P(),
        P(),
        P(),
        P(),
        P(),
        P(),
        P(),
        P(),
        P(),
        P("ep", None),
        P("ep", None, None),
        P("ep", None, None),
        P("ep", None, None),
        P(),
        P(None, "ep"),
        P(None, "ep"),
        P("ep", None),
    )
    return jax.shard_map(
        on_device,
        mesh=mesh,
        in_specs=placed,
        out_specs=(P("ep", None), P(None, "ep", None)),
        check_vma=False,
    )
```

profile of v0, /device:TPU:0, one launch (start us, length us, event | category | flops | bytes accessed | tf_op | source)
XLA Modules:
  0.0 196.9 jit_solution(16768890376965123161)
XLA Ops:
  0.7 0.8 exp.26
  1.5 1.0 fusion.43
  2.5 2.1 %convolution_convert_fusion.1 = bf16[16,512]{1,0:T(8,128)(2,1)S(1)} fusion(bf16[2048,512]{1,0:T(8,128)(2,1)} %param.29, bf16[16,2048]{1,0:T(8,128)(2,1)} %param.26, f32[2048]{0:T(1024)} %param.28, f32[16]{0:T(128)S(1)} %add_rsqrt_fusion.1), kind=kOutput, calls=%fused_computation.30 | convolution fusion | flops 33693696 | bytes 2187328 | tf_op jit(solution)/shard_map/dot_general | solution.py:40
  5.2 0.4 fusion.15
  5.7 0.4 fusion.16
  6.1 0.7 copy-done.13
  8.0 2.5 %multiply_reduce_fusion.1 = (f32[16]{0:T(128)S(1)}, f32[16,2048]{1,0:T(8,128)S(1)}) fusion(bf16[512,2048]{1,0:T(8,128)(2,1)} %param.40, f32[16,512]{1,0:T(8,128)S(1)} %fusion.75, bf16[16,512]{1,0:T(8,128)(2,1)S(1)} %fusion.63, bf16[512,512]{1,0:T(8,128)(2,1)} %param.39, bf16[16,2048]{1,0:T(8,128)(2,1)S(1)} %copy-done.21), kind=kOutput, calls=%fused_computation.78 | convolution fusion | flops 42180592 | bytes 2867264 | tf_op jit(solution)/shard_map/dot_general | solution.py:68
  10.7 1.2 collective-permute-done
  12.0 1.7 collective-permute-start.1
  13.7 4.0 %collective-permute-done.1 = bf16[32,2048]{1,0:T(8,128)(2,1)S(1)} collective-permute-done((bf16[32,2048]{1,0:T(8,128)(2,1)S(1)}, bf16[32,2048]{1,0:T(8,128)(2,1)S(1)}, u32[]{:S(2)}, u32[]{:S(2)}) %collective-permute-start.1) | collective-permute-done | bytes 131104 | tf_op jit(solution)/shard_map/ppermute | solution.py:10
  17.6 0.8 maximum_select_fusion.3
  18.4 3.1 %collective-permute-start.2 = (bf16[64,2048]{1,0:T(8,128)(2,1)}, bf16[64,2048]{1,0:T(8,128)(2,1)}, u32[]{:S(2)}, u32[]{:S(2)}) collective-permute-start(bf16[64,2048]{1,0:T(8,128)(2,1)} %maximum_select_fusion.3), channel_id=1, source_target_pairs={{0,4},{1,5},{2,6},{3,7},{4,0},{5,1},{6,2},{7,3},{8,12},{9,13},{10,... | collective-permute-start | bytes 786440 | tf_op jit(solution)/shard_map/ppermute | solution.py:10
  21.5 1.0 pad_maximum_fusion.2
  22.5 1.9 collective-permute-start.5
  24.4 3.3 %collective-permute-done.2 = bf16[64,2048]{1,0:T(8,128)(2,1)} collective-permute-done((bf16[64,2048]{1,0:T(8,128)(2,1)}, bf16[64,2048]{1,0:T(8,128)(2,1)}, u32[]{:S(2)}, u32[]{:S(2)}) %collective-permute-start.2) | collective-permute-done | bytes 262176 | tf_op jit(solution)/shard_map/ppermute | solution.py:10
  27.7 2.3 %maximum_select_fusion.2 = bf16[128,2048]{1,0:T(8,128)(2,1)} fusion(bf16[64,2048]{1,0:T(8,128)(2,1)} %maximum_select_fusion.3, bf16[64,2048]{1,0:T(8,128)(2,1)} %collective-permute-done.2, pred[]{:T(512)S(6)} %eq.50), kind=kLoop, calls=%fused_computation.45 | loop fusion | flops 2359296 | bytes 1048577 | tf_op jit(solution)/shard_map/jit(_where)/select_n | solution.py:161
  30.0 1.7 collective-permute-start.3
  31.6 10.9 %collective-permute-done.3 = bf16[128,2048]{1,0:T(8,128)(2,1)} collective-permute-done((bf16[128,2048]{1,0:T(8,128)(2,1)}, bf16[128,2048]{1,0:T(8,128)(2,1)}, u32[]{:S(2)}, u32[]{:S(2)}) %collective-permute-start.3) | collective-permute-done | bytes 524320 | tf_op jit(solution)/shard_map/ppermute | solution.py:10
  42.5 3.0 %maximum_select_fusion.1 = bf16[256,2048]{1,0:T(8,128)(2,1)} fusion(bf16[128,2048]{1,0:T(8,128)(2,1)} %maximum_select_fusion.2, bf16[128,2048]{1,0:T(8,128)(2,1)} %collective-permute-done.3, pred[]{:T(512)S(6)} %eq.51), kind=kLoop, calls=%fused_computation.40 | loop fusion | flops 4718592 | bytes 2097153 | tf_op jit(solution)/shard_map/jit(_where)/select_n | solution.py:161
  45.6 3.3 %collective-permute-start.4 = (bf16[256,2048]{1,0:T(8,128)(2,1)}, bf16[256,2048]{1,0:T(8,128)(2,1)}, u32[]{:S(2)}, u32[]{:S(2)}) collective-permute-start(bf16[256,2048]{1,0:T(8,128)(2,1)} %maximum_select_fusion.1), channel_id=1, source_target_pairs={{0,16},{1,17},{2,18},{3,19},{4,20},{5,21},{6,22},{7,23},{8,24},{9,... | collective-permute-start | bytes 3145736 | tf_op jit(solution)/shard_map/ppermute | solution.py:10
  48.9 1.3 pad_maximum_fusion.1
  50.2 3.9 %collective-permute-start.6 = (bf16[3,2048,128]{1,2,0:T(8,128)(2,1)}, bf16[3,2048,128]{1,2,0:T(8,128)(2,1)}, u32[]{:S(2)}, u32[]{:S(2)}) collective-permute-start(bf16[3,2048,128]{1,2,0:T(8,128)(2,1)} %pad_maximum_fusion.1), channel_id=1, source_target_pairs={{0,64},{1,65},{2,66},{3,67},{4,68},{5,69},{6,70},{7,71},{8,72},{9,... | collective-permute-start | bytes 4718600 | tf_op jit(solution)/shard_map/ppermute | solution.py:10
  54.7 0.9 broadcast_in_dim.19
  55.5 1.9 reshape.147
  57.7 2.0 %scatter_custom_fusion = bf16[256,2048]{1,0:T(8,128)(2,1)S(1)} fusion(s32[96]{0:T(128)S(1)} %fusion.66, bf16[96,2048]{1,0:T(8,128)(2,1)} %reshape.147, bf16[]{:T(256)} %constant.48.clone.1), kind=kCustom, calls=%fused_computation.51 | custom fusion | bytes 1049088 | tf_op jit(solution)/shard_map/scatter | solution.py:192
  59.7 1.6 reshape.129
  61.2 6.1 %all-to-all-start = ((bf16[128,2,2048]{2,1,0:T(2,128)(2,1)}), bf16[128,2,2048]{2,1,0:T(2,128)(2,1)S(1)}, u32[]{:S(2)}, u32[]{:S(2)}) async-start(bf16[128,2,2048]{2,1,0:T(2,128)(2,1)} %reshape.129), calls=%async_computation | async-start | bytes 2097152 | tf_op jit(solution)/shard_map/all_to_all | solution.py:194
  67.3 10.9 %collective-permute-done.4 = bf16[256,2048]{1,0:T(8,128)(2,1)} collective-permute-done((bf16[256,2048]{1,0:T(8,128)(2,1)}, bf16[256,2048]{1,0:T(8,128)(2,1)}, u32[]{:S(2)}, u32[]{:S(2)}) %collective-permute-start.4) | collective-permute-done | bytes 1048608 | tf_op jit(solution)/shard_map/ppermute | solution.py:10
  78.3 3.1 %fusion.70 = f32[1,512]{1,0:T(1,128)S(1)} fusion(f32[2048,1]{0,1:T(1,128)S(1)} %bitcast.80, bf16[256,2048]{1,0:T(8,128)(2,1)} %maximum_select_fusion.1, bf16[256,2048]{1,0:T(8,128)(2,1)} %collective-permute-done.4, pred[]{:T(512)S(6)} %eq.52), kind=kOutput, calls=%fused_computation.122 | convolution fusion | flops 11534336 | bytes 2107393 | tf_op jit(solution)/shard_map/dot_general | solution.py:167
  81.3 15.9 %collective-permute-done.6 = bf16[3,2048,128]{1,2,0:T(8,128)(2,1)} collective-permute-done((bf16[3,2048,128]{1,2,0:T(8,128)(2,1)}, bf16[3,2048,128]{1,2,0:T(8,128)(2,1)}, u32[]{:S(2)}, u32[]{:S(2)}) %collective-permute-start.6) | collective-permute-done | bytes 1572896 | tf_op jit(solution)/shard_map/ppermute | solution.py:10
  97.2 1.6 pad_maximum_fusion
  98.8 1.7 copy-done.4
  100.5 4.0 %fusion.23 = f32[512,256]{1,0:T(8,128)} fusion(bf16[3,2048,256]{1,2,0:T(8,128)(2,1)S(1)} %pad_maximum_fusion, bf16[256,2048]{1,0:T(8,128)(2,1)} %maximum_select_fusion.1, bf16[256,2048]{1,0:T(8,128)(2,1)} %collective-permute-done.4, pred[]{:T(512)S(6)} %eq.52), kind=kOutput, calls=%fused_computation.37 | convolution fusion | flops 546308096 | bytes 3670017 | tf_op jit(solution)/shard_map/dot_general | solution.py:169
  104.4 7.5 %fusion.22 = f32[512,2048]{1,0:T(8,128)} fusion(bf16[3,2048,256]{1,2,0:T(8,128)(2,1)} %copy-done.4, f32[512,256]{1,0:T(8,128)} %fusion.23, f32[512]{0:T(512)S(1)} %add_divide_fusion, bf16[256,2048]{1,0:T(8,128)(2,1)} %maximum_select_fusion.1, bf16[256,2048]{1,0:T(8,128)(2,1)} %collective-permute-done.4, pred[]{:T(512)S(6)} %eq.52), kind=kOutput, calls=%fused_computation.35 | convolution fusion | flops 1084096512 | bytes 8914945 | tf_op jit(solution)/shard_map/dot_general | solution.py:171
  112.0 3.4 %select_convert_fusion = bf16[256,2048]{1,0:T(8,128)(2,1)} fusion(f32[512,2048]{1,0:T(8,128)} %fusion.22, pred[]{:T(512)S(6)} %eq.52), kind=kLoop, calls=%fused_computation.15 | loop fusion | flops 524288 | bytes 3145729 | tf_op jit(solution)/shard_map/convert_element_type | solution.py:182
  116.0 0.8 copy.60
  116.8 0.8 stack_reshape.6
  117.6 1.1 stack_reshape.7
  118.9 1.2 convolution_exponential_fusion
  120.6 18.1 %collective-permute-done.7 = bf16[256,2048]{1,0:T(8,128)(2,1)} collective-permute-done((bf16[256,2048]{1,0:T(8,128)(2,1)}, bf16[256,2048]{1,0:T(8,128)(2,1)}, u32[]{:S(2)}, u32[]{:S(2)}) %collective-permute-start.7) | collective-permute-done | bytes 1048608 | tf_op jit(solution)/shard_map/ppermute | solution.py:10
  138.7 3.0 %convert_add_fusion = f32[256,2048]{1,0:T(8,128)S(1)} fusion(bf16[256,2048]{1,0:T(8,128)(2,1)} %collective-permute-done.7, f32[512,2048]{1,0:T(8,128)} %fusion.22, pred[]{:T(512)S(6)} %eq.52), kind=kLoop, calls=%fused_computation.14 | loop fusion | flops 1572864 | bytes 7340033 | tf_op jit(solution)/shard_map/add | solution.py:181
  141.7 1.3 copy-done.1
  143.0 0.9 select_convert_fusion.1
  143.9 0.8 collective-permute-start.8
  144.7 0.7 pad_maximum_fusion.3
  145.4 1.2 reshape.130
  146.6 3.6 %fusion.6 = f32[256,512]{1,0:T(8,128)} fusion(bf16[256,2048]{1,0:T(8,128)(2,1)} %reshape.130, bf16[1,2048,512]{2,1,0:T(8,128)(2,1)} %param.45), kind=kOutput, calls=%fused_computation.12 | convolution fusion | flops 536870912 | bytes 3670016 | tf_op jit(solution)/shard_map/dot_general | solution.py:96
  150.2 3.4 %collective-permute-done.8 = bf16[128,2048]{1,0:T(8,128)(2,1)} collective-permute-done((bf16[128,2048]{1,0:T(8,128)(2,1)}, bf16[128,2048]{1,0:T(8,128)(2,1)}, u32[]{:S(2)}, u32[]{:S(2)}) %collective-permute-start.8) | collective-permute-done | bytes 524320 | tf_op jit(solution)/shard_map/ppermute | solution.py:10
  153.6 1.2 convert_add_fusion.1
  154.8 0.7 select_convert_fusion.2
  155.6 3.1 %collective-permute-start.9 = (bf16[64,2048]{1,0:T(8,128)(2,1)}, bf16[64,2048]{1,0:T(8,128)(2,1)S(1)}, u32[]{:S(2)}, u32[]{:S(2)}) collective-permute-start(bf16[64,2048]{1,0:T(8,128)(2,1)} %select_convert_fusion.2), channel_id=1, source_target_pairs={{0,4},{1,5},{2,6},{3,7},{4,0},{5,1},{6,2},{7,3},{8,12},{9,13},{10,... | collective-permute-start | bytes 786440 | tf_op jit(solution)/shard_map/ppermute | solution.py:10
  158.6 4.3 %convolution_convert_fusion = bf16[256,2048]{1,0:T(8,128)(2,1)} fusion(bf16[1,512,2048]{2,1,0:T(8,128)(2,1)S(1)} %copy-done, bf16[256,2048]{1,0:T(8,128)(2,1)} %reshape.130, bf16[1,2048,512]{2,1,0:T(8,128)(2,1)} %param.46, f32[256,512]{1,0:T(8,128)} %fusion.6), kind=kOutput, calls=%fused_computation.4 | convolution fusion | flops 1075052544 | bytes 6815744 | tf_op jit(solution)/shard_map/dot_general | solution.py:99
  162.9 2.5 %reshape.131 = bf16[128,2,2048]{2,1,0:T(2,128)(2,1)} reshape(bf16[256,2048]{1,0:T(8,128)(2,1)} %convolution_convert_fusion) | data formatting | bytes 2097152 | tf_op jit(solution)/shard_map/reshape | solution.py:198
  165.5 6.5 %all-to-all-start.1 = ((bf16[128,2,2048]{2,1,0:T(2,128)(2,1)}), bf16[128,2,2048]{2,1,0:T(2,128)(2,1)}, u32[]{:S(2)}, u32[]{:S(2)}) async-start(bf16[128,2,2048]{2,1,0:T(2,128)(2,1)} %reshape.131), calls=%async_computation.1 | async-start | bytes 2097152 | tf_op jit(solution)/shard_map/all_to_all | solution.py:197
  172.1 0.8 copy-done.3
  172.9 0.7 select_convert_fusion.3
  173.6 0.9 collective-permute-start.10
  174.6 16.7 %all-to-all-done.1 = bf16[128,2,2048]{2,1,0:T(2,128)(2,1)} async-done(((bf16[128,2,2048]{2,1,0:T(2,128)(2,1)}), bf16[128,2,2048]{2,1,0:T(2,128)(2,1)}, u32[]{:S(2)}, u32[]{:S(2)}) %all-to-all-start.1) | async-done | bytes 1048608 | tf_op jit(solution)/shard_map/all_to_all | solution.py:197
  191.3 1.5 reshape.132
  192.7 0.8 gather_fusion
  193.7 1.2 convert_add_fusion.3
  195.0 0.4 multiply_reduce_fusion
  195.4 0.8 collective-permute-done.11
  196.2 0.7 add_convert_fusion
  (113 shorter events, 4.5 us)
Async XLA Ops:
  0.6 158.0 %copy-start = (bf16[1,512,2048]{2,1,0:T(8,128)(2,1)S(1)}, bf16[1,512,2048]{2,1,0:T(8,128)(2,1)}, u32[]{:S(2)}) copy-start(bf16[1,512,2048]{2,1,0:T(8,128)(2,1)} %param.47) | copy-start | bytes 6291460
  0.6 4.1 %copy-start.25 = (f32[2,16,2048]{2,1,0:T(8,128)S(1)}, f32[2,16,2048]{2,1,0:T(8,128)}, u32[]{:S(2)}) copy-start(f32[2,16,2048]{2,1,0:T(8,128)} %param.27) | copy-start | bytes 786436
  0.7 4.4 %copy-start.28 = (f32[32,64]{1,0:T(8,128)S(1)}, f32[32,64]{1,0:T(8,128)}, u32[]{:S(2)}) copy-start(f32[32,64]{1,0:T(8,128)} %param.31) | copy-start | bytes 24580
  0.7 4.4 %copy-start.29 = (f32[32,64]{1,0:T(8,128)S(1)}, f32[32,64]{1,0:T(8,128)}, u32[]{:S(2)}) copy-start(f32[32,64]{1,0:T(8,128)} %param.30) | copy-start | bytes 24580
  0.7 4.5 %copy-start.19 = (f32[32,64,16]{1,2,0:T(8,128)S(1)}, f32[32,64,16]{1,2,0:T(8,128)}, u32[]{:S(2)}) copy-start(f32[32,64,16]{1,2,0:T(8,128)} %param.34) | copy-start | bytes 393220
  0.7 4.5 %copy-start.20 = (f32[32,64,16]{1,2,0:T(8,128)S(1)}, f32[32,64,16]{1,2,0:T(8,128)}, u32[]{:S(2)}) copy-start(f32[32,64,16]{1,2,0:T(8,128)} %param.33) | copy-start | bytes 393220
  5.0 1.8 copy-start.24
  5.0 1.9 copy-start.26
  5.6 1.3 copy-start.15
  5.7 1.8 copy-start.31
  5.7 2.3 %copy-start.21 = (bf16[16,2048]{1,0:T(8,128)(2,1)S(1)}, bf16[16,2048]{1,0:T(8,128)(2,1)}, u32[]{:S(2)}) copy-start(bf16[16,2048]{1,0:T(8,128)(2,1)} %param.26) | copy-start | bytes 196612
  6.1 0.7 copy-start.13
  6.8 1.0 copy-start.22
  7.2 3.3 %copy-start.30 = (f32[2048]{0:T(1024)S(1)}, f32[2048]{0:T(1024)}, u32[]{:S(2)}) copy-start(f32[2048]{0:T(1024)} %param.41) | copy-start | bytes 24580
  7.8 13.7 %copy-start.7 = (bf16[64,2048]{1,0:T(8,128)(2,1)S(1)}, bf16[64,2048]{1,0:T(8,128)(2,1)}, u32[]{:S(2)}) copy-start(bf16[64,2048]{1,0:T(8,128)(2,1)} %param.51) | copy-start | bytes 786436
  7.8 13.7 %copy-start.8 = (bf16[2048,64]{0,1:T(8,128)(2,1)S(1)}, bf16[2048,64]{0,1:T(8,128)(2,1)}, u32[]{:S(2)}) copy-start(bf16[2048,64]{0,1:T(8,128)(2,1)} %param.50) | copy-start | bytes 786436
  7.8 13.7 %copy-start.10 = (bf16[2048,64]{0,1:T(8,128)(2,1)S(1)}, bf16[2048,64]{0,1:T(8,128)(2,1)}, u32[]{:S(2)}) copy-start(bf16[2048,64]{0,1:T(8,128)(2,1)} %param.49) | copy-start | bytes 786436
  10.5 11.0 %copy-start.17 = (f32[16,2048]{1,0:T(8,128)}, f32[16,2048]{1,0:T(8,128)S(1)}, u32[]{:S(2)}) copy-start(f32[16,2048]{1,0:T(8,128)S(1)} %get-tuple-element.13) | copy-start | bytes 393220
  10.6 1.3 collective-permute-start
  12.0 5.6 %collective-permute-start.1 = (bf16[32,2048]{1,0:T(8,128)(2,1)S(1)}, bf16[32,2048]{1,0:T(8,128)(2,1)S(1)}, u32[]{:S(2)}, u32[]{:S(2)}) collective-permute-start(bf16[32,2048]{1,0:T(8,128)(2,1)S(1)} %maximum_select_fusion.4), channel_id=1, source_target_pairs={{0,2},{1,3},{2,0},{3,1},{4,6},{5,7},{6,4},{7,5},{8,10},{9,11},{10,... | collective-permute-start | bytes 393224 | tf_op jit(solution)/shard_map/ppermute | solution.py:10
  18.4 9.3 %collective-permute-start.2 = (bf16[64,2048]{1,0:T(8,128)(2,1)}, bf16[64,2048]{1,0:T(8,128)(2,1)}, u32[]{:S(2)}, u32[]{:S(2)}) collective-permute-start(bf16[64,2048]{1,0:T(8,128)(2,1)} %maximum_select_fusion.3), channel_id=1, source_target_pairs={{0,4},{1,5},{2,6},{3,7},{4,0},{5,1},{6,2},{7,3},{8,12},{9,13},{10,... | collective-permute-start | bytes 786440 | tf_op jit(solution)/shard_map/ppermute | solution.py:10
  22.5 26.4 %collective-permute-start.5 = (bf16[3,2048,64]{1,2,0:T(8,128)(2,1)}, bf16[3,2048,64]{1,2,0:T(8,128)(2,1)S(1)}, u32[]{:S(2)}, u32[]{:S(2)}) collective-permute-start(bf16[3,2048,64]{1,2,0:T(8,128)(2,1)} %pad_maximum_fusion.2), channel_id=1, source_target_pairs={{0,32},{1,33},{2,34},{3,35},{4,36},{5,37},{6,38},{7,39},{8,40},{9,... | collective-permute-start | bytes 2359304 | tf_op jit(solution)/shard_map/ppermute | solution.py:10
  30.0 12.6 %collective-permute-start.3 = (bf16[128,2048]{1,0:T(8,128)(2,1)}, bf16[128,2048]{1,0:T(8,128)(2,1)}, u32[]{:S(2)}, u32[]{:S(2)}) collective-permute-start(bf16[128,2048]{1,0:T(8,128)(2,1)} %maximum_select_fusion.2), channel_id=1, source_target_pairs={{0,8},{1,9},{2,10},{3,11},{4,12},{5,13},{6,14},{7,15},{8,0},{9,1},... | collective-permute-start | bytes 1572872 | tf_op jit(solution)/shard_map/ppermute | solution.py:10
  31.6 17.2 %copy-start.11 = (bf16[2048,64]{0,1:T(8,128)(2,1)S(1)}, bf16[2048,64]{0,1:T(8,128)(2,1)}, u32[]{:S(2)}) copy-start(bf16[2048,64]{0,1:T(8,128)(2,1)} %param.49) | copy-start | bytes 786436
  45.6 8.5 %copy-start.27 = (s32[16,6]{0,1:T(8,128)S(1)}, s32[16,6]{0,1:T(8,128)}, u32[]{:S(2)}) copy-start(s32[16,6]{0,1:T(8,128)} %param.44) | copy-start | bytes 1156
  45.6 32.7 %collective-permute-start.4 = (bf16[256,2048]{1,0:T(8,128)(2,1)}, bf16[256,2048]{1,0:T(8,128)(2,1)}, u32[]{:S(2)}, u32[]{:S(2)}) collective-permute-start(bf16[256,2048]{1,0:T(8,128)(2,1)} %maximum_select_fusion.1), channel_id=1, source_target_pairs={{0,16},{1,17},{2,18},{3,19},{4,20},{5,21},{6,22},{7,23},{8,24},{9,... | collective-permute-start | bytes 3145736 | tf_op jit(solution)/shard_map/ppermute | solution.py:10
  48.9 8.6 %copy-start.5 = (bf16[3,2048,64]{1,2,0:T(8,128)(2,1)}, bf16[3,2048,64]{1,2,0:T(8,128)(2,1)S(1)}, u32[]{:S(2)}) copy-start(bf16[3,2048,64]{1,2,0:T(8,128)(2,1)S(1)} %collective-permute-done.5) | copy-start | bytes 2359300
  50.2 47.0 %collective-permute-start.6 = (bf16[3,2048,128]{1,2,0:T(8,128)(2,1)}, bf16[3,2048,128]{1,2,0:T(8,128)(2,1)}, u32[]{:S(2)}, u32[]{:S(2)}) collective-permute-start(bf16[3,2048,128]{1,2,0:T(8,128)(2,1)} %pad_maximum_fusion.1), channel_id=1, source_target_pairs={{0,64},{1,65},{2,66},{3,67},{4,68},{5,69},{6,70},{7,71},{8,72},{9,... | collective-permute-start | bytes 4718600 | tf_op jit(solution)/shard_map/ppermute | solution.py:10
  59.7 18.6 %copy-start.33 = (f32[2048]{0:T(1024)S(1)}, f32[2048]{0:T(1024)}, u32[]{:S(2)}) copy-start(f32[2048]{0:T(1024)} %param.48) | copy-start | bytes 24580
  61.2 84.2 %all-to-all-start = ((bf16[128,2,2048]{2,1,0:T(2,128)(2,1)}), bf16[128,2,2048]{2,1,0:T(2,128)(2,1)S(1)}, u32[]{:S(2)}, u32[]{:S(2)}) async-start(bf16[128,2,2048]{2,1,0:T(2,128)(2,1)} %reshape.129), calls=%async_computation | async-start | bytes 2097152 | tf_op jit(solution)/shard_map/all_to_all | solution.py:194
  78.3 18.9 %copy-start.6 = (bf16[3,2048,64]{1,2,0:T(8,128)(2,1)S(1)}, bf16[3,2048,64]{1,2,0:T(8,128)(2,1)}, u32[]{:S(2)}) copy-start(bf16[3,2048,64]{1,2,0:T(8,128)(2,1)} %copy-done.5) | copy-start | bytes 2359300
  78.3 18.9 %copy-start.9 = (bf16[2048,64]{0,1:T(8,128)(2,1)S(1)}, bf16[2048,64]{0,1:T(8,128)(2,1)}, u32[]{:S(2)}) copy-start(bf16[2048,64]{0,1:T(8,128)(2,1)} %param.50) | copy-start | bytes 786436
  78.3 18.9 %copy-start.12 = (bf16[2048,64]{0,1:T(8,128)(2,1)S(1)}, bf16[2048,64]{0,1:T(8,128)(2,1)}, u32[]{:S(2)}) copy-start(bf16[2048,64]{0,1:T(8,128)(2,1)} %param.49) | copy-start | bytes 786436
  98.8 1.7 copy-start.4
  111.9 3.8 %copy-start.32 = (bf16[2048,4]{0,1:T(4,128)(2,1)S(1)}, bf16[2048,4]{0,1:T(4,128)(2,1)}, u32[]{:S(2)}) copy-start(bf16[2048,4]{0,1:T(4,128)(2,1)} %param.42) | copy-start | bytes 49156
  112.0 3.9 %copy-start.14 = (f32[16,32,64]{2,0,1:T(8,128)S(1)}, f32[16,32,64]{2,0,1:T(8,128)}, u32[]{:S(2)}) copy-start(f32[16,32,64]{2,0,1:T(8,128)} %copy-done.13) | copy-start | bytes 393220
  112.0 4.0 %copy-start.16 = (f32[16,32,64]{2,0,1:T(8,128)S(1)}, f32[16,32,64]{2,0,1:T(8,128)}, u32[]{:S(2)}) copy-start(f32[16,32,64]{2,0,1:T(8,128)} %copy-done.15) | copy-start | bytes 393220
  115.4 23.3 %collective-permute-start.7 = (bf16[256,2048]{1,0:T(8,128)(2,1)}, bf16[256,2048]{1,0:T(8,128)(2,1)}, u32[]{:S(2)}, u32[]{:S(2)}) collective-permute-start(bf16[256,2048]{1,0:T(8,128)(2,1)} %select_convert_fusion), channel_id=1, source_target_pairs={{0,16},{1,17},{2,18},{3,19},{4,20},{5,21},{6,22},{7,23},{8,24},{9,... | collective-permute-start | bytes 3145736 | tf_op jit(solution)/shard_map/ppermute | solution.py:10
  120.6 24.1 %copy-start.23 = (f32[1,16,2048]{2,1,0:T(8,128)S(1)}, f32[1,16,2048]{2,1,0:T(8,128)}, u32[]{:S(2)}) copy-start(f32[1,16,2048]{2,1,0:T(8,128)} %stack_reshape.6) | copy-start | bytes 393220
  141.7 1.3 copy-start.1
  143.9 9.7 %collective-permute-start.8 = (bf16[128,2048]{1,0:T(8,128)(2,1)}, bf16[128,2048]{1,0:T(8,128)(2,1)}, u32[]{:S(2)}, u32[]{:S(2)}) collective-permute-start(bf16[128,2048]{1,0:T(8,128)(2,1)} %select_convert_fusion.1), channel_id=1, source_target_pairs={{0,8},{1,9},{2,10},{3,11},{4,12},{5,13},{6,14},{7,15},{8,0},{9,1},... | collective-permute-start | bytes 1572872 | tf_op jit(solution)/shard_map/ppermute | solution.py:10
  146.6 7.0 %copy-start.2 = (f32[256,2048]{1,0:T(8,128)S(1)}, f32[256,2048]{1,0:T(8,128)}, u32[]{:S(2)}) copy-start(f32[256,2048]{1,0:T(8,128)} %copy-done.1) | copy-start | bytes 6291460
  155.6 16.4 %collective-permute-start.9 = (bf16[64,2048]{1,0:T(8,128)(2,1)}, bf16[64,2048]{1,0:T(8,128)(2,1)S(1)}, u32[]{:S(2)}, u32[]{:S(2)}) collective-permute-start(bf16[64,2048]{1,0:T(8,128)(2,1)} %select_convert_fusion.2), channel_id=1, source_target_pairs={{0,4},{1,5},{2,6},{3,7},{4,0},{5,1},{6,2},{7,3},{8,12},{9,13},{10,... | collective-permute-start | bytes 786440 | tf_op jit(solution)/shard_map/ppermute | solution.py:10
  165.5 25.8 %all-to-all-start.1 = ((bf16[128,2,2048]{2,1,0:T(2,128)(2,1)}), bf16[128,2,2048]{2,1,0:T(2,128)(2,1)}, u32[]{:S(2)}, u32[]{:S(2)}) async-start(bf16[128,2,2048]{2,1,0:T(2,128)(2,1)} %reshape.131), calls=%async_computation.1 | async-start | bytes 2097152 | tf_op jit(solution)/shard_map/all_to_all | solution.py:197
  172.1 0.8 copy-start.3
  173.6 20.1 %collective-permute-start.10 = (bf16[32,2048]{1,0:T(8,128)(2,1)}, bf16[32,2048]{1,0:T(8,128)(2,1)}, u32[]{:S(2)}, u32[]{:S(2)}) collective-permute-start(bf16[32,2048]{1,0:T(8,128)(2,1)} %select_convert_fusion.3), channel_id=1, source_target_pairs={{0,2},{1,3},{2,0},{3,1},{4,6},{5,7},{6,4},{7,5},{8,10},{9,11},{10,... | collective-permute-start | bytes 393224 | tf_op jit(solution)/shard_map/ppermute | solution.py:10
  193.7 2.5 %copy-start.18 = (f32[16,2048]{1,0:T(8,128)S(1)}, f32[16,2048]{1,0:T(8,128)}, u32[]{:S(2)}) copy-start(f32[16,2048]{1,0:T(8,128)} %copy-done.17) | copy-start | bytes 393220
  194.9 1.3 collective-permute-start.11
where the time goes:
time: 199 us; the launch traced here: 197 us
  waiting for transfers between devices  85.2 us (43%)
  starting transfers between devices  33.4 us (17%)
  matrix products  29.6 us (15%)
  other arithmetic  25 us (13%)
  local copies, waits for them, and re-layouts  22.4 us (11%)
    ppermute x12, waiting for transfers between devices, from_partner(): lax.ppermute(array, axis, [(i, i ^ 1 << bit) for i in range(lax.axis_size...  68.5 us
    ppermute x12, starting transfers between devices, from_partner(): lax.ppermute(array, axis, [(i, i ^ 1 << bit) for i in range(lax.axis_size...  20.8 us
    all_to_all x1, waiting for transfers between devices, on_device(): lax.all_to_all(result.reshape(senders, items, inner_width), 'ep', split_a...  16.7 us
    dot_general x1, matrix products, on_device(): lax.dot_general(block_hidden, packed[2], (((1,), (1,)), ((), ())), prefer...  7.53 us
    all_to_all x1, starting transfers between devices, on_device(): lax.all_to_all(result.reshape(senders, items, inner_width), 'ep', split_a...  6.54 us
    all_to_all x1, starting transfers between devices, on_device(): lax.all_to_all(outgoing, 'ep', split_axis=0, concat_axis=0, tiled=True)  6.08 us
    select_n x4, other arithmetic, on_device(): jnp.where(upper, jnp.concatenate([other, block], 0), jnp.concatenate([blo...  6.06 us
    convert_element_type x5, other arithmetic, on_device(): outgoing_half.astype(jnp.bfloat16)  5.76 us
  transfers between devices with their start and end apart: 14, of which 10 were waited for; matrix products, arithmetic and copies ran while one was open for 30% of the time, Pallas kernels for 0%

commit v1 on v0

v1 whole, which is shorter than its diff:
```python
import jax
import jax.numpy as jnp
from jax import lax
from jax.experimental import pallas as pl
from jax.experimental.pallas import tpu as pltpu
from jax.sharding import PartitionSpec as P

EPS = 1e-05
F32 = jnp.float32
BF16 = jnp.bfloat16
MESH = pl.DeviceIdType.MESH
ORDERS = (("x", "y", "z"), ("y", "z", "x"), ("z", "x", "y"))
GATHER_COLS = ((0, 768), (768, 768), (1536, 768))
SCATTER_COLS = ((0, 768), (768, 512), (1280, 768))
KINDS = (
    [("m1", 0, s) for s in (1, -1)]
    + [("f1", 0, s) for s in (1, -1)]
    + [("m2", o, s) for o in (0, 1, 3, 2) for s in (1, -1)]
    + [("f2", 0, 1), ("f2", 1, 1), ("f2", 3, -1), ("f2", 2, -1)]
    + [("m3a", o, s) for o in (0, 1, 3, 2) for s in (1, -1)]
    + [("m3", o, s) for o in (1, 3, 2) for s in (1, -1)]
    + [("f3", 0, 1), ("f3", 1, 1), ("f3", 3, -1), ("f3", 2, -1)]
)
SLOT = {kind: i for i, kind in enumerate(KINDS)}
FORWARD_PLUS = (0, 1)


def dot(a, b):
    return jnp.dot(a, b, preferred_element_type=F32)


def dot_nt(a, b):
    return lax.dot_general(a, b, (((1,), (1,)), ((), ())), preferred_element_type=F32)


def layer_kernel(
    normed_ref,
    resid_ref,
    ids_ref,
    vector_ref,
    group_ref,
    router_ref,
    gate_hbm,
    up_hbm,
    down_hbm,
    eg_hbm,
    eu_hbm,
    ed_hbm,
    out_ref,
    own,
    x,
    w_in,
    w_out,
    eg,
    eu,
    ed,
    hc,
    ct,
    picked,
    group_rows,
    p,
    r1,
    r2,
    r3,
    local_sem,
    swap_send,
    swap_recv,
    ag_send,
    ag_recv,
    rs_send,
    rs_recv,
):
    me = lax.axis_index("ep")
    core = lax.rem(me, 2)
    pos = {"x": lax.rem(me // 2, 4), "y": lax.rem(me // 8, 4), "z": me // 32}
    near = {d: [lax.rem(pos[d] + k, 4) for k in range(4)] for d in "xyz"}

    def device(at):
        return ((at["z"] * 4 + at["y"]) * 4 + at["x"]) * 2 + core

    def neighbour(d, s):
        at = dict(pos)
        at[d] = near[d][s % 4]
        return device(at)

    peers = {(d, s): neighbour(d, s) for d in "xyz" for s in (1, -1)}
    partner = me + 1 - 2 * core

    barrier = pltpu.get_barrier_semaphore()
    for peer in [*peers.values(), partner]:
        pl.semaphore_signal(barrier, inc=1, device_id=(peer,), device_id_type=MESH)

    def rows(i):
        return pl.ds(pl.multiple_of(i * 64, 64), 64)

    weights = [
        (gate_hbm, w_in.at[rows(core)]),
        (up_hbm, w_in.at[rows(2 + core)]),
        (down_hbm, w_out.at[rows(core)]),
        (eg_hbm, eg.at[core]),
        (eu_hbm, eu.at[core]),
        (ed_hbm, ed.at[core]),
    ]
    local = [pltpu.make_async_copy(s, t, local_sem.at[i]) for i, (s, t) in enumerate(weights)]
    for copy in local:
        copy.start()
    swaps = [
        pltpu.make_async_remote_copy(
            src_ref=s,
            dst_ref=t,
            send_sem=swap_send.at[i],
            recv_sem=swap_recv.at[i],
            device_id=(partner,),
            device_id_type=MESH,
        )
        for i, (s, t) in enumerate(weights)
    ]

    normed = normed_ref[...]
    own[:, pl.ds(0, 2048)] = normed
    ids = ids_ref[...]
    lanes = lax.broadcasted_iota(jnp.int32, (16, 128), 1)
    chosen = jnp.zeros((16, 128), F32)
    for t in range(6):
        chosen = chosen + jnp.where(ids[:, t : t + 1] == lanes, 1.0, 0.0)
    earlier = jnp.where(
        lax.broadcasted_iota(jnp.int32, (16, 16), 1) < lax.broadcasted_iota(jnp.int32, (16, 16), 0),
        1.0,
        0.0,
    )
    ordinal = dot(earlier.astype(BF16), chosen.astype(BF16))
    own[:, pl.ds(2048, 128)] = (chosen * (1.0 + ordinal)).astype(BF16)
    branch = jax.nn.sigmoid(
        jnp.sum(normed.astype(F32) * vector_ref[...], axis=1, keepdims=True)
    )
    high = branch.astype(BF16).astype(F32)
    middle = (branch - high).astype(BF16).astype(F32)
    low = branch - high - middle
    extra = jnp.where(lanes == 0, high, jnp.where(lanes == 1, middle, jnp.where(lanes == 2, low, 0.0)))
    own[:, pl.ds(2176, 128)] = extra.astype(BF16)
    own_copy = pltpu.make_async_copy(
        own, x.at[pos["z"], pos["y"], pos["x"]], local_sem.at[6]
    )
    own_copy.start()

    pl.semaphore_wait(barrier, 7)
    for copy in swaps:
        copy.start()

    def view(ref, colour, offsets, cols):
        at = {}
        for d, o in zip(ORDERS[colour], offsets):
            at[d] = slice(None) if o is None else near[d][o % 4]
        return ref.at[at["z"], at["y"], at["x"], :, cols]

    def gather_copy(colour, kind, receiving=False):
        name, o, s = kind
        start, width = GATHER_COLS[colour]
        cols = pl.ds(start, width)
        order = ORDERS[colour]
        back = -s if receiving else 0
        if name == "m1":
            d, where = order[0], (back, 0, 0)
        elif name == "f1":
            d, where = order[0], (back - s, 0, 0)
            half = width // 2
            cols = pl.ds(start, half) if s == 1 else pl.ds(start + half, half)
        elif name == "m2":
            d, where = order[1], (o, back, 0)
        elif name == "f2":
            d, where = order[1], (o, back - s, 0)
        elif name == "m3a":
            d, where = order[2], (o, 0, back)
        elif name == "m3":
            d, where = order[2], (None, o, back)
        else:
            d, where = order[2], (None, o, back - s)
        target = view(x, colour, where, cols)
        source = target
        if name == "m1" or (name in ("m2", "m3a") and o == 0):
            source = own.at[:, cols]
            if receiving:
                source = target
        i = SLOT[kind]
        return pltpu.make_async_remote_copy(
            src_ref=source,
            dst_ref=target,
            send_sem=ag_send.at[colour, i],
            recv_sem=ag_recv.at[colour, i],
            device_id=(peers[d, s],),
            device_id_type=MESH,
        )

    started = []

    def send(colour, name, o, s):
        copy = gather_copy(colour, (name, o, s))
        copy.start()
        started.append(copy)

    def both(colour, name, o):
        send(colour, name, o, 1)
        send(colour, name, o, -1)

    def receive(colour, name, o, s):
        gather_copy(colour, (name, o, s), True).wait_recv()

    colours = range(3)
    for c in colours:
        both(c, "m1", 0)
    for c in colours:
        both(c, "m2", 0)
    for c in colours:
        both(c, "m3a", 0)
    own_copy.wait()
    for s in (1, -1):
        for c in colours:
            receive(c, "m1", 0, s)
            o = 3 if s == 1 else 1
            send(c, "f1", 0, s)
            both(c, "m2", o)
            both(c, "m3a", o)
    for c in colours:
        receive(c, "m2", 0, 1)
        send(c, "f2", 0, 1)
        receive(c, "m2", 0, -1)
    for c in colours:
        receive(c, "f1", 0, 1)
        receive(c, "f1", 0, -1)
        both(c, "m2", 2)
        both(c, "m3a", 2)
    for o in (3, 1):
        for c in colours:
            receive(c, "m2", o, 1)
            if o == 1:
                send(c, "f2", 1, 1)
            receive(c, "m2", o, -1)
            if o == 3:
                send(c, "f2", 3, -1)
    for c in colours:
        receive(c, "m2", 2, 1)
        receive(c, "m2", 2, -1)
        send(c, "f2", 2, -1)
        both(c, "m3", 3)
        both(c, "m3", 1)
    for c in colours:
        for o in (0, 1, 3, 2):
            receive(c, "m3a", o, 1)
        send(c, "f3", 0, 1)
        for o in (0, 1, 3, 2):
            receive(c, "m3a", o, -1)
    for c in colours:
        for o, s in ((0, 1), (1, 1), (3, -1), (2, -1)):
            receive(c, "f2", o, s)
        both(c, "m3", 2)
    for c in colours:
        receive(c, "m3", 3, 1)
        receive(c, "m3", 3, -1)
        send(c, "f3", 3, -1)
        receive(c, "m3", 1, 1)
        send(c, "f3", 1, 1)
        receive(c, "m3", 1, -1)
    for c in colours:
        receive(c, "m3", 2, 1)
        receive(c, "m3", 2, -1)
        send(c, "f3", 2, -1)
    for c in colours:
        for o, s in ((0, 1), (1, 1), (3, -1), (2, -1)):
            receive(c, "f3", o, s)

    for copy in local:
        copy.wait()
    for copy in swaps:
        copy.wait_recv()

    first = me - core

    @pl.loop(0, 4)
    def _(zi):
        block = x.at[zi]
        values = block[:, :, :, pl.ds(0, 2048)].reshape(256, 2048)
        products = dot_nt(values, w_in[...])
        gate_part = products[:, :128]
        up_part = products[:, 128:]
        extras = block[:, :, :, pl.ds(2176, 128)].reshape(256, 128)
        scale = dot(extras, jnp.ones((128, 128), BF16))
        hidden = (scale * jax.nn.silu(gate_part) * up_part).astype(BF16)
        hc[zi, :, :, :, pl.ds(0, 128)] = hidden.reshape(4, 4, 16, 128)
        table = block[:, :, :, pl.ds(2048, 128)].reshape(256, 128)
        slot = lax.broadcasted_iota(jnp.int32, (128, 256), 1)
        expert_of = jnp.where(
            lax.broadcasted_iota(jnp.int32, (128, 256), 0) == first + slot // 128, 1.0, 0.0
        ).astype(BF16)
        entry = dot(table, expert_of)
        row = lax.broadcasted_iota(jnp.int32, (256, 256), 0)
        lane = lax.broadcasted_iota(jnp.int32, (256, 256), 1)
        wanted = (lax.rem(lane // 64, 2) + 1).astype(F32)
        sender = lax.rem(lane, 64)
        hit = (entry == wanted) & (sender == zi * 16 + row // 16)
        hc[zi, :, :, :, pl.ds(128, 256)] = (
            jnp.where(hit, 1.0, 0.0).astype(BF16).reshape(4, 4, 16, 256)
        )
        slot_t = lax.broadcasted_iota(jnp.int32, (256, 128), 0)
        expert_t = jnp.where(
            lax.broadcasted_iota(jnp.int32, (256, 128), 1) == first + slot_t // 128, 1.0, 0.0
        ).astype(BF16)
        entry_t = dot_nt(expert_t, table)
        wanted_t = (lax.rem(row // 64, 2) + 1).astype(F32)
        hit_t = (entry_t == wanted_t) & (lax.rem(row, 64) == zi * 16 + lane // 16)
        ct[:, pl.ds(pl.multiple_of(zi * 256, 256), 256)] = jnp.where(hit_t, 1.0, 0.0).astype(BF16)

    pick = ct[...]

    @pl.loop(0, 4)
    def _(j):
        cols = pl.ds(pl.multiple_of(j * 512, 512), 512)
        picked[:, cols] = dot(pick, x[:, :, :, :, cols].reshape(1024, 512)).astype(BF16)

    choices = dot(pick, x[:, :, :, :, pl.ds(2048, 128)].reshape(1024, 128))

    for g in range(4):
        group_rows[pl.ds(32 * g, 32), :] = jnp.broadcast_to(
            group_ref[pl.ds(g, 1), :].astype(F32), (32, 2048)
        ).astype(BF16)
    selected = picked[...]
    group_exp = jnp.exp(dot_nt(selected, group_rows[...]))
    inner_exp = jnp.exp(dot(selected, router_ref[...]))
    lane = lax.broadcasted_iota(jnp.int32, (256, 128), 1)
    row = lax.broadcasted_iota(jnp.int32, (256, 128), 0)
    group_sum = jnp.sum(jnp.where(lax.rem(lane, 32) == 0, group_exp, 0.0), axis=1, keepdims=True)
    inner_sum = jnp.zeros((256, 128), F32)
    for g in range(4):
        inside = lane // 32 == g
        total = jnp.sum(jnp.where(inside, inner_exp, 0.0), axis=1, keepdims=True)
        inner_sum = jnp.where(inside, total, inner_sum)
    inner = inner_exp / inner_sum
    joint = (group_exp / group_sum) * inner
    mine = lane == first + row // 128
    numerator = jnp.sum(jnp.where(mine, joint, 0.0), axis=1, keepdims=True)
    taken = choices > 0.0
    denominator = jnp.sum(jnp.where(taken, inner, 0.0), axis=1, keepdims=True)
    live = jnp.sum(jnp.where(taken, 1.0, 0.0), axis=1, keepdims=True) > 0.0
    gates = jnp.where(live, numerator / jnp.where(live, denominator, 1.0), 0.0)

    for e in range(2):
        rows_in = selected[e * 128 : (e + 1) * 128]
        gate_part = dot(rows_in, eg[e])
        up_part = dot(rows_in, eu[e])
        hidden = (jax.nn.silu(gate_part) * up_part).astype(BF16)
        result = dot(hidden, ed[e])
        weighted = result * gates[e * 128 : (e + 1) * 128]
        w_out[pl.ds(128 + e * 128, 128), :] = weighted.astype(BF16)

    def scatter_copy(colour, kind, receiving=False):
        name, o, s = kind
        start, width = SCATTER_COLS[colour]
        cols = pl.ds(start, width)
        order = ORDERS[colour]
        half = width // 2
        k = 0 if s == 1 else 1
        if name == "m1":
            d, where = order[0], (-s, 0, 0)
            target = r1.at[colour, k, :, pl.ds(0, width)]
        elif name == "f1":
            d, where = order[0], (2, 0, 0)
            cols = pl.ds(start, half) if s == 1 else pl.ds(start + half, half)
            target = r1.at[colour, 2 + k, :, pl.ds(0, half)]
        elif name == "m2":
            d, where = order[1], (o, -s, 0)
            target = r2.at[colour, k, o, :, pl.ds(0, width)]
        elif name == "f2":
            d, where = order[1], (o, 2, 0)
            target = r2.at[colour, 2, o, :, pl.ds(0, width)]
        elif name == "m3":
            d, where = order[2], (None, o, -s)
            target = r3.at[colour, k, o, :, :, pl.ds(0, width)]
        else:
            d, where = order[2], (None, o, 2)
            target = r3.at[colour, 2, o, :, :, pl.ds(0, width)]
        i = SLOT[kind] if kind in SLOT else SLOT["m3a", o, s]
        return pltpu.make_async_remote_copy(
            src_ref=target if receiving else view(p, colour, where, cols),
            dst_ref=target,
            send_sem=rs_send.at[colour, i],
            recv_sem=rs_recv.at[colour, i],
            device_id=(peers[d, -s],),
            device_id_type=MESH,
        )

    def pass_on(colour, name, o, s):
        copy = scatter_copy(colour, (name, o, s))
        copy.start()
        started.append(copy)

    def arrive(colour, name, o, s):
        scatter_copy(colour, (name, o, s), True).wait_recv()

    def partial(colour, o):
        start, width = SCATTER_COLS[colour]
        d = ORDERS[colour][2]
        i = near[d][o]
        cols = pl.ds(start, width)
        if d == "z":
            left = hc[i]
        elif d == "y":
            left = hc[:, i]
        else:
            left = hc[:, :, i]
        values = dot(left.reshape(256, 384), w_out[:, cols]).astype(BF16).reshape(4, 4, 16, width)
        if d == "z":
            p[i, :, :, :, cols] = values
        elif d == "y":
            p[:, i, :, :, cols] = values
        else:
            p[:, :, i, :, cols] = values

    def block(colour, where, cols=None):
        start, width = SCATTER_COLS[colour]
        return view(p, colour, where, pl.ds(start, width) if cols is None else cols)

    def add(colour, where, *arrived, cols=None):
        ref = block(colour, where, cols)
        total = ref[...].astype(F32)
        for a in arrived:
            total = total + a[...].astype(F32)
        ref[...] = total.astype(BF16)

    def in3(c, k, o):
        return r3.at[c, k, o, :, :, pl.ds(0, SCATTER_COLS[c][1])]

    def in2(c, k, o):
        return r2.at[c, k, o, :, pl.ds(0, SCATTER_COLS[c][1])]

    backwards = (2, 3, 1, 0)

    def sign_of(o):
        return 1 if o in FORWARD_PLUS else -1

    for c in colours:
        partial(c, 2)
        for o in backwards:
            pass_on(c, "f3", o, sign_of(o))
    for s in (1, -1):
        for c in colours:
            partial(c, (-s) % 4)
            for o in backwards:
                if sign_of(o) != s:
                    pass_on(c, "m3", o, s)
    for c in colours:
        partial(c, 0)
    for o in backwards:
        for c in colours:
            s = sign_of(o)
            arrive(c, "f3", o, s)
            add(c, (None, o, -s), in3(c, 2, o))
            pass_on(c, "m3", o, s)
    for o in backwards:
        for c in colours:
            arrive(c, "m3", o, 1)
            arrive(c, "m3", o, -1)
            add(c, (None, o, 0), in3(c, 0, o), in3(c, 1, o))
            if o == 2:
                for q in backwards:
                    pass_on(c, "f2", q, sign_of(q))
            elif o in (1, 3):
                s = -1 if o == 1 else 1
                for q in backwards:
                    if sign_of(q) != s:
                        pass_on(c, "m2", q, s)
    for q in backwards:
        for c in colours:
            s = sign_of(q)
            arrive(c, "f2", q, s)
            add(c, (q, -s, 0), in2(c, 2, q))
            pass_on(c, "m2", q, s)
    for q in backwards:
        for c in colours:
            arrive(c, "m2", q, 1)
            arrive(c, "m2", q, -1)
            add(c, (q, 0, 0), in2(c, 0, q), in2(c, 1, q))
            if q == 2:
                pass_on(c, "f1", 0, 1)
                pass_on(c, "f1", 0, -1)
    for s in (1, -1):
        for c in colours:
            start, width = SCATTER_COLS[c]
            half = width // 2
            arrive(c, "f1", 0, s)
            cols = pl.ds(start, half) if s == 1 else pl.ds(start + half, half)
            add(c, (-s, 0, 0), r1.at[c, 2 if s == 1 else 3, :, pl.ds(0, half)], cols=cols)
            pass_on(c, "m1", 0, s)
    for c in colours:
        start, width = SCATTER_COLS[c]
        cols = pl.ds(start, width)
        arrive(c, "m1", 0, 1)
        arrive(c, "m1", 0, -1)
        total = resid_ref[:, cols].astype(F32) + block(c, (0, 0, 0))[...].astype(F32)
        for k in range(2):
            total = total + r1[c, k, :, pl.ds(0, width)].astype(F32)
        out_ref[:, cols] = total.astype(BF16)

    for copy in started:
        copy.wait_send()
    for copy in swaps:
        copy.wait_send()


def layer(normed, resid, route_ids, dense_vector, w_group, w_expert, dense_gate, dense_up,
          dense_down, expert_gate, expert_up, expert_down):
    kinds = len(KINDS)
    vmem = pl.BlockSpec(memory_space=pltpu.VMEM)
    hbm = pl.BlockSpec(memory_space=pl.ANY)
    return pl.pallas_call(
        layer_kernel,
        out_shape=jax.ShapeDtypeStruct((16, 2048), BF16),
        in_specs=[vmem] * 6 + [hbm] * 6,
        out_specs=vmem,
        scratch_shapes=[
            pltpu.VMEM((16, 2304), BF16),
            pltpu.VMEM((4, 4, 4, 16, 2304), BF16),
            pltpu.VMEM((256, 2048), BF16),
            pltpu.VMEM((384, 2048), BF16),
            pltpu.VMEM((2, 2048, 512), BF16),
            pltpu.VMEM((2, 2048, 512), BF16),
            pltpu.VMEM((2, 512, 2048), BF16),
            pltpu.VMEM((4, 4, 4, 16, 384), BF16),
            pltpu.VMEM((256, 1024), BF16),
            pltpu.VMEM((256, 2048), BF16),
            pltpu.VMEM((128, 2048), BF16),
            pltpu.VMEM((4, 4, 4, 16, 2048), BF16),
            pltpu.VMEM((3, 4, 16, 768), BF16),
            pltpu.VMEM((3, 3, 4, 16, 768), BF16),
            pltpu.VMEM((3, 3, 4, 4, 16, 768), BF16),
            pltpu.SemaphoreType.DMA((7,)),
            pltpu.SemaphoreType.DMA((6,)),
            pltpu.SemaphoreType.DMA((6,)),
            pltpu.SemaphoreType.DMA((3, kinds)),
            pltpu.SemaphoreType.DMA((3, kinds)),
            pltpu.SemaphoreType.DMA((3, kinds)),
            pltpu.SemaphoreType.DMA((3, kinds)),
        ],
        compiler_params=pltpu.CompilerParams(
            collective_id=0, has_side_effects=True, vmem_limit_bytes=58 * 1024 * 1024
        ),
        cost_estimate=pl.CostEstimate(flops=8_000_000_000, bytes_accessed=20_000_000, transcendentals=0),
    )(
        normed,
        resid,
        route_ids,
        dense_vector.reshape(1, -1),
        jnp.transpose(w_group),
        w_expert,
        jnp.transpose(dense_gate),
        jnp.transpose(dense_up),
        dense_down,
        expert_gate[0],
        expert_up[0],
        expert_down[0],
    )


def rms_scale(values, gain):
    widened = values.astype(jnp.float32)
    scaled = widened * lax.rsqrt(jnp.mean(widened * widened, axis=-1, keepdims=True) + EPS)
    return (scaled * gain).astype(jnp.bfloat16)


def state_mixer(
    tokens,
    state,
    norm_mix,
    w_drive,
    lam_real,
    lam_imag,
    log_step,
    b_real,
    b_imag,
    readout_real,
    readout_imaginary,
    d_skip,
    w_value,
    w_glugate,
    w_output,
):
    row_count = tokens.shape[0]
    group_count, state_dimension = lam_real.shape
    channels = b_real.shape[2]
    normed_in = rms_scale(tokens, norm_mix)
    drive = jnp.dot(normed_in, w_drive, preferred_element_type=jnp.float32).astype(jnp.bfloat16)
    time_step = jnp.exp(log_step)[:, None]
    magnitude = jnp.exp(lam_real * time_step)
    decay_re = magnitude * jnp.cos(lam_imag * time_step)
    decay_im = magnitude * jnp.sin(lam_imag * time_step)
    modulus = lam_real * lam_real + lam_imag * lam_imag
    factor_re = ((decay_re - 1.0) * lam_real + decay_im * lam_imag) / modulus
    factor_im = (decay_im * lam_real - (decay_re - 1.0) * lam_imag) / modulus
    map_re = factor_re[:, :, None] * b_real - factor_im[:, :, None] * b_imag
    map_im = factor_re[:, :, None] * b_imag + factor_im[:, :, None] * b_real
    drive_wide = drive.astype(jnp.float32)
    grouped = drive_wide.reshape(row_count, group_count, channels)
    input_re = jnp.einsum("gpc,sgc->sgp", map_re, grouped)
    input_im = jnp.einsum("gpc,sgc->sgp", map_im, grouped)
    old_re = state[0].reshape(row_count, group_count, state_dimension)
    old_im = state[1].reshape(row_count, group_count, state_dimension)
    incoming_real = decay_re * old_re - decay_im * old_im + input_re
    incoming_imaginary = decay_re * old_im + decay_im * old_re + input_im
    projected_output = jnp.einsum("xej,fxj->fxe", readout_real, incoming_real) - jnp.einsum(
        "xej,fxj->fxe", readout_imaginary, incoming_imaginary
    )
    readout = jax.nn.gelu(
        projected_output.reshape(row_count, group_count * channels) + d_skip * drive_wide
    ).astype(jnp.bfloat16)
    value_part = jnp.dot(readout, w_value, preferred_element_type=jnp.float32)
    gate_part = jnp.dot(readout, w_glugate, preferred_element_type=jnp.float32)
    mixed = (value_part * jax.nn.sigmoid(gate_part)).astype(jnp.bfloat16)
    resid = (
        tokens.astype(jnp.float32) + jnp.dot(mixed, w_output, preferred_element_type=jnp.float32)
    ).astype(jnp.bfloat16)
    new_state = jnp.stack(
        [incoming_real.reshape(row_count, -1), incoming_imaginary.reshape(row_count, -1)]
    )
    return (resid, new_state)


def on_device(
    tokens,
    state,
    norm_mix,
    w_drive,
    lam_real,
    lam_imag,
    log_step,
    b_real,
    b_imag,
    readout_real,
    readout_imaginary,
    d_skip,
    w_value,
    w_glugate,
    w_output,
    norm_ffn,
    w_group,
    w_expert,
    route_ids,
    expert_gate,
    expert_up,
    expert_down,
    dense_vector,
    dense_gate,
    dense_up,
    dense_down,
):
    resid, new_state = state_mixer(
        tokens,
        state,
        norm_mix,
        w_drive,
        lam_real,
        lam_imag,
        log_step,
        b_real,
        b_imag,
        readout_real,
        readout_imaginary,
        d_skip,
        w_value,
        w_glugate,
        w_output,
    )
    normed = rms_scale(resid, norm_ffn)
    layer_out = layer(
        normed, resid, route_ids, dense_vector, w_group, w_expert, dense_gate, dense_up,
        dense_down, expert_gate, expert_up, expert_down,
    )
    return (layer_out, new_state)


def solution(mesh):
    placed = (
        P("ep", None),
        P(None, "ep", None),
        P(),
        P(),
        P(),
        P(),
        P(),
        P(),
        P(),
        P(),
        P(),
        P(),
        P(),
        P(),
        P(),
        P(),
        P(),
        P(),
        P("ep", None),
        P("ep", None, None),
        P("ep", None, None),
        P("ep", None, None),
        P(),
        P(None, "ep"),
        P(None, "ep"),
        P("ep", None),
    )
    return jax.shard_map(
        on_device,
        mesh=mesh,
        in_specs=placed,
        out_specs=(P("ep", None), P(None, "ep", None)),
        check_vma=False,
    )
```

time: 199 us -> 88.8 us (0.45)
  waiting for transfers between devices: 85.2 us -> 0 us
  Pallas kernels: 0 us -> 71.5 us
  starting transfers between devices: 33.4 us -> 0 us
  matrix products: 29.6 us -> 6.91 us
  other arithmetic: 25 us -> 3.94 us
  local copies, waits for them, and re-layouts: 22.4 us -> 5.11 us
    pallas_call x0 -> x1, Pallas kernels: none -> 71.5 us  [layer(): pl.pallas_call(layer_kernel, out_shape=jax.ShapeDtypeStruct((16, 2048), B...]
    ppermute x12 -> x0, waiting for transfers between devices: 68.5 us -> none  [from_partner(): lax.ppermute(array, axis, [(i, i ^ 1 << bit) for i in range(lax.axis_size...]
    dot_general x7 -> x0, matrix products: 23.8 us -> none  [the longest x1 7.53 us: on_device(): lax.dot_general(block_hidden, packed[2], (((1,), (1,)), ((), ())), prefer...]
    ppermute x12 -> x0, starting transfers between devices: 20.8 us -> none  [from_partner(): lax.ppermute(array, axis, [(i, i ^ 1 << bit) for i in range(lax.axis_size...]
    all_to_all x2 -> x0, waiting for transfers between devices: 16.7 us -> none  [the longest x1 16.7 us: on_device(): lax.all_to_all(result.reshape(senders, items, inner_width), 'ep', split_a...]
    all_to_all x2 -> x0, starting transfers between devices: 12.6 us -> none  [the longest x1 6.54 us: on_device(): lax.all_to_all(result.reshape(senders, items, inner_width), 'ep', split_a...]
    reshape x6 -> x0, local copies, waits for them, and re-layouts: 8.78 us -> none  [the longest x1 2.54 us: on_device(): result.reshape(senders, items, inner_width)]
    convert_element_type x7 -> x0, other arithmetic: 6.5 us -> none  [the longest x5 5.76 us: on_device(): outgoing_half.astype(jnp.bfloat16)]
  transfers between devices with their start and end apart: 14 -> 0, of which waited for: 10 -> 0; matrix products, arithmetic and copies ran while one was open for 30% -> 0% of each run, Pallas kernels for 0% -> 0%
where the time goes in v1:
time: 88.8 us; the launch traced here: 88.3 us
  Pallas kernels  71.5 us (81%)
  matrix products  6.91 us (8%)
  local copies, waits for them, and re-layouts  5.11 us (6%)
  other arithmetic  3.94 us (4%)
    pallas_call x1, Pallas kernels, layer(): pl.pallas_call(layer_kernel, out_shape=jax.ShapeDtypeStruct((16, 2048), B...  71.5 us
    unnamed x30, local copies, waits for them, and re-layouts  2.31 us
    dot_general x1, matrix products, state_mixer(): jnp.dot(normed_in, w_drive, preferred_element_type=jnp.float32)  2.07 us

profile of v1, /device:TPU:0, one launch (start us, length us, event | category | flops | bytes accessed | tf_op | source)
XLA Modules:
  0.0 88.3 jit_solution(12049660600313338692)
XLA Ops:
  0.6 0.0 copy-start
  0.6 0.0 copy-start.2
  0.7 0.0 copy-start.1
  0.7 0.8 exp.9
  1.5 1.5 %cosine_multiply_fusion = (f32[32,64]{1,0:T(8,128)S(1)}, f32[32,64]{1,0:T(8,128)}, f32[32,64]{1,0:T(8,128)}, f32[32,64]{1,0:T(8,128)}) fusion(f32[32,64]{1,0:T(8,128)} %param.31, f32[32,64]{1,0:T(8,128)} %param.30, f32[32]{0:T(128)S(1)} %exp.9), kind=kLoop, calls=%fused_computation.54 | loop fusion | flops 32768 | bytes 49280 | tf_op jit(solution)/shard_map/mul | solution.py:592
  3.0 1.0 %fusion.41 = (f32[1,16,2048]{2,1,0:T(8,128)S(1)}, f32[1,16,2048]{2,1,0:T(8,128)S(1)}) fusion(f32[2,16,2048]{2,1,0:T(8,128)} %param.27), kind=kLoop, calls=%fused_computation.59 | loop fusion | bytes 524288 | tf_op jit(solution)/shard_map/slice | solution.py:603
  4.0 0.1 reshape_squeeze.6
  4.1 0.1 reshape_squeeze.7
  4.2 1.0 %fusion.18 = f32[16]{0:T(128)S(1)} fusion(bf16[16,2048]{1,0:T(8,128)(2,1)} %param.26), kind=kLoop, calls=%fused_computation.29 | loop fusion | flops 98288 | bytes 65600 | tf_op jit(solution)/shard_map/reduce_sum | solution.py:564
  5.2 2.1 %convolution_convert_fusion = bf16[16,512]{1,0:T(8,128)(2,1)S(1)} fusion(bf16[2048,512]{1,0:T(8,128)(2,1)} %param.29, bf16[16,2048]{1,0:T(8,128)(2,1)} %param.26, f32[2048]{0:T(1024)} %param.28, f32[16]{0:T(128)S(1)} %add_rsqrt_fusion.1), kind=kOutput, calls=%fused_computation.13 | convolution fusion | flops 33693696 | bytes 2187328 | tf_op jit(solution)/shard_map/dot_general | solution.py:589
  7.2 0.0 copy-start.8
  7.2 0.6 copy-done.8
  7.8 0.1 reshape.37
  8.0 0.0 copy-done.2
  8.0 0.0 copy-done.1
  8.0 0.0 copy-start.5
  8.0 0.0 copy-start.7
  8.0 1.2 %fusion.2 = f32[16,32,64]{2,0,1:T(8,128)S(1)} fusion(f32[32,64,16]{1,2,0:T(8,128)S(1)} %copy-done.2, f32[32,64,16]{1,2,0:T(8,128)S(1)} %copy-done.1, f32[16,32,64]{2,1,0:T(8,128)S(1)} %reshape_squeeze.7, f32[16,32,64]{2,1,0:T(8,128)S(1)} %reshape_squeeze.6, f32[32,64]{1,0:T(8,128)} %get-tuple-element.6, f32[32,64]{1,0:T(8,128)} %get-tuple-element.7, ...), kind=kOutput, calls=%fused_computation.5 | convolution fusion | flops 1277952 | bytes 704512 | tf_op jit(solution)/shard_map/gpc,sgc->sgp/dot_general | solution.py:602
  9.2 1.4 %fusion.3 = f32[16,32,64]{2,0,1:T(8,128)S(1)} fusion(f32[32,64,16]{1,2,0:T(8,128)S(1)} %copy-done.1, f32[32,64,16]{1,2,0:T(8,128)} %param.33, f32[16,32,64]{2,1,0:T(8,128)S(1)} %reshape_squeeze.7, f32[16,32,64]{2,1,0:T(8,128)S(1)} %reshape_squeeze.6, f32[32,64]{1,0:T(8,128)} %get-tuple-element.6, f32[32,64]{1,0:T(8,128)} %get-tuple-element.7, ...), kind=kOutput, calls=%fused_computation.7 | convolution fusion | flops 1277952 | bytes 704512 | tf_op jit(solution)/shard_map/gpc,sgc->sgp/dot_general | solution.py:601
  10.6 0.0 copy-done.5
  10.6 0.0 copy-start.9
  10.7 0.0 copy-start.13
  10.7 0.0 copy-start.4
  10.7 0.0 copy-start.3
  10.7 0.2 fusion.42
  10.9 0.0 copy-done.7
  10.9 0.2 fusion.1
  11.1 0.0 copy-start.11
  11.1 0.0 copy-start.12
  11.1 0.1 copy.38
  11.2 0.2 reshape.38
  11.3 0.0 copy-done.9
  11.4 0.0 copy-done.13
  11.4 0.3 copy-done.4
  11.7 0.2 fusion.43
  11.9 0.0 copy-done
  11.9 0.0 copy-done.3
  11.9 1.7 %fusion.15 = (f32[16]{0:T(128)S(1)}, bf16[16,2048]{1,0:T(8,128)(2,1)S(1)}) fusion(bf16[512,2048]{1,0:T(8,128)(2,1)S(1)} %copy-done, f32[16,512]{1,0:T(8,128)S(1)} %fusion.43, bf16[16,512]{1,0:T(8,128)(2,1)S(1)} %fusion.37, bf16[512,512]{1,0:T(8,128)(2,1)} %param.39, bf16[16,2048]{1,0:T(8,128)(2,1)S(1)} %copy-done.3), kind=kOutput, calls=%fused_computation.26 | convolution fusion | flops 42180592 | bytes 2801728 | tf_op jit(solution)/shard_map/dot_general | solution.py:617
  13.6 0.0 copy-start.6
  13.6 0.0 copy-done.11
  13.6 0.7 fusion.17.normed_ref
  14.4 0.0 copy-done.12
  14.4 0.7 copy.39.ids_ref
  15.0 0.0 copy-done.6
  15.0 71.5 %shard_map.257 = bf16[16,2048]{1,0:T(8,128)(2,1)} custom-call(bf16[16,2048]{1,0:T(8,128)(2,1)} %fusion.17.normed_ref, bf16[16,2048]{1,0:T(8,128)(2,1)} %copy-done.6, s32[16,6]{1,0:T(8,128)} %copy.39.ids_ref, f32[1,2048]{1,0:T(1,128)} %bitcast.33, bf16[4,2048]{1,0:T(4,128)(2,1)} %bitcast.32, bf16[2048,128]{1,0:T(8,128)(2,1)} %router_ref.1, ...), custom_call_target="tpu_custom_call" | custom-call | flops 8000000000 | bytes 20000000 | tf_op jit(solution)/shard_map/pallas_call | solution.py:513
  86.6 0.0 copy-start.10
  86.6 0.1 copy.41
  86.7 0.1 stack_reshape.7
  86.8 0.1 copy.40
  86.9 0.1 stack_reshape.6
  87.0 0.7 pad_maximum_fusion
  87.7 0.0 copy-done.10
  87.7 0.6 copy.51
  (3 shorter events, 0.0 us)
Async XLA Ops:
  0.6 11.3 %copy-start = (bf16[512,2048]{1,0:T(8,128)(2,1)S(1)}, bf16[512,2048]{1,0:T(8,128)(2,1)}, u32[]{:S(2)}) copy-start(bf16[512,2048]{1,0:T(8,128)(2,1)} %param.40) | copy-start | bytes 6291460
  0.6 7.3 %copy-start.2 = (f32[32,64,16]{1,2,0:T(8,128)S(1)}, f32[32,64,16]{1,2,0:T(8,128)}, u32[]{:S(2)}) copy-start(f32[32,64,16]{1,2,0:T(8,128)} %param.33) | copy-start | bytes 393220
  0.7 7.3 %copy-start.1 = (f32[32,64,16]{1,2,0:T(8,128)S(1)}, f32[32,64,16]{1,2,0:T(8,128)}, u32[]{:S(2)}) copy-start(f32[32,64,16]{1,2,0:T(8,128)} %param.34) | copy-start | bytes 393220
  7.2 0.6 copy-start.8
  8.0 2.6 %copy-start.5 = (f32[32,16,64]{2,1,0:T(8,128)S(1)}, f32[32,16,64]{2,1,0:T(8,128)}, u32[]{:S(2)}) copy-start(f32[32,16,64]{2,1,0:T(8,128)} %param.35) | copy-start | bytes 393220
  8.0 2.8 %copy-start.7 = (f32[32,16,64]{2,1,0:T(8,128)S(1)}, f32[32,16,64]{2,1,0:T(8,128)}, u32[]{:S(2)}) copy-start(f32[32,16,64]{2,1,0:T(8,128)} %param.36) | copy-start | bytes 393220
  10.6 0.7 copy-start.9
  10.7 0.7 copy-start.13
  10.7 1.1 %copy-start.4 = (bf16[512,512]{1,0:T(8,128)(2,1)S(1)}, bf16[512,512]{1,0:T(8,128)(2,1)}, u32[]{:S(2)}) copy-start(bf16[512,512]{1,0:T(8,128)(2,1)} %param.38) | copy-start | bytes 1572868
  10.7 1.2 %copy-start.3 = (bf16[16,2048]{1,0:T(8,128)(2,1)S(1)}, bf16[16,2048]{1,0:T(8,128)(2,1)}, u32[]{:S(2)}) copy-start(bf16[16,2048]{1,0:T(8,128)(2,1)} %param.26) | copy-start | bytes 196612
  11.1 2.6 %copy-start.11 = (f32[2048]{0:T(1024)S(1)}, f32[2048]{0:T(1024)}, u32[]{:S(2)}) copy-start(f32[2048]{0:T(1024)} %param.41) | copy-start | bytes 24580
  11.1 3.3 %copy-start.12 = (s32[16,6]{0,1:T(8,128)S(1)}, s32[16,6]{0,1:T(8,128)}, u32[]{:S(2)}) copy-start(s32[16,6]{0,1:T(8,128)} %param.44) | copy-start | bytes 1156
  13.6 1.4 %copy-start.6 = (bf16[16,2048]{1,0:T(8,128)(2,1)}, bf16[16,2048]{1,0:T(8,128)(2,1)S(1)}, u32[]{:S(2)}) copy-start(bf16[16,2048]{1,0:T(8,128)(2,1)S(1)} %get-tuple-element.9.resid_ref) | copy-start | bytes 196612
  86.6 1.2 %copy-start.10 = (bf16[16,2048]{1,0:T(8,128)(2,1)S(1)}, bf16[16,2048]{1,0:T(8,128)(2,1)}, u32[]{:S(2)}) copy-start(bf16[16,2048]{1,0:T(8,128)(2,1)} %shard_map.257) | copy-start | bytes 196612

commit v2 on v1

--- a/solution.py
+++ b/solution.py
@@ -34,12 +34,26 @@
 
 
 def layer_kernel(
-    normed_ref,
-    resid_ref,
-    ids_ref,
-    vector_ref,
-    group_ref,
-    router_ref,
+    tokens_hbm,
+    state_hbm,
+    norm_mix_hbm,
+    w_drive_hbm,
+    lam_real_hbm,
+    lam_imag_hbm,
+    log_step_hbm,
+    b_real_hbm,
+    b_imag_hbm,
+    readout_real_hbm,
+    readout_imag_hbm,
+    d_skip_hbm,
+    w_value_hbm,
+    w_glugate_hbm,
+    w_output_hbm,
+    norm_ffn_hbm,
+    group_hbm,
+    router_hbm,
+    ids_hbm,
+    vector_hbm,
     gate_hbm,
     up_hbm,
     down_hbm,
@@ -47,6 +61,33 @@
     eu_hbm,
     ed_hbm,
     out_ref,
+    state_out,
+    tokens_ref,
+    state_ref,
+    norm_mix_ref,
+    w_drive_ref,
+    lam_real_ref,
+    lam_imag_ref,
+    log_step_ref,
+    b_real_ref,
+    b_imag_ref,
+    readout_real_ref,
+    readout_imag_ref,
+    d_skip_ref,
+    w_value_ref,
+    w_glugate_ref,
+    w_output_ref,
+    norm_ffn_ref,
+    group_ref,
+    router_ref,
+    ids_ref,
+    vector_ref,
+    input_re,
+    input_im,
+    readout_re,
+    readout_im,
+    decay_rows,
+    resid_ref,
     own,
     x,
     w_in,
@@ -62,6 +103,7 @@
     r1,
     r2,
     r3,
+    load_sem,
     local_sem,
     swap_send,
     swap_recv,
@@ -89,6 +131,28 @@
     barrier = pltpu.get_barrier_semaphore()
     for peer in [*peers.values(), partner]:
         pl.semaphore_signal(barrier, inc=1, device_id=(peer,), device_id_type=MESH)
+
+    sources = (
+        lam_real_hbm, lam_imag_hbm, log_step_hbm, b_real_hbm, b_imag_hbm, readout_real_hbm,
+        readout_imag_hbm, tokens_hbm, norm_mix_hbm, w_drive_hbm, state_hbm, d_skip_hbm,
+        w_value_hbm, w_glugate_hbm, w_output_hbm, norm_ffn_hbm, ids_hbm, vector_hbm, group_hbm,
+        router_hbm,
+    )
+    targets = (
+        lam_real_ref, lam_imag_ref, log_step_ref, b_real_ref, b_imag_ref, readout_real_ref,
+        readout_imag_ref, tokens_ref, norm_mix_ref, w_drive_ref, state_ref, d_skip_ref,
+        w_value_ref, w_glugate_ref, w_output_ref, norm_ffn_ref, ids_ref, vector_ref, group_ref,
+        router_ref,
+    )
+    loads = [
+        pltpu.make_async_copy(a, b, load_sem.at[i]) for i, (a, b) in enumerate(zip(sources, targets))
+    ]
+    for copy in loads:
+        copy.start()
+
+    def loaded(first, last):
+        for copy in loads[first:last]:
+            copy.wait()
 
     def rows(i):
         return pl.ds(pl.multiple_of(i * 64, 64), 64)
@@ -116,18 +180,82 @@
         for i, (s, t) in enumerate(weights)
     ]
 
-    normed = normed_ref[...]
+    for ref in (input_re, input_im, readout_re, readout_im):
+        ref[...] = jnp.zeros((4, 128, 512), BF16)
+    loaded(0, 7)
+    square = lax.broadcasted_iota(jnp.int32, (32, 32), 0) == lax.broadcasted_iota(
+        jnp.int32, (32, 32), 1
+    )
+    time_step = jnp.sum(
+        jnp.where(square, jnp.exp(log_step_ref[...]), 0.0), axis=1, keepdims=True
+    )
+    lam_re = lam_real_ref[...]
+    lam_im = lam_imag_ref[...]
+    magnitude = jnp.exp(lam_re * time_step)
+    decay_re = magnitude * jnp.cos(lam_im * time_step)
+    decay_im = magnitude * jnp.sin(lam_im * time_step)
+    modulus = lam_re * lam_re + lam_im * lam_im
+    factor_re = ((decay_re - 1.0) * lam_re + decay_im * lam_im) / modulus
+    factor_im = (decay_im * lam_re - (decay_re - 1.0) * lam_im) / modulus
+    for g in range(32):
+        q, j = divmod(g, 8)
+        at = (q, pl.ds(16 * j, 16), pl.ds(64 * j, 64))
+        f_re = factor_re[g : g + 1]
+        f_im = factor_im[g : g + 1]
+        b_re = b_real_ref[g]
+        b_im = b_imag_ref[g]
+        input_re[at] = (f_re * b_re - f_im * b_im).astype(BF16)
+        input_im[at] = (f_re * b_im + f_im * b_re).astype(BF16)
+        readout_re[at] = readout_real_ref[g].astype(BF16)
+        readout_im[at] = readout_imag_ref[g].astype(BF16)
+        lane = pl.ds(64 * g, 64)
+        decay_rows[pl.ds(0, 1), lane] = decay_re[g : g + 1]
+        decay_rows[pl.ds(1, 1), lane] = decay_im[g : g + 1]
+
+    def rms_scale(values, gain):
+        mean = jnp.mean(values * values, axis=1, keepdims=True)
+        return (values * lax.rsqrt(mean + EPS) * gain).astype(BF16)
+
+    loaded(7, 10)
+    tokens = tokens_ref[...].astype(F32)
+    drive = dot(rms_scale(tokens, norm_mix_ref[...]), w_drive_ref[...]).astype(BF16)
+    loaded(10, 12)
+    projected = []
+    for q in range(4):
+        channels = drive[:, 128 * q : 128 * q + 128]
+        cols = pl.ds(512 * q, 512)
+        old_re = state_ref[0, :, cols]
+        old_im = state_ref[1, :, cols]
+        d_re = decay_rows[pl.ds(0, 1), cols]
+        d_im = decay_rows[pl.ds(1, 1), cols]
+        new_re = d_re * old_re - d_im * old_im + dot(channels, input_re[q])
+        new_im = d_re * old_im + d_im * old_re + dot(channels, input_im[q])
+        state_out[0, :, cols] = new_re
+        state_out[1, :, cols] = new_im
+        projected.append(
+            dot_nt(new_re.astype(BF16), readout_re[q]) - dot_nt(new_im.astype(BF16), readout_im[q])
+        )
+    skipped = d_skip_ref[...] * drive.astype(F32)
+    readout = jax.nn.gelu(jnp.concatenate(projected, axis=1) + skipped).astype(BF16)
+    loaded(12, 15)
+    value_part = dot(readout, w_value_ref[...])
+    gate_part = dot(readout, w_glugate_ref[...])
+    mixed = (value_part * jax.nn.sigmoid(gate_part)).astype(BF16)
+    resid = (tokens + dot(mixed, w_output_ref[...])).astype(BF16)
+    resid_ref[...] = resid
+    loaded(15, 20)
+    normed = rms_scale(resid.astype(F32), norm_ffn_ref[...])
+
     own[:, pl.ds(0, 2048)] = normed
-    ids = ids_ref[...]
+    ids = ids_ref[...].astype(F32)
     lanes = lax.broadcasted_iota(jnp.int32, (16, 128), 1)
+    this = lax.broadcasted_iota(jnp.int32, (16, 16), 0)
+    that = lax.broadcasted_iota(jnp.int32, (16, 16), 1)
     chosen = jnp.zeros((16, 128), F32)
     for t in range(6):
-        chosen = chosen + jnp.where(ids[:, t : t + 1] == lanes, 1.0, 0.0)
-    earlier = jnp.where(
-        lax.broadcasted_iota(jnp.int32, (16, 16), 1) < lax.broadcasted_iota(jnp.int32, (16, 16), 0),
-        1.0,
-        0.0,
-    )
+        column = jnp.sum(jnp.where(this == that, ids[t : t + 1], 0.0), axis=1, keepdims=True)
+        chosen = chosen + jnp.where(column == lanes.astype(F32), 1.0, 0.0)
+    earlier = jnp.where(that < this, 1.0, 0.0)
     ordinal = dot(earlier.astype(BF16), chosen.astype(BF16))
     own[:, pl.ds(2048, 128)] = (chosen * (1.0 + ordinal)).astype(BF16)
     branch = jax.nn.sigmoid(
@@ -505,123 +633,6 @@
         copy.wait_send()
 
 
-def layer(normed, resid, route_ids, dense_vector, w_group, w_expert, dense_gate, dense_up,
-          dense_down, expert_gate, expert_up, expert_down):
-    kinds = len(KINDS)
-    vmem = pl.BlockSpec(memory_space=pltpu.VMEM)
-    hbm = pl.BlockSpec(memory_space=pl.ANY)
-    return pl.pallas_call(
-        layer_kernel,
-        out_shape=jax.ShapeDtypeStruct((16, 2048), BF16),
-        in_specs=[vmem] * 6 + [hbm] * 6,
-        out_specs=vmem,
-        scratch_shapes=[
-            pltpu.VMEM((16, 2304), BF16),
-            pltpu.VMEM((4, 4, 4, 16, 2304), BF16),
-            pltpu.VMEM((256, 2048), BF16),
-            pltpu.VMEM((384, 2048), BF16),
-            pltpu.VMEM((2, 2048, 512), BF16),
-            pltpu.VMEM((2, 2048, 512), BF16),
-            pltpu.VMEM((2, 512, 2048), BF16),
-            pltpu.VMEM((4, 4, 4, 16, 384), BF16),
-            pltpu.VMEM((256, 1024), BF16),
-            pltpu.VMEM((256, 2048), BF16),
-            pltpu.VMEM((128, 2048), BF16),
-            pltpu.VMEM((4, 4, 4, 16, 2048), BF16),
-            pltpu.VMEM((3, 4, 16, 768), BF16),
-            pltpu.VMEM((3, 3, 4, 16, 768), BF16),
-            pltpu.VMEM((3, 3, 4, 4, 16, 768), BF16),
-            pltpu.SemaphoreType.DMA((7,)),
-            pltpu.SemaphoreType.DMA((6,)),
-            pltpu.SemaphoreType.DMA((6,)),
-            pltpu.SemaphoreType.DMA((3, kinds)),
-            pltpu.SemaphoreType.DMA((3, kinds)),
-            pltpu.SemaphoreType.DMA((3, kinds)),
-            pltpu.SemaphoreType.DMA((3, kinds)),
-        ],
-        compiler_params=pltpu.CompilerParams(
-            collective_id=0, has_side_effects=True, vmem_limit_bytes=58 * 1024 * 1024
-        ),
-        cost_estimate=pl.CostEstimate(flops=8_000_000_000, bytes_accessed=20_000_000, transcendentals=0),
-    )(
-        normed,
-        resid,
-        route_ids,
-        dense_vector.reshape(1, -1),
-        jnp.transpose(w_group),
-        w_expert,
-        jnp.transpose(dense_gate),
-        jnp.transpose(dense_up),
-        dense_down,
-        expert_gate[0],
-        expert_up[0],
-        expert_down[0],
-    )
-
-
-def rms_scale(values, gain):
-    widened = values.astype(jnp.float32)
-    scaled = widened * lax.rsqrt(jnp.mean(widened * widened, axis=-1, keepdims=True) + EPS)
-    return (scaled * gain).astype(jnp.bfloat16)
-
-
-def state_mixer(
-    tokens,
-    state,
-    norm_mix,
-    w_drive,
-    lam_real,
-    lam_imag,
-    log_step,
-    b_real,
-    b_imag,
-    readout_real,
-    readout_imaginary,
-    d_skip,
-    w_value,
-    w_glugate,
-    w_output,
-):
-    row_count = tokens.shape[0]
-    group_count, state_dimension = lam_real.shape
-    channels = b_real.shape[2]
-    normed_in = rms_scale(tokens, norm_mix)
-    drive = jnp.dot(normed_in, w_drive, preferred_element_type=jnp.float32).astype(jnp.bfloat16)
-    time_step = jnp.exp(log_step)[:, None]
-    magnitude = jnp.exp(lam_real * time_step)
-    decay_re = magnitude * jnp.cos(lam_imag * time_step)
-    decay_im = magnitude * jnp.sin(lam_imag * time_step)
-    modulus = lam_real * lam_real + lam_imag * lam_imag
-    factor_re = ((decay_re - 1.0) * lam_real + decay_im * lam_imag) / modulus
-    factor_im = (decay_im * lam_real - (decay_re - 1.0) * lam_imag) / modulus
-    map_re = factor_re[:, :, None] * b_real - factor_im[:, :, None] * b_imag
-    map_im = factor_re[:, :, None] * b_imag + factor_im[:, :, None] * b_real
-    drive_wide = drive.astype(jnp.float32)
-    grouped = drive_wide.reshape(row_count, group_count, channels)
-    input_re = jnp.einsum("gpc,sgc->sgp", map_re, grouped)
-    input_im = jnp.einsum("gpc,sgc->sgp", map_im, grouped)
-    old_re = state[0].reshape(row_count, group_count, state_dimension)
-    old_im = state[1].reshape(row_count, group_count, state_dimension)
-    incoming_real = decay_re * old_re - decay_im * old_im + input_re
-    incoming_imaginary = decay_re * old_im + decay_im * old_re + input_im
-    projected_output = jnp.einsum("xej,fxj->fxe", readout_real, incoming_real) - jnp.einsum(
-        "xej,fxj->fxe", readout_imaginary, incoming_imaginary
-    )
-    readout = jax.nn.gelu(
-        projected_output.reshape(row_count, group_count * channels) + d_skip * drive_wide
-    ).astype(jnp.bfloat16)
-    value_part = jnp.dot(readout, w_value, preferred_element_type=jnp.float32)
-    gate_part = jnp.dot(readout, w_glugate, preferred_element_type=jnp.float32)
-    mixed = (value_part * jax.nn.sigmoid(gate_part)).astype(jnp.bfloat16)
-    resid = (
-        tokens.astype(jnp.float32) + jnp.dot(mixed, w_output, preferred_element_type=jnp.float32)
-    ).astype(jnp.bfloat16)
-    new_state = jnp.stack(
-        [incoming_real.reshape(row_count, -1), incoming_imaginary.reshape(row_count, -1)]
-    )
-    return (resid, new_state)
-
-
 def on_device(
     tokens,
     state,
@@ -650,29 +661,102 @@
     dense_up,
     dense_down,
 ):
-    resid, new_state = state_mixer(
+    kinds = len(KINDS)
+    vmem = pl.BlockSpec(memory_space=pltpu.VMEM)
+    hbm = pl.BlockSpec(memory_space=pl.ANY)
+    return pl.pallas_call(
+        layer_kernel,
+        out_shape=(
+            jax.ShapeDtypeStruct((16, 2048), BF16),
+            jax.ShapeDtypeStruct((2, 16, 2048), F32),
+        ),
+        in_specs=[hbm] * 26,
+        out_specs=(vmem, vmem),
+        scratch_shapes=[
+            pltpu.VMEM((16, 2048), BF16),
+            pltpu.VMEM((2, 16, 2048), F32),
+            pltpu.VMEM((1, 2048), F32),
+            pltpu.VMEM((2048, 512), BF16),
+            pltpu.VMEM((32, 64), F32),
+            pltpu.VMEM((32, 64), F32),
+            pltpu.VMEM((1, 32), F32),
+            pltpu.VMEM((32, 16, 64), F32),
+            pltpu.VMEM((32, 16, 64), F32),
+            pltpu.VMEM((32, 16, 64), F32),
+            pltpu.VMEM((32, 16, 64), F32),
+            pltpu.VMEM((1, 512), F32),
+            pltpu.VMEM((512, 512), BF16),
+            pltpu.VMEM((512, 512), BF16),
+            pltpu.VMEM((512, 2048), BF16),
+            pltpu.VMEM((1, 2048), F32),
+            pltpu.VMEM((4, 2048), BF16),
+            pltpu.VMEM((2048, 128), BF16),
+            pltpu.VMEM((6, 16), jnp.int32),
+            pltpu.VMEM((1, 2048), F32),
+            pltpu.VMEM((4, 128, 512), BF16),
+            pltpu.VMEM((4, 128, 512), BF16),
+            pltpu.VMEM((4, 128, 512), BF16),
+            pltpu.VMEM((4, 128, 512), BF16),
+            pltpu.VMEM((2, 2048), F32),
+            pltpu.VMEM((16, 2048), BF16),
+            pltpu.VMEM((16, 2304), BF16),
+            pltpu.VMEM((4, 4, 4, 16, 2304), BF16),
+            pltpu.VMEM((256, 2048), BF16),
+            pltpu.VMEM((384, 2048), BF16),
+            pltpu.VMEM((2, 2048, 512), BF16),
+            pltpu.VMEM((2, 2048, 512), BF16),
+            pltpu.VMEM((2, 512, 2048), BF16),
+            pltpu.VMEM((4, 4, 4, 16, 384), BF16),
+            pltpu.VMEM((256, 1024), BF16),
+            pltpu.VMEM((256, 2048), BF16),
+            pltpu.VMEM((128, 2048), BF16),
+            pltpu.VMEM((4, 4, 4, 16, 2048), BF16),
+            pltpu.VMEM((3, 4, 16, 768), BF16),
+            pltpu.VMEM((3, 3, 4, 16, 768), BF16),
+            pltpu.VMEM((3, 3, 4, 4, 16, 768), BF16),
+            pltpu.SemaphoreType.DMA((20,)),
+            pltpu.SemaphoreType.DMA((7,)),
+            pltpu.SemaphoreType.DMA((6,)),
+            pltpu.SemaphoreType.DMA((6,)),
+            pltpu.SemaphoreType.DMA((3, kinds)),
+            pltpu.SemaphoreType.DMA((3, kinds)),
+            pltpu.SemaphoreType.DMA((3, kinds)),
+            pltpu.SemaphoreType.DMA((3, kinds)),
+        ],
+        compiler_params=pltpu.CompilerParams(
+            collective_id=0, has_side_effects=True, vmem_limit_bytes=58 * 1024 * 1024
+        ),
+        cost_estimate=pl.CostEstimate(
+            flops=8_000_000_000, bytes_accessed=20_000_000, transcendentals=0
+        ),
+    )(
         tokens,
         state,
-        norm_mix,
+        norm_mix.reshape(1, -1),
         w_drive,
         lam_real,
         lam_imag,
-        log_step,
-        b_real,
-        b_imag,
+        log_step.reshape(1, -1),
+        jnp.transpose(b_real, (0, 2, 1)),
+        jnp.transpose(b_imag, (0, 2, 1)),
         readout_real,
         readout_imaginary,
-        d_skip,
+        d_skip.reshape(1, -1),
         w_value,
         w_glugate,
         w_output,
-    )
-    normed = rms_scale(resid, norm_ffn)
-    layer_out = layer(
-        normed, resid, route_ids, dense_vector, w_group, w_expert, dense_gate, dense_up,
-        dense_down, expert_gate, expert_up, expert_down,
-    )
-    return (layer_out, new_state)
+        norm_ffn.reshape(1, -1),
+        jnp.transpose(w_group),
+        w_expert,
+        jnp.transpose(route_ids),
+        dense_vector.reshape(1, -1),
+        jnp.transpose(dense_gate),
+        jnp.transpose(dense_up),
+        dense_down,
+        expert_gate[0],
+        expert_up[0],
+        expert_down[0],
+    )
 
 
 def solution(mesh):

time: 88.8 us -> 78.8 us (0.89)
  matrix products: 6.91 us -> 0 us
  other arithmetic: 3.94 us -> 0 us
  Pallas kernels: 71.5 us -> 74.6 us
  local copies, waits for them, and re-layouts: 5.11 us -> 3.14 us
    dot_general x7 -> x0, matrix products: 6.91 us -> none  [the longest x1 2.07 us: state_mixer(): jnp.dot(normed_in, w_drive, preferred_element_type=jnp.float32)]
    pallas_call x1, Pallas kernels: 71.5 us -> 74.6 us  [on_device(): pl.pallas_call(layer_kernel, out_shape=(jax.ShapeDtypeStruct((16, 2048),...]
    mul x1 -> x0, other arithmetic: 1.5 us -> none  [state_mixer(): decay_re = magnitude * jnp.cos(lam_imag * time_step)]
    slice x1 -> x0, local copies, waits for them, and re-layouts: 0.99 us -> none  [state_mixer(): old_re = state[0].reshape(row_count, group_count, state_dimension)]
    reduce_sum x1 -> x0, other arithmetic: 0.97 us -> none  [rms_scale(): jnp.mean(widened * widened, axis=-1, keepdims=True) + EPS]
    unnamed x30 -> x2, local copies, waits for them, and re-layouts: 2.31 us -> 3.14 us
where the time goes in v2:
time: 78.8 us; the launch traced here: 78.4 us
  Pallas kernels  74.6 us (95%)
  local copies, waits for them, and re-layouts  3.14 us (4%)
    pallas_call x1, Pallas kernels, on_device(): pl.pallas_call(layer_kernel, out_shape=(jax.ShapeDtypeStruct((16, 2048),...  74.6 us
    unnamed x2, local copies, waits for them, and re-layouts  3.14 us

profile of v2, /device:TPU:0, one launch (start us, length us, event | category | flops | bytes accessed | tf_op | source)
XLA Modules:
  0.0 78.4 jit_solution(8284170569532769359)
XLA Ops:
  0.6 74.6 %shard_map.257 = (bf16[16,2048]{1,0:T(8,128)(2,1)}, f32[2,16,2048]{2,1,0:T(8,128)}) custom-call(bf16[16,2048]{1,0:T(8,128)(2,1)} %tokens_hbm.1, f32[2,16,2048]{2,1,0:T(8,128)} %state_hbm.1, f32[1,2048]{1,0:T(1,128)} %bitcast.22, bf16[2048,512]{1,0:T(8,128)(2,1)} %w_drive_hbm.1, f32[32,64]{1,0:T(8,128)} %lam_real_hbm.1, f32[32,64]{1,0:T(8,128)} %lam_imag_hbm.1, ...), custom_call_target="tpu_custom_call" | custom-call | flops 8000000000 | bytes 20000000 | tf_op jit(solution)/shard_map/pallas_call | solution.py:667
  75.3 1.5 %copy.30 = bf16[16,2048]{1,0:T(8,128)(2,1)} copy(bf16[16,2048]{1,0:T(8,128)(2,1)} %get-tuple-element.4) | data formatting | bytes 131072
  76.8 1.7 %copy.31 = f32[2,16,2048]{2,1,0:T(8,128)} copy(f32[2,16,2048]{2,1,0:T(8,128)} %get-tuple-element.5) | data formatting | bytes 524288

commit v3 on v2

v3 whole, which is shorter than its diff:
```python
import heapq

import jax
import jax.numpy as jnp
from jax import lax
from jax.experimental import pallas as pl
from jax.experimental.pallas import tpu as pltpu
from jax.sharding import PartitionSpec as P

EPS = 1e-05
F32 = jnp.float32
BF16 = jnp.bfloat16
MESH = pl.DeviceIdType.MESH
ORDERS = (("x", "y", "z"), ("y", "z", "x"), ("z", "x", "y"))
COLS = ((0, 640), (640, 640), (1280, 768))
HALVES = (384, 384, 384)
RATE, DELAY, AHEAD, STEP = 46700.0, 2.0, 1.0, 0.36


def sign_of(offset):
    return 1 if offset in (0, 1) else -1


def messages():
    one = [("m1", s) for s in (1, -1)] + [("f1", s) for s in (1, -1)]
    two = [("m2", o, s) for o in range(4) for s in (1, -1)] + [("f2", o) for o in range(4)]
    pairs = [(o, q) for o in range(4) for q in range(4)]
    three = [("m3", o, q, s) for o, q in pairs for s in (1, -1)] + [("f3", o, q) for o, q in pairs]
    return one + two + three


SLOT = {m: i for i, m in enumerate(messages())}


def link_of(c, m):
    phase = int(m[0][1]) - 1
    s = m[-1] if m[0] in ("m1", "m2", "m3", "f1") else sign_of(m[-1])
    return ORDERS[c][phase], s


def bytes_of(c, m):
    width = COLS[c][1]
    if m[0] == "f1":
        width = HALVES[c] if m[1] == 1 else width - HALVES[c]
    return 32.0 * width


def simulate(first, react, rank):
    queue, waiting, free, count = [], {}, {}, 0
    sent, came, ready = {}, {}, {}

    def push(t, kind, item):
        nonlocal count
        count += 1
        heapq.heappush(queue, (t, count, kind, item))

    for t, items in first:
        for item in items:
            push(t, "ready", item)
    while queue:
        t, _, kind, item = heapq.heappop(queue)
        if kind == "ready":
            ready[item] = t
            count += 1
            heapq.heappush(waiting.setdefault(link_of(*item), []), (rank(item), count, item))
            links = [link_of(*item)]
        elif kind == "free":
            links = [item]
        else:
            came[item] = t
            links = []
            for new in react(item):
                push(t, "ready", new)
        for k in links:
            if free.get(k, 0.0) <= t + 1e-9 and waiting.get(k):
                _, _, m = heapq.heappop(waiting[k])
                free[k] = t + bytes_of(*m) / RATE
                sent[m] = t
                push(free[k], "free", k)
                push(free[k] + DELAY, "came", m)
    steps = [(t, 0, "receive", m) for m, t in came.items()]
    steps += [(max(ready[m], t - AHEAD), 1, "send", m) for m, t in sent.items()]
    return steps, sent


def plan_gather():
    halves = {}

    def present(c, o, q):
        new = [(c, ("m2", o, 1)), (c, ("m2", o, -1))] if q == 0 else []
        return new + [(c, ("m3", o, q, 1)), (c, ("m3", o, q, -1))]

    def react(item):
        c, m = item
        if m[0] == "m1":
            return [(c, ("f1", m[1]))] + present(c, 3 if m[1] == 1 else 1, 0)
        if m[0] == "f1":
            halves[c] = halves.get(c, 0) + 1
            return present(c, 2, 0) if halves[c] == 2 else []
        if m[0] == "m2":
            o, s = m[1:]
            new = [(c, ("f2", o))] if sign_of(o) == s else []
            return new + present(c, o, 3 if s == 1 else 1)
        if m[0] == "f2":
            return present(c, m[1], 2)
        if m[0] == "m3" and sign_of(m[2]) == m[3]:
            return [(c, ("f3", m[1], m[2]))]
        return []

    start = [(c, ("m1", s)) for c in range(3) for s in (1, -1)]
    for c in range(3):
        start += present(c, 0, 0)
    rank = {"m1": 0, "f1": 0, "m2": 1, "f2": 1, "m3": 2, "f3": 3}
    steps, sent = simulate([(0.0, start)], react, lambda item: rank[item[1][0]])
    return [(kind, *m) for _, _, kind, m in sorted(steps, key=lambda s: s[:2])], sent, steps


def plan_scatter(sent):
    seen = {}

    def react(item):
        c, m = item

        def both(key):
            seen[c, key] = seen.get((c, key), 0) + 1
            return seen[c, key] == 2

        def level2(o, q):
            if q == 2:
                return [(c, ("f2", o))]
            if q == 0:
                return level1(o)
            s = -1 if q == 1 else 1
            return [(c, ("m2", o, s))] if sign_of(o) != s or both(("m2", o, s)) else []

        def level1(o):
            seen[c, "sum", o] = seen.get((c, "sum", o), 0) + 1
            if seen[c, "sum", o] < 3:
                return []
            if o == 2:
                return [(c, ("f1", 1)), (c, ("f1", -1))]
            if o == 0:
                return []
            s = -1 if o == 1 else 1
            return [(c, ("m1", s))] if both(("m1", s)) else []

        if m[0] == "f3":
            s = sign_of(m[2])
            return [(c, ("m3", m[1], m[2], s))] if both(("m3",) + m[1:] + (s,)) else []
        if m[0] == "m3":
            return level2(m[1], m[2]) if both(("sum3",) + m[1:3]) else []
        if m[0] == "f2":
            s = sign_of(m[1])
            return [(c, ("m2", m[1], s))] if both(("m2", m[1], s)) else []
        if m[0] == "m2":
            return level1(m[1])
        if m[0] == "f1":
            return [(c, ("m1", m[1]))] if both(("m1", m[1])) else []
        return []

    first, products, t = [], [], 0.0
    pairs = [(o, q) for o in range(4) for q in range(4)]
    for k in (2, 3, 1, 0):
        for c in range(3):
            products.append((t, 0, "product", (c, k)))
            t += STEP
            if k == 2:
                first.append((t, [(c, ("f3", o, q)) for o, q in pairs]))
            elif k in (1, 3):
                s = -1 if k == 1 else 1
                free = [(c, ("m3", o, q, s)) for o, q in pairs if sign_of(q) != s]
                first.append((t, free))
                for o, q in pairs:
                    if sign_of(q) == s:
                        seen[c, ("m3", o, q, s)] = 1
    last = max(sent.values())
    steps, out = simulate(first, react, lambda item: last - sent[item])
    steps = steps + products
    return [(kind, *m) for _, _, kind, m in sorted(steps, key=lambda s: s[:2])], out, steps


def dot(a, b):
    return jnp.dot(a, b, preferred_element_type=F32)


def dot_nt(a, b):
    return lax.dot_general(a, b, (((1,), (1,)), ((), ())), preferred_element_type=F32)


def layer_kernel(
    tokens_hbm,
    state_hbm,
    norm_mix_hbm,
    w_drive_hbm,
    lam_real_hbm,
    lam_imag_hbm,
    log_step_hbm,
    b_real_hbm,
    b_imag_hbm,
    readout_real_hbm,
    readout_imag_hbm,
    d_skip_hbm,
    w_value_hbm,
    w_glugate_hbm,
    w_output_hbm,
    norm_ffn_hbm,
    group_hbm,
    router_hbm,
    ids_hbm,
    vector_hbm,
    gate_hbm,
    up_hbm,
    down_hbm,
    eg_hbm,
    eu_hbm,
    ed_hbm,
    out_ref,
    state_out,
    tokens_ref,
    state_ref,
    norm_mix_ref,
    w_drive_ref,
    lam_real_ref,
    lam_imag_ref,
    log_step_ref,
    b_real_ref,
    b_imag_ref,
    readout_real_ref,
    readout_imag_ref,
    d_skip_ref,
    w_value_ref,
    w_glugate_ref,
    w_output_ref,
    norm_ffn_ref,
    group_ref,
    router_ref,
    ids_ref,
    vector_ref,
    input_re,
    input_im,
    readout_re,
    readout_im,
    decay_rows,
    resid_ref,
    own,
    x,
    w_in,
    w_out,
    eg,
    eu,
    ed,
    ids_all,
    ids_own,
    sums,
    hc,
    picking,
    group_rows,
    p,
    r1,
    r2,
    r3,
    load_sem,
    local_sem,
    swap_send,
    swap_recv,
    id_send,
    id_recv,
    ag_send,
    ag_recv,
    rs_send,
    rs_recv,
):
    me = lax.axis_index("ep")
    core = lax.rem(me, 2)
    pos = {"x": lax.rem(me // 2, 4), "y": lax.rem(me // 8, 4), "z": me // 32}
    near = {d: [lax.rem(pos[d] + k, 4) for k in range(4)] for d in "xyz"}

    def device(at):
        return ((at["z"] * 4 + at["y"]) * 4 + at["x"]) * 2 + core

    def neighbour(d, s):
        at = dict(pos)
        at[d] = near[d][s % 4]
        return device(at)

    peers = {(d, s): neighbour(d, s) for d in "xyz" for s in (1, -1, 2)}
    partner = me + 1 - 2 * core

    barrier = pltpu.get_barrier_semaphore()
    for peer in [*peers.values(), partner]:
        pl.semaphore_signal(barrier, inc=1, device_id=(peer,), device_id_type=MESH)

    sources = (
        lam_real_hbm, lam_imag_hbm, log_step_hbm, b_real_hbm, b_imag_hbm, readout_real_hbm,
        readout_imag_hbm, tokens_hbm, norm_mix_hbm, w_drive_hbm, state_hbm, d_skip_hbm,
        w_value_hbm, w_glugate_hbm, w_output_hbm, norm_ffn_hbm, ids_hbm, vector_hbm, group_hbm,
        router_hbm,
    )
    targets = (
        lam_real_ref, lam_imag_ref, log_step_ref, b_real_ref, b_imag_ref, readout_real_ref,
        readout_imag_ref, tokens_ref, norm_mix_ref, w_drive_ref, state_ref, d_skip_ref,
        w_value_ref, w_glugate_ref, w_output_ref, norm_ffn_ref, ids_ref, vector_ref, group_ref,
        router_ref,
    )
    loads = [
        pltpu.make_async_copy(a, b, load_sem.at[i]) for i, (a, b) in enumerate(zip(sources, targets))
    ]
    for copy in loads:
        copy.start()

    def loaded(first, last):
        for copy in loads[first:last]:
            copy.wait()

    def rows(i):
        return pl.ds(pl.multiple_of(i * 64, 64), 64)

    weights = [
        (gate_hbm, w_in.at[rows(core)]),
        (up_hbm, w_in.at[rows(2 + core)]),
        (down_hbm, w_out.at[rows(core)]),
        (eg_hbm, eg.at[core]),
        (eu_hbm, eu.at[core]),
        (ed_hbm, ed.at[core]),
    ]
    local = [pltpu.make_async_copy(s, t, local_sem.at[i]) for i, (s, t) in enumerate(weights)]
    for copy in local:
        copy.start()
    pieces = list(weights[:3])
    for s, t in weights[3:]:
        depth = s.shape[0] // 4
        pieces += [(s.at[pl.ds(i * depth, depth)], t.at[pl.ds(i * depth, depth)]) for i in range(4)]
    swaps = [
        pltpu.make_async_remote_copy(
            src_ref=s,
            dst_ref=t,
            send_sem=swap_send.at[i],
            recv_sem=swap_recv.at[i],
            device_id=(partner,),
            device_id_type=MESH,
        )
        for i, (s, t) in enumerate(pieces)
    ]

    for ref in (input_re, input_im, readout_re, readout_im):
        ref[...] = jnp.zeros((4, 128, 512), BF16)
    loaded(0, 7)
    square = lax.broadcasted_iota(jnp.int32, (32, 32), 0) == lax.broadcasted_iota(
        jnp.int32, (32, 32), 1
    )
    time_step = jnp.sum(
        jnp.where(square, jnp.exp(log_step_ref[...]), 0.0), axis=1, keepdims=True
    )
    lam_re = lam_real_ref[...]
    lam_im = lam_imag_ref[...]
    magnitude = jnp.exp(lam_re * time_step)
    decay_re = magnitude * jnp.cos(lam_im * time_step)
    decay_im = magnitude * jnp.sin(lam_im * time_step)
    modulus = lam_re * lam_re + lam_im * lam_im
    factor_re = ((decay_re - 1.0) * lam_re + decay_im * lam_im) / modulus
    factor_im = (decay_im * lam_re - (decay_re - 1.0) * lam_im) / modulus
    for g in range(32):
        q, j = divmod(g, 8)
        at = (q, pl.ds(16 * j, 16), pl.ds(64 * j, 64))
        f_re = factor_re[g : g + 1]
        f_im = factor_im[g : g + 1]
        b_re = b_real_ref[g]
        b_im = b_imag_ref[g]
        input_re[at] = (f_re * b_re - f_im * b_im).astype(BF16)
        input_im[at] = (f_re * b_im + f_im * b_re).astype(BF16)
        readout_re[at] = readout_real_ref[g].astype(BF16)
        readout_im[at] = readout_imag_ref[g].astype(BF16)
        lane = pl.ds(64 * g, 64)
        decay_rows[pl.ds(0, 1), lane] = decay_re[g : g + 1]
        decay_rows[pl.ds(1, 1), lane] = decay_im[g : g + 1]

    pl.semaphore_wait(barrier, 10)
    for copy in swaps[:7]:
        copy.start()

    def rms_scale(values, gain):
        mean = jnp.mean(values * values, axis=1, keepdims=True)
        return (values * lax.rsqrt(mean + EPS) * gain).astype(BF16)

    loaded(7, 10)
    tokens = tokens_ref[...].astype(F32)
    drive = dot(rms_scale(tokens, norm_mix_ref[...]), w_drive_ref[...]).astype(BF16)
    loaded(10, 12)
    projected = []
    for q in range(4):
        channels = drive[:, 128 * q : 128 * q + 128]
        cols = pl.ds(512 * q, 512)
        old_re = state_ref[0, :, cols]
        old_im = state_ref[1, :, cols]
        d_re = decay_rows[pl.ds(0, 1), cols]
        d_im = decay_rows[pl.ds(1, 1), cols]
        new_re = d_re * old_re - d_im * old_im + dot(channels, input_re[q])
        new_im = d_re * old_im + d_im * old_re + dot(channels, input_im[q])
        state_out[0, :, cols] = new_re
        state_out[1, :, cols] = new_im
        projected.append(
            dot_nt(new_re.astype(BF16), readout_re[q]) - dot_nt(new_im.astype(BF16), readout_im[q])
        )
    skipped = d_skip_ref[...] * drive.astype(F32)
    readout = jax.nn.gelu(jnp.concatenate(projected, axis=1) + skipped).astype(BF16)
    loaded(12, 15)
    value_part = dot(readout, w_value_ref[...])
    gate_part = dot(readout, w_glugate_ref[...])
    mixed = (value_part * jax.nn.sigmoid(gate_part)).astype(BF16)
    resid = (tokens + dot(mixed, w_output_ref[...])).astype(BF16)
    resid_ref[...] = resid
    loaded(15, 20)
    normed = rms_scale(resid.astype(F32), norm_ffn_ref[...])

    own[...] = normed

    ids = ids_ref[...].astype(F32)
    lanes = lax.broadcasted_iota(jnp.int32, (16, 128), 1)
    down = lax.broadcasted_iota(jnp.int32, (16, 128), 0)
    this = lax.broadcasted_iota(jnp.int32, (16, 16), 0)
    that = lax.broadcasted_iota(jnp.int32, (16, 16), 1)
    columns = [
        jnp.sum(jnp.where(this == that, ids[t : t + 1], 0.0), axis=1, keepdims=True)
        for t in range(6)
    ]
    chosen = jnp.zeros((16, 128), F32)
    for column in columns:
        chosen = chosen + jnp.where(column == lanes.astype(F32), 1.0, 0.0)
    earlier = jnp.where(that < this, 1.0, 0.0)
    ordinal = dot(earlier.astype(BF16), chosen.astype(BF16))
    branch = jax.nn.sigmoid(
        jnp.sum(normed.astype(F32) * vector_ref[...], axis=1, keepdims=True)
    )
    words = jnp.where(lanes == 96 + down, branch, 0.0)
    for t, column in enumerate(columns):
        rank = jnp.sum(
            jnp.where(column == lanes.astype(F32), ordinal, 0.0), axis=1, keepdims=True
        )
        words = words + jnp.where(lanes == 16 * t + down, column + 128.0 * rank, 0.0)
    words = jnp.sum(words, axis=0, keepdims=True)
    ids_own[...] = words
    ids_all[pos["z"], pos["y"], pos["x"]] = words
    x[pos["z"], pos["y"], pos["x"]] = normed

    def view(ref, colour, offsets, cols):
        at = {}
        for d, o in zip(ORDERS[colour], offsets):
            at[d] = slice(None) if o is None else near[d][o % 4]
        return ref.at[at["z"], at["y"], at["x"], :, cols]

    def columns_of(colour, m):
        start, width = COLS[colour]
        if m[0] != "f1":
            return pl.ds(start, width)
        half = HALVES[colour]
        return pl.ds(start, half) if m[1] == 1 else pl.ds(start + half, width - half)

    def gather_copy(colour, m, receiving=False):
        d, s = link_of(colour, m)
        back = -s if receiving else 0
        where = {
            "m1": lambda: (back, 0, 0),
            "f1": lambda: (back - s, 0, 0),
            "m2": lambda: (m[1], back, 0),
            "f2": lambda: (m[1], back - s, 0),
            "m3": lambda: (m[1], m[2], back),
            "f3": lambda: (m[1], m[2], back - s),
        }[m[0]]()
        cols = columns_of(colour, m)
        target = view(x, colour, where, cols)
        source = own.at[:, cols] if where == (0, 0, 0) else target
        return pltpu.make_async_remote_copy(
            src_ref=source,
            dst_ref=target,
            send_sem=ag_send.at[colour, SLOT[m]],
            recv_sem=ag_recv.at[colour, SLOT[m]],
            device_id=(peers[d, s],),
            device_id_type=MESH,
        )

    started = []

    def id_copy(level, s, receiving=False):
        d = "xyz"[level]
        at = {"x": near["x"][0], "y": near["y"][0], "z": near["z"][0]}
        at[d] = near[d][-s % 4] if receiving else near[d][0]
        for axis in "xyz"[:level]:
            at[axis] = slice(None)
        target = ids_all.at[at["z"], at["y"], at["x"]]
        i = level * 3 + s % 4 - 1
        return pltpu.make_async_remote_copy(
            src_ref=ids_own if level == 0 and not receiving else target,
            dst_ref=target,
            send_sem=id_send.at[i],
            recv_sem=id_recv.at[i],
            device_id=(peers[d, s],),
            device_id_type=MESH,
        )

    def ids_send(level):
        for s in (1, -1, 2):
            copy = id_copy(level, s)
            copy.start()
            started.append(copy)

    def ids_receive(level):
        for s in (1, -1, 2):
            id_copy(level, s, True).wait_recv()

    first = me - core

    def slab_of(ref, d, k, cols):
        i = near[d][k]
        if d == "z":
            return ref[i, :, :, :, cols]
        if d == "y":
            return ref[:, i, :, :, cols]
        return ref[:, :, i, :, cols]

    def slab_store(ref, d, k, cols, values):
        i = near[d][k]
        values = values.reshape(4, 4, 16, values.shape[-1])
        if d == "z":
            ref[i, :, :, :, cols] = values
        elif d == "y":
            ref[:, i, :, :, cols] = values
        else:
            ref[:, :, i, :, cols] = values

    tables = {}

    def read_ids():
        table = ids_all[...].reshape(64, 128)
        lane = lax.broadcasted_iota(jnp.int32, (64, 128), 1)
        sender = lax.broadcasted_iota(jnp.int32, (64, 128), 0)
        found = []
        for e in range(2):
            for k in range(2):
                wanted = (first + e + 128 * k).astype(F32)
                hit = (table == wanted) & (lane < 96)
                row = jnp.where(hit, lax.rem(lane, 16) + 16 * sender, -1)
                found.append(jnp.max(row.astype(F32), axis=1, keepdims=True))
        code = jnp.concatenate(found, axis=0)
        tables["code"] = code
        wide = jnp.broadcast_to(code, (256, 256))
        diagonal = lax.broadcasted_iota(jnp.int32, (256, 256), 0) == lax.broadcasted_iota(
            jnp.int32, (256, 256), 1
        )
        across = jnp.sum(jnp.where(diagonal, wide, 0.0), axis=0, keepdims=True)
        tables["across"] = across

    def slots_by_rows(z):
        number = z * 256 + lax.broadcasted_iota(jnp.int32, (256, 256), 0)
        hot = jnp.where(number.astype(F32) == tables["across"], 1.0, 0.0).astype(BF16)
        hc[z, :, :, :, pl.ds(128, 256)] = hot.reshape(4, 4, 16, 256)

    def read_choices():
        code = tables["code"]
        table = ids_all[...].reshape(64, 128)
        lane = lax.broadcasted_iota(jnp.int32, (64, 128), 1)
        slot = lax.broadcasted_iota(jnp.int32, (256, 64), 0)
        same = lax.rem(slot, 64) == lax.broadcasted_iota(jnp.int32, (256, 64), 1)
        choices = dot(
            jnp.where(same, 1.0, 0.0).astype(BF16), jnp.where(lane < 96, table, 0.0).astype(BF16)
        )
        lane = lax.broadcasted_iota(jnp.int32, (256, 128), 1)
        within = code - 16.0 * lax.rem(
            lax.broadcasted_iota(jnp.int32, (256, 1), 0), 64
        ).astype(F32)
        taken = jnp.zeros((256, 128), F32)
        for t in range(6):
            word = jnp.sum(
                jnp.where(lane.astype(F32) == within + 16.0 * t, choices, 0.0), axis=1, keepdims=True
            )
            expert = jnp.where(word >= 128.0, word - 128.0, word)
            hit = (expert == lane.astype(F32)) & (code >= 0.0)
            taken = jnp.where(hit, 1.0, taken)
        tables["taken"] = taken

    def use_slab(colour, k):
        start, width = COLS[colour]
        cols = pl.ds(start, width)
        d = ORDERS[colour][2]
        values = slab_of(x, d, k, cols).reshape(256, width)
        every = pl.ds(0, 256)
        total = slab_of(sums, d, k, every).reshape(256, 256) + dot_nt(values, w_in[:, cols])
        slab_store(sums, d, k, every, total)
        lane = lax.broadcasted_iota(jnp.int32, (1, 256), 1)
        a, b, r = lane // 64, lax.rem(lane // 16, 4), lax.rem(lane, 16)
        i = near[d][k]
        if d == "z":
            sender = i * 16 + a * 4 + b
        elif d == "y":
            sender = a * 16 + i * 4 + b
        else:
            sender = a * 16 + b * 4 + i
        number = (sender * 16 + r).astype(F32)
        hot = jnp.where(tables["code"] == number, 1.0, 0.0).astype(BF16)
        rows = dot(hot, values)
        if k == 0:
            picking[:, cols] = rows
        else:
            picking[:, cols] += rows

    for g in range(4):
        group_rows[pl.ds(32 * g, 32), :] = jnp.broadcast_to(
            group_ref[pl.ds(g, 1), :].astype(F32), (32, 2048)
        ).astype(BF16)
    sums[...] = jnp.zeros((4, 4, 4, 16, 256), F32)

    gather_steps, gather_sent, _ = plan_gather()
    scatter_steps, _, _ = plan_scatter(gather_sent)
    ids_send(0)
    done = 0
    ready = []
    arrived = {}
    level = 0
    for action, c, m in gather_steps:
        if action == "send":
            copy = gather_copy(c, m)
            copy.start()
            started.append(copy)
            continue
        if done == 6:
            ids_receive(0)
            ids_send(1)
        if done == 44:
            ids_receive(1)
            ids_send(2)
        if done == 88:
            ids_receive(2)
            read_ids()
            for copy in local[:3]:
                copy.wait()
            for copy in swaps[:3]:
                copy.wait_recv()
        if done in (92, 96, 100, 104):
            slots_by_rows((done - 92) // 4)
        if done == 108:
            read_choices()
        if done >= 16 and done % 12 == 4 and 7 + done // 12 - 1 < len(swaps):
            swaps[7 + done // 12 - 1].start()
        gather_copy(c, m, True).wait_recv()
        done += 1
        k = {"f3": 2, "m3": (3 if m[-1] == 1 else 1)}.get(m[0], 0)
        arrived[c, k] = arrived.get((c, k), 1 if k == 0 else 0) + (0.5 if m[0] == "f1" else 1)
        if arrived[c, k] == 16:
            ready.append((c, k))
        if done >= 88:
            while ready:
                use_slab(*ready.pop(0))
    for copy in local[3:]:
        copy.wait()
    for copy in swaps[3:]:
        copy.wait_recv()


    @pl.loop(0, 4)
    def _(zi):
        products = sums[zi].reshape(256, 256)
        words = jnp.broadcast_to(ids_all[zi], (4, 4, 16, 128)).reshape(256, 128)
        lane = lax.broadcasted_iota(jnp.int32, (256, 128), 1)
        row = lax.broadcasted_iota(jnp.int32, (256, 128), 0)
        own_word = lane == 96 + lax.rem(row, 16)
        scale = jnp.sum(jnp.where(own_word, words, 0.0), axis=1, keepdims=True)
        hidden = (scale * jax.nn.silu(products[:, :128]) * products[:, 128:]).astype(BF16)
        hc[zi, :, :, :, pl.ds(0, 128)] = hidden.reshape(4, 4, 16, 128)

    selected = picking[...].astype(BF16)
    group_exp = jnp.exp(dot_nt(selected, group_rows[...]))
    inner_exp = jnp.exp(dot(selected, router_ref[...]))
    lane = lax.broadcasted_iota(jnp.int32, (256, 128), 1)
    row = lax.broadcasted_iota(jnp.int32, (256, 128), 0)
    group_sum = jnp.sum(jnp.where(lax.rem(lane, 32) == 0, group_exp, 0.0), axis=1, keepdims=True)
    inner_sum = jnp.zeros((256, 128), F32)
    for g in range(4):
        inside = lane // 32 == g
        total = jnp.sum(jnp.where(inside, inner_exp, 0.0), axis=1, keepdims=True)
        inner_sum = jnp.where(inside, total, inner_sum)
    inner = inner_exp / inner_sum
    joint = (group_exp / group_sum) * inner
    mine = lane == first + row // 128
    numerator = jnp.sum(jnp.where(mine, joint, 0.0), axis=1, keepdims=True)
    denominator = jnp.sum(tables["taken"] * inner, axis=1, keepdims=True)
    live = tables["code"] >= 0.0
    gates = jnp.where(live, numerator / jnp.where(live, denominator, 1.0), 0.0)

    for e in range(2):
        rows_in = selected[e * 128 : (e + 1) * 128]
        gate_part = dot(rows_in, eg[e])
        up_part = dot(rows_in, eu[e])
        hidden = (jax.nn.silu(gate_part) * up_part).astype(BF16)
        result = dot(hidden, ed[e])
        weighted = result * gates[e * 128 : (e + 1) * 128]
        w_out[pl.ds(128 + e * 128, 128), :] = weighted.astype(BF16)

    def landing(colour, m):
        width = COLS[colour][1]
        if m[0] == "m1":
            return r1.at[colour, 0 if m[1] == 1 else 1, :, pl.ds(0, width)]
        if m[0] == "f1":
            width = HALVES[colour] if m[1] == 1 else width - HALVES[colour]
            return r1.at[colour, 2 if m[1] == 1 else 3, :, pl.ds(0, width)]
        if m[0] == "m2":
            return r2.at[colour, 0 if m[2] == 1 else 1, m[1], :, pl.ds(0, width)]
        if m[0] == "f2":
            return r2.at[colour, 2, m[1], :, pl.ds(0, width)]
        if m[0] == "m3":
            return r3.at[colour, 0 if m[3] == 1 else 1, m[1], m[2], :, pl.ds(0, width)]
        return r3.at[colour, 2, m[1], m[2], :, pl.ds(0, width)]

    def scatter_copy(colour, m, receiving=False):
        d, s = link_of(colour, m)
        where = {
            "m1": lambda: (-s, 0, 0),
            "f1": lambda: (2, 0, 0),
            "m2": lambda: (m[1], -s, 0),
            "f2": lambda: (m[1], 2, 0),
            "m3": lambda: (m[1], m[2], -s),
            "f3": lambda: (m[1], m[2], 2),
        }[m[0]]()
        target = landing(colour, m)
        return pltpu.make_async_remote_copy(
            src_ref=target if receiving else view(p, colour, where, columns_of(colour, m)),
            dst_ref=target,
            send_sem=rs_send.at[colour, SLOT[m]],
            recv_sem=rs_recv.at[colour, SLOT[m]],
            device_id=(peers[d, -s],),
            device_id_type=MESH,
        )

    def product(colour, k):
        start, width = COLS[colour]
        cols = pl.ds(start, width)
        d = ORDERS[colour][2]
        left = slab_of(hc, d, k, pl.ds(0, 384)).reshape(256, 384)
        slab_store(p, d, k, cols, dot(left, w_out[:, cols]).astype(BF16))

    def add(colour, where, *messages, cols=None):
        start, width = COLS[colour]
        ref = view(p, colour, where, pl.ds(start, width) if cols is None else cols)
        total = ref[...].astype(F32)
        for m in messages:
            total = total + landing(colour, m)[...].astype(F32)
        ref[...] = total.astype(BF16)

    landed = set()
    done = 0
    for action, *what in scatter_steps:
        if action == "product":
            product(*what)
            continue
        c, m = what
        if action == "send":
            copy = scatter_copy(c, m)
            copy.start()
            started.append(copy)
            continue
        done += 1
        scatter_copy(c, m, True).wait_recv()
        landed.add((c, m))
        if m[0] == "f3":
            add(c, (m[1], m[2], -sign_of(m[2])), m)
        elif m[0] == "m3":
            other = ("m3", m[1], m[2], -m[3])
            if (c, other) in landed:
                add(c, (m[1], m[2], 0), m, other)
        elif m[0] == "f2":
            add(c, (m[1], -sign_of(m[1]), 0), m)
        elif m[0] == "m2":
            other = ("m2", m[1], -m[2])
            if (c, other) in landed:
                add(c, (m[1], 0, 0), m, other)
        elif m[0] == "f1":
            add(c, (-m[1], 0, 0), m, cols=columns_of(c, m))
    for c in range(3):
        start, width = COLS[c]
        cols = pl.ds(start, width)
        total = resid_ref[:, cols].astype(F32) + view(p, c, (0, 0, 0), cols)[...].astype(F32)
        for k in range(2):
            total = total + r1[c, k, :, pl.ds(0, width)].astype(F32)
        out_ref[:, cols] = total.astype(BF16)

    for copy in started:
        copy.wait_send()
    for copy in swaps:
        copy.wait_send()


def on_device(
    tokens,
    state,
    norm_mix,
    w_drive,
    lam_real,
    lam_imag,
    log_step,
    b_real,
    b_imag,
    readout_real,
    readout_imaginary,
    d_skip,
    w_value,
    w_glugate,
    w_output,
    norm_ffn,
    w_group,
    w_expert,
    route_ids,
    expert_gate,
    expert_up,
    expert_down,
    dense_vector,
    dense_gate,
    dense_up,
    dense_down,
):
    kinds = len(SLOT)
    vmem = pl.BlockSpec(memory_space=pltpu.VMEM)
    hbm = pl.BlockSpec(memory_space=pltpu.HBM)
    return pl.pallas_call(
        layer_kernel,
        out_shape=(
            jax.ShapeDtypeStruct((16, 2048), BF16),
            jax.ShapeDtypeStruct((2, 16, 2048), F32),
        ),
        in_specs=[hbm] * 26,
        out_specs=(vmem, vmem),
        scratch_shapes=[
            pltpu.VMEM((16, 2048), BF16),
            pltpu.VMEM((2, 16, 2048), F32),
            pltpu.VMEM((1, 2048), F32),
            pltpu.VMEM((2048, 512), BF16),
            pltpu.VMEM((32, 64), F32),
            pltpu.VMEM((32, 64), F32),
            pltpu.VMEM((1, 32), F32),
            pltpu.VMEM((32, 16, 64), F32),
            pltpu.VMEM((32, 16, 64), F32),
            pltpu.VMEM((32, 16, 64), F32),
            pltpu.VMEM((32, 16, 64), F32),
            pltpu.VMEM((1, 512), F32),
            pltpu.VMEM((512, 512), BF16),
            pltpu.VMEM((512, 512), BF16),
            pltpu.VMEM((512, 2048), BF16),
            pltpu.VMEM((1, 2048), F32),
            pltpu.VMEM((4, 2048), BF16),
            pltpu.VMEM((2048, 128), BF16),
            pltpu.VMEM((6, 16), jnp.int32),
            pltpu.VMEM((1, 2048), F32),
            pltpu.VMEM((4, 128, 512), BF16),
            pltpu.VMEM((4, 128, 512), BF16),
            pltpu.VMEM((4, 128, 512), BF16),
            pltpu.VMEM((4, 128, 512), BF16),
            pltpu.VMEM((2, 2048), F32),
            pltpu.VMEM((16, 2048), BF16),
            pltpu.VMEM((16, 2048), BF16),
            pltpu.VMEM((4, 4, 4, 16, 2048), BF16),
            pltpu.VMEM((256, 2048), BF16),
            pltpu.VMEM((384, 2048), BF16),
            pltpu.VMEM((2, 2048, 512), BF16),
            pltpu.VMEM((2, 2048, 512), BF16),
            pltpu.VMEM((2, 512, 2048), BF16),
            pltpu.VMEM((4, 4, 4, 1, 128), F32),
            pltpu.VMEM((1, 128), F32),
            pltpu.VMEM((4, 4, 4, 16, 256), F32),
            pltpu.VMEM((4, 4, 4, 16, 384), BF16),
            pltpu.VMEM((256, 2048), F32),
            pltpu.VMEM((128, 2048), BF16),
            pltpu.VMEM((4, 4, 4, 16, 2048), BF16),
            pltpu.VMEM((3, 4, 16, 768), BF16),
            pltpu.VMEM((3, 3, 4, 16, 768), BF16),
            pltpu.VMEM((3, 3, 4, 4, 16, 768), BF16),
            pltpu.SemaphoreType.DMA((20,)),
            pltpu.SemaphoreType.DMA((6,)),
            pltpu.SemaphoreType.DMA((15,)),
            pltpu.SemaphoreType.DMA((15,)),
            pltpu.SemaphoreType.DMA((9,)),
            pltpu.SemaphoreType.DMA((9,)),
            pltpu.SemaphoreType.DMA((3, kinds)),
            pltpu.SemaphoreType.DMA((3, kinds)),
            pltpu.SemaphoreType.DMA((3, kinds)),
            pltpu.SemaphoreType.DMA((3, kinds)),
        ],
        compiler_params=pltpu.CompilerParams(
            collective_id=0, has_side_effects=True, vmem_limit_bytes=47 * 1024 * 1024
        ),
        cost_estimate=pl.CostEstimate(
            flops=8_000_000_000, bytes_accessed=20_000_000, transcendentals=0
        ),
    )(*[pltpu.with_memory_space_constraint(a, pltpu.HBM) for a in (
        tokens,
        state,
        norm_mix.reshape(1, -1),
        w_drive,
        lam_real,
        lam_imag,
        log_step.reshape(1, -1),
        jnp.transpose(b_real, (0, 2, 1)),
        jnp.transpose(b_imag, (0, 2, 1)),
        readout_real,
        readout_imaginary,
        d_skip.reshape(1, -1),
        w_value,
        w_glugate,
        w_output,
        norm_ffn.reshape(1, -1),
        jnp.transpose(w_group),
        w_expert,
        jnp.transpose(route_ids),
        dense_vector.reshape(1, -1),
        jnp.transpose(dense_gate),
        jnp.transpose(dense_up),
        dense_down,
        expert_gate[0],
        expert_up[0],
        expert_down[0],
    )])


def solution(mesh):
    placed = (
        P("ep", None),
        P(None, "ep", None),
        P(),
        P(),
        P(),
        P(),
        P(),
        P(),
        P(),
        P(),
        P(),
        P(),
        P(),
        P(),
        P(),
        P(),
        P(),
        P(),
        P("ep", None),
        P("ep", None, None),
        P("ep", None, None),
        P("ep", None, None),
        P(),
        P(None, "ep"),
        P(None, "ep"),
        P("ep", None),
    )
    return jax.shard_map(
        on_device,
        mesh=mesh,
        in_specs=placed,
        out_specs=(P("ep", None), P(None, "ep", None)),
        check_vma=False,
    )
```

time: 78.8 us -> 72.1 us (0.915)
  Pallas kernels: 74.6 us -> 70 us
  local copies, waits for them, and re-layouts: 3.14 us -> 1.33 us
    pallas_call x1, Pallas kernels: 74.6 us -> 70 us  [on_device(): pl.pallas_call(layer_kernel, out_shape=(jax.ShapeDtypeStruct((16, 2048),...]
    unnamed x2, local copies, waits for them, and re-layouts: 3.14 us -> 1.33 us
where the time goes in v3:
time: 72.1 us; the launch traced here: 72 us
  Pallas kernels  70 us (97%)
  local copies, waits for them, and re-layouts  1.33 us (2%)
    pallas_call x1, Pallas kernels, on_device(): pl.pallas_call(layer_kernel, out_shape=(jax.ShapeDtypeStruct((16, 2048),...  70 us

profile of v3, /device:TPU:0, one launch (start us, length us, event | category | flops | bytes accessed | tf_op | source)
XLA Modules:
  0.0 72.0 jit_solution(6155609227193243688)
XLA Ops:
  0.6 70.0 %shard_map.257 = (bf16[16,2048]{1,0:T(8,128)(2,1)S(1)}, f32[2,16,2048]{2,1,0:T(8,128)S(1)}) custom-call(bf16[16,2048]{1,0:T(8,128)(2,1)} %tokens_hbm.1, f32[2,16,2048]{2,1,0:T(8,128)} %state_hbm.1, f32[1,2048]{1,0:T(1,128)} %bitcast.22, bf16[2048,512]{1,0:T(8,128)(2,1)} %w_drive_hbm.1, f32[32,64]{1,0:T(8,128)} %lam_real_hbm.1, f32[32,64]{1,0:T(8,128)} %lam_imag_hbm.1, ...), custom_call_target="tpu_custom_call" | custom-call | flops 8000000000 | bytes 20000000 | tf_op jit(solution)/shard_map/pallas_call | solution.py:821
  70.6 0.6 copy.30
  71.3 0.7 copy.31

commit v4 on v3

--- a/solution.py
+++ b/solution.py
@@ -13,7 +13,6 @@
 MESH = pl.DeviceIdType.MESH
 ORDERS = (("x", "y", "z"), ("y", "z", "x"), ("z", "x", "y"))
 COLS = ((0, 640), (640, 640), (1280, 768))
-HALVES = (384, 384, 384)
 RATE, DELAY, AHEAD, STEP = 46700.0, 2.0, 1.0, 0.36
 
 
@@ -21,28 +20,46 @@
     return 1 if offset in (0, 1) else -1
 
 
-def messages():
-    one = [("m1", s) for s in (1, -1)] + [("f1", s) for s in (1, -1)]
-    two = [("m2", o, s) for o in range(4) for s in (1, -1)] + [("f2", o) for o in range(4)]
-    pairs = [(o, q) for o in range(4) for q in range(4)]
-    three = [("m3", o, q, s) for o, q in pairs for s in (1, -1)] + [("f3", o, q) for o, q in pairs]
-    return one + two + three
-
-
-SLOT = {m: i for i, m in enumerate(messages())}
-
-
 def link_of(c, m):
     phase = int(m[0][1]) - 1
-    s = m[-1] if m[0] in ("m1", "m2", "m3", "f1") else sign_of(m[-1])
-    return ORDERS[c][phase], s
+    return ORDERS[c][phase], m[-1] if m[0] in ("m1", "m2", "m3") else sign_of(m[-1])
 
 
 def bytes_of(c, m):
-    width = COLS[c][1]
-    if m[0] == "f1":
-        width = HALVES[c] if m[1] == 1 else width - HALVES[c]
-    return 32.0 * width
+    return 32.0 * COLS[c][1] * (2 if m == ("m1", 2) else 1)
+
+
+def queue_of(c, m):
+    d, s = link_of(c, m)
+    return d, 1 if s == 2 else s
+
+
+def gather_group(m):
+    if m[0] == "f3":
+        return ("f3",), 16
+    if m[0] == "m3" and sign_of(m[2]) != m[3]:
+        return ("m3", m[3]), 8
+    return m, 1
+
+
+def scatter_group(m):
+    if m[0] in ("m2", "m3"):
+        return m[:-1], 2
+    return (("m1",), 3) if m[0] == "m1" else (m, 1)
+
+
+def grouped(steps, group):
+    seen, out = {}, []
+    for _, _, kind, what in sorted(steps, key=lambda step: step[:2]):
+        if kind == "receive":
+            name, size = group(what[1])
+            key = (what[0], name)
+            seen[key] = seen.get(key, 0) + 1
+            if seen[key] < size:
+                continue
+            what = key
+        out.append((kind, *what))
+    return out
 
 
 def simulate(first, react, rank):
@@ -62,8 +79,8 @@
         if kind == "ready":
             ready[item] = t
             count += 1
-            heapq.heappush(waiting.setdefault(link_of(*item), []), (rank(item), count, item))
-            links = [link_of(*item)]
+            heapq.heappush(waiting.setdefault(queue_of(*item), []), (rank(item), count, item))
+            links = [queue_of(*item)]
         elif kind == "free":
             links = [item]
         else:
@@ -77,15 +94,13 @@
                 free[k] = t + bytes_of(*m) / RATE
                 sent[m] = t
                 push(free[k], "free", k)
-                push(free[k] + DELAY, "came", m)
+                push(free[k] + (DELAY + 0.8 if m[1] == ("m1", 2) else DELAY), "came", m)
     steps = [(t, 0, "receive", m) for m, t in came.items()]
     steps += [(max(ready[m], t - AHEAD), 1, "send", m) for m, t in sent.items()]
     return steps, sent
 
 
 def plan_gather():
-    halves = {}
-
     def present(c, o, q):
         new = [(c, ("m2", o, 1)), (c, ("m2", o, -1))] if q == 0 else []
         return new + [(c, ("m3", o, q, 1)), (c, ("m3", o, q, -1))]
@@ -93,10 +108,7 @@
     def react(item):
         c, m = item
         if m[0] == "m1":
-            return [(c, ("f1", m[1]))] + present(c, 3 if m[1] == 1 else 1, 0)
-        if m[0] == "f1":
-            halves[c] = halves.get(c, 0) + 1
-            return present(c, 2, 0) if halves[c] == 2 else []
+            return present(c, {1: 3, -1: 1, 2: 2}[m[1]], 0)
         if m[0] == "m2":
             o, s = m[1:]
             new = [(c, ("f2", o))] if sign_of(o) == s else []
@@ -107,12 +119,12 @@
             return [(c, ("f3", m[1], m[2]))]
         return []
 
-    start = [(c, ("m1", s)) for c in range(3) for s in (1, -1)]
+    start = [(c, ("m1", s)) for s in (1, -1, 2) for c in range(3)]
     for c in range(3):
         start += present(c, 0, 0)
-    rank = {"m1": 0, "f1": 0, "m2": 1, "f2": 1, "m3": 2, "f3": 3}
+    rank = {"m1": 0, "m2": 1, "f2": 1, "m3": 2, "f3": 3}
     steps, sent = simulate([(0.0, start)], react, lambda item: rank[item[1][0]])
-    return [(kind, *m) for _, _, kind, m in sorted(steps, key=lambda s: s[:2])], sent, steps
+    return grouped(steps, gather_group), sent
 
 
 def plan_scatter(sent):
@@ -137,12 +149,7 @@
             seen[c, "sum", o] = seen.get((c, "sum", o), 0) + 1
             if seen[c, "sum", o] < 3:
                 return []
-            if o == 2:
-                return [(c, ("f1", 1)), (c, ("f1", -1))]
-            if o == 0:
-                return []
-            s = -1 if o == 1 else 1
-            return [(c, ("m1", s))] if both(("m1", s)) else []
+            return [(c, ("m1", {1: -1, 2: 2, 3: 1}[o]))] if o else []
 
         if m[0] == "f3":
             s = sign_of(m[2])
@@ -154,8 +161,6 @@
             return [(c, ("m2", m[1], s))] if both(("m2", m[1], s)) else []
         if m[0] == "m2":
             return level1(m[1])
-        if m[0] == "f1":
-            return [(c, ("m1", m[1]))] if both(("m1", m[1])) else []
         return []
 
     first, products, t = [], [], 0.0
@@ -174,9 +179,21 @@
                     if sign_of(q) == s:
                         seen[c, ("m3", o, q, s)] = 1
     last = max(sent.values())
-    steps, out = simulate(first, react, lambda item: last - sent[item])
-    steps = steps + products
-    return [(kind, *m) for _, _, kind, m in sorted(steps, key=lambda s: s[:2])], out, steps
+    steps, _ = simulate(first, react, lambda item: last - sent[item])
+    return grouped(steps + products, scatter_group)
+
+
+def numbered(group):
+    one = [("m1", s) for s in (1, -1, 2)]
+    two = [("m2", o, s) for o in range(4) for s in (1, -1)] + [("f2", o) for o in range(4)]
+    pairs = [(o, q) for o in range(4) for q in range(4)]
+    three = [("m3", o, q, s) for o, q in pairs for s in (1, -1)] + [("f3", o, q) for o, q in pairs]
+    names = dict.fromkeys(group(m)[0] for m in one + two + three)
+    return {name: i for i, name in enumerate(names)}
+
+
+GATHER_SLOT = numbered(gather_group)
+SCATTER_SLOT = numbered(scatter_group)
 
 
 def dot(a, b):
@@ -218,24 +235,17 @@
     state_out,
     tokens_ref,
     state_ref,
-    norm_mix_ref,
+    norms_ref,
     w_drive_ref,
-    lam_real_ref,
-    lam_imag_ref,
+    lam_ref,
     log_step_ref,
-    b_real_ref,
-    b_imag_ref,
-    readout_real_ref,
-    readout_imag_ref,
+    maps_ref,
     d_skip_ref,
-    w_value_ref,
-    w_glugate_ref,
+    glu_ref,
     w_output_ref,
-    norm_ffn_ref,
     group_ref,
     router_ref,
     ids_ref,
-    vector_ref,
     input_re,
     input_im,
     readout_re,
@@ -290,27 +300,32 @@
     for peer in [*peers.values(), partner]:
         pl.semaphore_signal(barrier, inc=1, device_id=(peer,), device_id_type=MESH)
 
-    sources = (
-        lam_real_hbm, lam_imag_hbm, log_step_hbm, b_real_hbm, b_imag_hbm, readout_real_hbm,
-        readout_imag_hbm, tokens_hbm, norm_mix_hbm, w_drive_hbm, state_hbm, d_skip_hbm,
-        w_value_hbm, w_glugate_hbm, w_output_hbm, norm_ffn_hbm, ids_hbm, vector_hbm, group_hbm,
-        router_hbm,
+    def await_bytes(ref, semaphore):
+        pltpu.make_async_copy(ref, ref, semaphore).wait()
+
+    loads = (
+        ((lam_real_hbm, lam_imag_hbm), lam_ref),
+        ((log_step_hbm,), log_step_ref),
+        ((b_real_hbm, b_imag_hbm, readout_real_hbm, readout_imag_hbm), maps_ref),
+        ((tokens_hbm,), tokens_ref),
+        ((norm_mix_hbm, norm_ffn_hbm, vector_hbm), norms_ref),
+        ((w_drive_hbm,), w_drive_ref),
+        ((state_hbm,), state_ref),
+        ((d_skip_hbm,), d_skip_ref),
+        ((w_value_hbm, w_glugate_hbm), glu_ref),
+        ((w_output_hbm,), w_output_ref),
+        ((ids_hbm,), ids_ref),
+        ((group_hbm,), group_ref),
+        ((router_hbm,), router_ref),
     )
-    targets = (
-        lam_real_ref, lam_imag_ref, log_step_ref, b_real_ref, b_imag_ref, readout_real_ref,
-        readout_imag_ref, tokens_ref, norm_mix_ref, w_drive_ref, state_ref, d_skip_ref,
-        w_value_ref, w_glugate_ref, w_output_ref, norm_ffn_ref, ids_ref, vector_ref, group_ref,
-        router_ref,
-    )
-    loads = [
-        pltpu.make_async_copy(a, b, load_sem.at[i]) for i, (a, b) in enumerate(zip(sources, targets))
-    ]
-    for copy in loads:
-        copy.start()
-
-    def loaded(first, last):
-        for copy in loads[first:last]:
-            copy.wait()
+    for i, (sources, target) in enumerate(loads):
+        for j, source in enumerate(sources):
+            part = target.at[j] if len(sources) > 1 else target
+            pltpu.make_async_copy(source, part, load_sem.at[i]).start()
+
+    def loaded(begin, end):
+        for i in range(begin, end):
+            await_bytes(loads[i][1], load_sem.at[i])
 
     def rows(i):
         return pl.ds(pl.multiple_of(i * 64, 64), 64)
@@ -323,13 +338,15 @@
         (eu_hbm, eu.at[core]),
         (ed_hbm, ed.at[core]),
     ]
-    local = [pltpu.make_async_copy(s, t, local_sem.at[i]) for i, (s, t) in enumerate(weights)]
-    for copy in local:
-        copy.start()
-    pieces = list(weights[:3])
-    for s, t in weights[3:]:
+    group = (0, 0, 0, 1, 2, 3)
+    for i, (s, t) in zip(group, weights):
+        pltpu.make_async_copy(s, t, local_sem.at[i]).start()
+    pieces = [(0, *pair) for pair in weights[:3]]
+    for j, (s, t) in enumerate(weights[3:]):
         depth = s.shape[0] // 4
-        pieces += [(s.at[pl.ds(i * depth, depth)], t.at[pl.ds(i * depth, depth)]) for i in range(4)]
+        for i in range(4):
+            part = pl.ds(i * depth, depth)
+            pieces.append((1 + j, s.at[part], t.at[part]))
     swaps = [
         pltpu.make_async_remote_copy(
             src_ref=s,
@@ -339,20 +356,25 @@
             device_id=(partner,),
             device_id_type=MESH,
         )
-        for i, (s, t) in enumerate(pieces)
+        for i, s, t in pieces
     ]
+    swapped = (w_out.at[pl.ds(0, 192)], eg.at[0], eu.at[0], ed.at[0])
+
+    def weights_wait(i):
+        await_bytes(swapped[i], local_sem.at[i])
+        await_bytes(swapped[i], swap_recv.at[i])
 
     for ref in (input_re, input_im, readout_re, readout_im):
         ref[...] = jnp.zeros((4, 128, 512), BF16)
-    loaded(0, 7)
+    loaded(0, 3)
     square = lax.broadcasted_iota(jnp.int32, (32, 32), 0) == lax.broadcasted_iota(
         jnp.int32, (32, 32), 1
     )
     time_step = jnp.sum(
         jnp.where(square, jnp.exp(log_step_ref[...]), 0.0), axis=1, keepdims=True
     )
-    lam_re = lam_real_ref[...]
-    lam_im = lam_imag_ref[...]
+    lam_re = lam_ref[0]
+    lam_im = lam_ref[1]
     magnitude = jnp.exp(lam_re * time_step)
     decay_re = magnitude * jnp.cos(lam_im * time_step)
     decay_im = magnitude * jnp.sin(lam_im * time_step)
@@ -364,12 +386,12 @@
         at = (q, pl.ds(16 * j, 16), pl.ds(64 * j, 64))
         f_re = factor_re[g : g + 1]
         f_im = factor_im[g : g + 1]
-        b_re = b_real_ref[g]
-        b_im = b_imag_ref[g]
+        b_re = maps_ref[0, g]
+        b_im = maps_ref[1, g]
         input_re[at] = (f_re * b_re - f_im * b_im).astype(BF16)
         input_im[at] = (f_re * b_im + f_im * b_re).astype(BF16)
-        readout_re[at] = readout_real_ref[g].astype(BF16)
-        readout_im[at] = readout_imag_ref[g].astype(BF16)
+        readout_re[at] = maps_ref[2, g].astype(BF16)
+        readout_im[at] = maps_ref[3, g].astype(BF16)
         lane = pl.ds(64 * g, 64)
         decay_rows[pl.ds(0, 1), lane] = decay_re[g : g + 1]
         decay_rows[pl.ds(1, 1), lane] = decay_im[g : g + 1]
@@ -382,10 +404,10 @@
         mean = jnp.mean(values * values, axis=1, keepdims=True)
         return (values * lax.rsqrt(mean + EPS) * gain).astype(BF16)
 
-    loaded(7, 10)
+    loaded(3, 6)
     tokens = tokens_ref[...].astype(F32)
-    drive = dot(rms_scale(tokens, norm_mix_ref[...]), w_drive_ref[...]).astype(BF16)
-    loaded(10, 12)
+    drive = dot(rms_scale(tokens, norms_ref[0]), w_drive_ref[...]).astype(BF16)
+    loaded(6, 8)
     projected = []
     for q in range(4):
         channels = drive[:, 128 * q : 128 * q + 128]
@@ -403,14 +425,14 @@
         )
     skipped = d_skip_ref[...] * drive.astype(F32)
     readout = jax.nn.gelu(jnp.concatenate(projected, axis=1) + skipped).astype(BF16)
-    loaded(12, 15)
-    value_part = dot(readout, w_value_ref[...])
-    gate_part = dot(readout, w_glugate_ref[...])
+    loaded(8, 10)
+    value_part = dot(readout, glu_ref[0])
+    gate_part = dot(readout, glu_ref[1])
     mixed = (value_part * jax.nn.sigmoid(gate_part)).astype(BF16)
     resid = (tokens + dot(mixed, w_output_ref[...])).astype(BF16)
     resid_ref[...] = resid
-    loaded(15, 20)
-    normed = rms_scale(resid.astype(F32), norm_ffn_ref[...])
+    loaded(10, 13)
+    normed = rms_scale(resid.astype(F32), norms_ref[1])
 
     own[...] = normed
 
@@ -429,7 +451,7 @@
     earlier = jnp.where(that < this, 1.0, 0.0)
     ordinal = dot(earlier.astype(BF16), chosen.astype(BF16))
     branch = jax.nn.sigmoid(
-        jnp.sum(normed.astype(F32) * vector_ref[...], axis=1, keepdims=True)
+        jnp.sum(normed.astype(F32) * norms_ref[2], axis=1, keepdims=True)
     )
     words = jnp.where(lanes == 96 + down, branch, 0.0)
     for t, column in enumerate(columns):
@@ -448,64 +470,58 @@
             at[d] = slice(None) if o is None else near[d][o % 4]
         return ref.at[at["z"], at["y"], at["x"], :, cols]
 
-    def columns_of(colour, m):
-        start, width = COLS[colour]
-        if m[0] != "f1":
-            return pl.ds(start, width)
-        half = HALVES[colour]
-        return pl.ds(start, half) if m[1] == 1 else pl.ds(start + half, width - half)
-
-    def gather_copy(colour, m, receiving=False):
+    def whole(colour):
+        return pl.ds(*COLS[colour])
+
+    def gather_copy(colour, m):
         d, s = link_of(colour, m)
-        back = -s if receiving else 0
         where = {
-            "m1": lambda: (back, 0, 0),
-            "f1": lambda: (back - s, 0, 0),
-            "m2": lambda: (m[1], back, 0),
-            "f2": lambda: (m[1], back - s, 0),
-            "m3": lambda: (m[1], m[2], back),
-            "f3": lambda: (m[1], m[2], back - s),
+            "m1": lambda: (0, 0, 0),
+            "m2": lambda: (m[1], 0, 0),
+            "f2": lambda: (m[1], -s, 0),
+            "m3": lambda: (m[1], m[2], 0),
+            "f3": lambda: (m[1], m[2], -s),
         }[m[0]]()
-        cols = columns_of(colour, m)
-        target = view(x, colour, where, cols)
-        source = own.at[:, cols] if where == (0, 0, 0) else target
+        target = view(x, colour, where, whole(colour))
         return pltpu.make_async_remote_copy(
-            src_ref=source,
+            src_ref=own.at[:, whole(colour)] if where == (0, 0, 0) else target,
             dst_ref=target,
-            send_sem=ag_send.at[colour, SLOT[m]],
-            recv_sem=ag_recv.at[colour, SLOT[m]],
+            send_sem=ag_send.at[colour, int(m[0][1]) - 1],
+            recv_sem=ag_recv.at[colour, GATHER_SLOT[gather_group(m)[0]]],
             device_id=(peers[d, s],),
             device_id_type=MESH,
         )
 
-    started = []
-
-    def id_copy(level, s, receiving=False):
-        d = "xyz"[level]
-        at = {"x": near["x"][0], "y": near["y"][0], "z": near["z"][0]}
-        at[d] = near[d][-s % 4] if receiving else near[d][0]
+    def gather_wait(colour, name):
+        size = {("f3",): 16}.get(name, 8 if len(name) == 2 and name[0] == "m3" else 1)
+        cols = whole(colour)
+        ref = {16: x.at[0, :, :, :, cols], 8: x.at[0, pl.ds(0, 2), :, :, cols]}.get(
+            size, x.at[0, 0, 0, :, cols]
+        )
+        await_bytes(ref, ag_recv.at[colour, GATHER_SLOT[name]])
+        return size
+
+    def ids_send(level):
+        at = dict(pos)
         for axis in "xyz"[:level]:
             at[axis] = slice(None)
         target = ids_all.at[at["z"], at["y"], at["x"]]
-        i = level * 3 + s % 4 - 1
-        return pltpu.make_async_remote_copy(
-            src_ref=ids_own if level == 0 and not receiving else target,
-            dst_ref=target,
-            send_sem=id_send.at[i],
-            recv_sem=id_recv.at[i],
-            device_id=(peers[d, s],),
-            device_id_type=MESH,
-        )
-
-    def ids_send(level):
         for s in (1, -1, 2):
-            copy = id_copy(level, s)
-            copy.start()
-            started.append(copy)
+            pltpu.make_async_remote_copy(
+                src_ref=target if level else ids_own,
+                dst_ref=target,
+                send_sem=id_send.at[level],
+                recv_sem=id_recv.at[level],
+                device_id=(peers["xyz"[level], s],),
+                device_id_type=MESH,
+            ).start()
+
+    def three(level):
+        three = pl.ds(0, 3)
+        return (ids_all.at[0, 0, three], ids_all.at[0, three], ids_all.at[three])[level]
 
     def ids_receive(level):
-        for s in (1, -1, 2):
-            id_copy(level, s, True).wait_recv()
+        await_bytes(three(level), id_recv.at[level])
 
     first = me - core
 
@@ -608,51 +624,59 @@
         ).astype(BF16)
     sums[...] = jnp.zeros((4, 4, 4, 16, 256), F32)
 
-    gather_steps, gather_sent, _ = plan_gather()
-    scatter_steps, _, _ = plan_scatter(gather_sent)
+    experts_in = {}
+
+    def use_columns(colour):
+        start, width = COLS[colour]
+        cols = pl.ds(start, width)
+        rows = picking[:, cols].astype(BF16)
+        parts = [dot_nt(rows, group_rows[:, cols]), dot(rows, router_ref[cols, :])]
+        for e in range(2):
+            mine = rows[e * 128 : (e + 1) * 128]
+            parts += [dot(mine, eg[e, cols, :]), dot(mine, eu[e, cols, :])]
+        for i, part in enumerate(parts):
+            experts_in[i] = experts_in[i] + part if i in experts_in else part
+
+    gather_steps, gather_sent = plan_gather()
+    scatter_steps = plan_scatter(gather_sent)
     ids_send(0)
     done = 0
     ready = []
     arrived = {}
-    level = 0
+    tasks = [
+        (6, lambda: (ids_receive(0), ids_send(1))),
+        (40, lambda: (ids_receive(1), ids_send(2))),
+        (84, lambda: (ids_receive(2), read_ids(), weights_wait(0))),
+        (88, lambda: slots_by_rows(0)),
+        (92, lambda: slots_by_rows(1)),
+        (96, lambda: slots_by_rows(2)),
+        (100, lambda: slots_by_rows(3)),
+        (104, read_choices),
+    ]
+    more = swaps[7:]
     for action, c, m in gather_steps:
         if action == "send":
-            copy = gather_copy(c, m)
-            copy.start()
-            started.append(copy)
+            gather_copy(c, m).start()
             continue
-        if done == 6:
-            ids_receive(0)
-            ids_send(1)
-        if done == 44:
-            ids_receive(1)
-            ids_send(2)
-        if done == 88:
-            ids_receive(2)
-            read_ids()
-            for copy in local[:3]:
-                copy.wait()
-            for copy in swaps[:3]:
-                copy.wait_recv()
-        if done in (92, 96, 100, 104):
-            slots_by_rows((done - 92) // 4)
-        if done == 108:
-            read_choices()
-        if done >= 16 and done % 12 == 4 and 7 + done // 12 - 1 < len(swaps):
-            swaps[7 + done // 12 - 1].start()
-        gather_copy(c, m, True).wait_recv()
-        done += 1
-        k = {"f3": 2, "m3": (3 if m[-1] == 1 else 1)}.get(m[0], 0)
-        arrived[c, k] = arrived.get((c, k), 1 if k == 0 else 0) + (0.5 if m[0] == "f1" else 1)
+        while tasks and done >= tasks[0][0]:
+            tasks.pop(0)[1]()
+        if more and done >= 12 * (8 - len(more)):
+            more.pop(0).start()
+        size = gather_wait(c, m)
+        done += size
+        k = 2 if m[0] == "f3" else (3 if m[-1] == 1 else 1) if m[0] == "m3" else 0
+        arrived[c, k] = arrived.get((c, k), 1 if k == 0 else 0) + size
         if arrived[c, k] == 16:
             ready.append((c, k))
-        if done >= 88:
-            while ready:
-                use_slab(*ready.pop(0))
-    for copy in local[3:]:
-        copy.wait()
-    for copy in swaps[3:]:
-        copy.wait_recv()
+        while ready and done >= 88:
+            c, k = ready.pop(0)
+            if k == 2 and not experts_in:
+                weights_wait(1)
+                weights_wait(2)
+            use_slab(c, k)
+            if k == 2:
+                use_columns(c)
+    weights_wait(3)
 
 
     @pl.loop(0, 4)
@@ -666,9 +690,8 @@
         hidden = (scale * jax.nn.silu(products[:, :128]) * products[:, 128:]).astype(BF16)
         hc[zi, :, :, :, pl.ds(0, 128)] = hidden.reshape(4, 4, 16, 128)
 
-    selected = picking[...].astype(BF16)
-    group_exp = jnp.exp(dot_nt(selected, group_rows[...]))
-    inner_exp = jnp.exp(dot(selected, router_ref[...]))
+    group_exp = jnp.exp(experts_in[0])
+    inner_exp = jnp.exp(experts_in[1])
     lane = lax.broadcasted_iota(jnp.int32, (256, 128), 1)
     row = lax.broadcasted_iota(jnp.int32, (256, 128), 0)
     group_sum = jnp.sum(jnp.where(lax.rem(lane, 32) == 0, group_exp, 0.0), axis=1, keepdims=True)
@@ -686,48 +709,54 @@
     gates = jnp.where(live, numerator / jnp.where(live, denominator, 1.0), 0.0)
 
     for e in range(2):
-        rows_in = selected[e * 128 : (e + 1) * 128]
-        gate_part = dot(rows_in, eg[e])
-        up_part = dot(rows_in, eu[e])
-        hidden = (jax.nn.silu(gate_part) * up_part).astype(BF16)
+        hidden = (jax.nn.silu(experts_in[2 + 2 * e]) * experts_in[3 + 2 * e]).astype(BF16)
         result = dot(hidden, ed[e])
         weighted = result * gates[e * 128 : (e + 1) * 128]
         w_out[pl.ds(128 + e * 128, 128), :] = weighted.astype(BF16)
 
     def landing(colour, m):
-        width = COLS[colour][1]
+        cols = pl.ds(0, COLS[colour][1])
+        i = {1: 0, -1: 1, 2: 2}
         if m[0] == "m1":
-            return r1.at[colour, 0 if m[1] == 1 else 1, :, pl.ds(0, width)]
-        if m[0] == "f1":
-            width = HALVES[colour] if m[1] == 1 else width - HALVES[colour]
-            return r1.at[colour, 2 if m[1] == 1 else 3, :, pl.ds(0, width)]
+            return r1.at[colour, i[m[1]], :, cols]
         if m[0] == "m2":
-            return r2.at[colour, 0 if m[2] == 1 else 1, m[1], :, pl.ds(0, width)]
+            return r2.at[colour, i[m[2]], m[1], :, cols]
         if m[0] == "f2":
-            return r2.at[colour, 2, m[1], :, pl.ds(0, width)]
+            return r2.at[colour, 2, m[1], :, cols]
         if m[0] == "m3":
-            return r3.at[colour, 0 if m[3] == 1 else 1, m[1], m[2], :, pl.ds(0, width)]
-        return r3.at[colour, 2, m[1], m[2], :, pl.ds(0, width)]
-
-    def scatter_copy(colour, m, receiving=False):
+            return r3.at[colour, i[m[3]], m[1], m[2], :, cols]
+        return r3.at[colour, 2, m[1], m[2], :, cols]
+
+    def scatter_copy(colour, m):
         d, s = link_of(colour, m)
         where = {
             "m1": lambda: (-s, 0, 0),
-            "f1": lambda: (2, 0, 0),
             "m2": lambda: (m[1], -s, 0),
             "f2": lambda: (m[1], 2, 0),
             "m3": lambda: (m[1], m[2], -s),
             "f3": lambda: (m[1], m[2], 2),
         }[m[0]]()
-        target = landing(colour, m)
         return pltpu.make_async_remote_copy(
-            src_ref=target if receiving else view(p, colour, where, columns_of(colour, m)),
-            dst_ref=target,
-            send_sem=rs_send.at[colour, SLOT[m]],
-            recv_sem=rs_recv.at[colour, SLOT[m]],
-            device_id=(peers[d, -s],),
+            src_ref=view(p, colour, where, whole(colour)),
+            dst_ref=landing(colour, m),
+            send_sem=rs_send.at[colour, int(m[0][1]) - 1],
+            recv_sem=rs_recv.at[colour, SCATTER_SLOT[scatter_group(m)[0]]],
+            device_id=(peers[d, s if s == 2 else -s],),
             device_id_type=MESH,
         )
+
+    def scatter_wait(colour, name):
+        cols = pl.ds(0, COLS[colour][1])
+        two = pl.ds(0, 2)
+        if name[0] == "m1":
+            ref = r1.at[colour, :, :, cols]
+        elif name[0] == "m2":
+            ref = r2.at[colour, two, name[1], :, cols]
+        elif name[0] == "m3":
+            ref = r3.at[colour, two, name[1], name[2], :, cols]
+        else:
+            ref = landing(colour, name)
+        await_bytes(ref, rs_recv.at[colour, SCATTER_SLOT[name]])
 
     def product(colour, k):
         start, width = COLS[colour]
@@ -736,15 +765,13 @@
         left = slab_of(hc, d, k, pl.ds(0, 384)).reshape(256, 384)
         slab_store(p, d, k, cols, dot(left, w_out[:, cols]).astype(BF16))
 
-    def add(colour, where, *messages, cols=None):
-        start, width = COLS[colour]
-        ref = view(p, colour, where, pl.ds(start, width) if cols is None else cols)
+    def add(colour, where, *messages):
+        ref = view(p, colour, where, whole(colour))
         total = ref[...].astype(F32)
         for m in messages:
             total = total + landing(colour, m)[...].astype(F32)
         ref[...] = total.astype(BF16)
 
-    landed = set()
     done = 0
     for action, *what in scatter_steps:
         if action == "product":
@@ -752,39 +779,41 @@
             continue
         c, m = what
         if action == "send":
-            copy = scatter_copy(c, m)
-            copy.start()
-            started.append(copy)
+            scatter_copy(c, m).start()
             continue
         done += 1
-        scatter_copy(c, m, True).wait_recv()
-        landed.add((c, m))
+        scatter_wait(c, m)
         if m[0] == "f3":
             add(c, (m[1], m[2], -sign_of(m[2])), m)
-        elif m[0] == "m3":
-            other = ("m3", m[1], m[2], -m[3])
-            if (c, other) in landed:
-                add(c, (m[1], m[2], 0), m, other)
         elif m[0] == "f2":
             add(c, (m[1], -sign_of(m[1]), 0), m)
+        elif m[0] == "m3":
+            add(c, (m[1], m[2], 0), (*m, 1), (*m, -1))
         elif m[0] == "m2":
-            other = ("m2", m[1], -m[2])
-            if (c, other) in landed:
-                add(c, (m[1], 0, 0), m, other)
-        elif m[0] == "f1":
-            add(c, (-m[1], 0, 0), m, cols=columns_of(c, m))
+            add(c, (m[1], 0, 0), (*m, 1), (*m, -1))
     for c in range(3):
         start, width = COLS[c]
         cols = pl.ds(start, width)
         total = resid_ref[:, cols].astype(F32) + view(p, c, (0, 0, 0), cols)[...].astype(F32)
-        for k in range(2):
+        for k in range(3):
             total = total + r1[c, k, :, pl.ds(0, width)].astype(F32)
         out_ref[:, cols] = total.astype(BF16)
 
-    for copy in started:
-        copy.wait_send()
-    for copy in swaps:
-        copy.wait_send()
+    for level in range(3):
+        await_bytes(three(level), id_send.at[level])
+    for i in range(4):
+        await_bytes(swapped[i], swap_send.at[i])
+    for c in range(3):
+        cols = whole(c)
+        three_blocks = pl.ds(0, 3)
+        sent = (
+            x.at[0, 0, three_blocks, :, cols],
+            x.at[0, three_blocks, :, :, cols],
+            x.at[three_blocks, :, :, :, cols],
+        )
+        for i in range(3):
+            await_bytes(sent[i], ag_send.at[c, i])
+            await_bytes(sent[i], rs_send.at[c, i])
 
 
 def on_device(
@@ -815,7 +844,6 @@
     dense_up,
     dense_down,
 ):
-    kinds = len(SLOT)
     vmem = pl.BlockSpec(memory_space=pltpu.VMEM)
     hbm = pl.BlockSpec(memory_space=pltpu.HBM)
     return pl.pallas_call(
@@ -829,24 +857,17 @@
         scratch_shapes=[
             pltpu.VMEM((16, 2048), BF16),
             pltpu.VMEM((2, 16, 2048), F32),
-            pltpu.VMEM((1, 2048), F32),
+            pltpu.VMEM((3, 1, 2048), F32),
             pltpu.VMEM((2048, 512), BF16),
-            pltpu.VMEM((32, 64), F32),
-            pltpu.VMEM((32, 64), F32),
+            pltpu.VMEM((2, 32, 64), F32),
             pltpu.VMEM((1, 32), F32),
-            pltpu.VMEM((32, 16, 64), F32),
-            pltpu.VMEM((32, 16, 64), F32),
-            pltpu.VMEM((32, 16, 64), F32),
-            pltpu.VMEM((32, 16, 64), F32),
+            pltpu.VMEM((4, 32, 16, 64), F32),
             pltpu.VMEM((1, 512), F32),
-            pltpu.VMEM((512, 512), BF16),
-            pltpu.VMEM((512, 512), BF16),
+            pltpu.VMEM((2, 512, 512), BF16),
             pltpu.VMEM((512, 2048), BF16),
-            pltpu.VMEM((1, 2048), F32),
             pltpu.VMEM((4, 2048), BF16),
             pltpu.VMEM((2048, 128), BF16),
             pltpu.VMEM((6, 16), jnp.int32),
-            pltpu.VMEM((1, 2048), F32),
             pltpu.VMEM((4, 128, 512), BF16),
             pltpu.VMEM((4, 128, 512), BF16),
             pltpu.VMEM((4, 128, 512), BF16),
@@ -867,19 +888,19 @@
             pltpu.VMEM((256, 2048), F32),
             pltpu.VMEM((128, 2048), BF16),
             pltpu.VMEM((4, 4, 4, 16, 2048), BF16),
-            pltpu.VMEM((3, 4, 16, 768), BF16),
+            pltpu.VMEM((3, 3, 16, 768), BF16),
             pltpu.VMEM((3, 3, 4, 16, 768), BF16),
             pltpu.VMEM((3, 3, 4, 4, 16, 768), BF16),
-            pltpu.SemaphoreType.DMA((20,)),
-            pltpu.SemaphoreType.DMA((6,)),
-            pltpu.SemaphoreType.DMA((15,)),
-            pltpu.SemaphoreType.DMA((15,)),
-            pltpu.SemaphoreType.DMA((9,)),
-            pltpu.SemaphoreType.DMA((9,)),
-            pltpu.SemaphoreType.DMA((3, kinds)),
-            pltpu.SemaphoreType.DMA((3, kinds)),
-            pltpu.SemaphoreType.DMA((3, kinds)),
-            pltpu.SemaphoreType.DMA((3, kinds)),
+            pltpu.SemaphoreType.DMA((13,)),
+            pltpu.SemaphoreType.DMA((4,)),
+            pltpu.SemaphoreType.DMA((4,)),
+            pltpu.SemaphoreType.DMA((4,)),
+            pltpu.SemaphoreType.DMA((3,)),
+            pltpu.SemaphoreType.DMA((3,)),
+            pltpu.SemaphoreType.DMA((3, 3)),
+            pltpu.SemaphoreType.DMA((3, len(GATHER_SLOT))),
+            pltpu.SemaphoreType.DMA((3, 3)),
+            pltpu.SemaphoreType.DMA((3, len(SCATTER_SLOT))),
         ],
         compiler_params=pltpu.CompilerParams(
             collective_id=0, has_side_effects=True, vmem_limit_bytes=47 * 1024 * 1024

time: 72.1 us -> 64.6 us (0.90)
  Pallas kernels: 70 us -> 62.4 us
    pallas_call x1, Pallas kernels: 70 us -> 62.4 us  [on_device(): pl.pallas_call(layer_kernel, out_shape=(jax.ShapeDtypeStruct((16, 2048),...]
where the time goes in v4:
time: 64.6 us; the launch traced here: 64.4 us
  Pallas kernels  62.4 us (97%)
  local copies, waits for them, and re-layouts  1.33 us (2%)
  between operations  0.65 us (1%)
    pallas_call x1, Pallas kernels, on_device(): pl.pallas_call(layer_kernel, out_shape=(jax.ShapeDtypeStruct((16, 2048),...  62.4 us
    unnamed x2, local copies, waits for them, and re-layouts  1.33 us

profile of v4, /device:TPU:0, one launch (start us, length us, event | category | flops | bytes accessed | tf_op | source)
XLA Modules:
  0.0 64.4 jit_solution(12659976271182042902)
XLA Ops:
  0.6 62.4 %shard_map.257 = (bf16[16,2048]{1,0:T(8,128)(2,1)S(1)}, f32[2,16,2048]{2,1,0:T(8,128)S(1)}) custom-call(bf16[16,2048]{1,0:T(8,128)(2,1)} %tokens_hbm.1, f32[2,16,2048]{2,1,0:T(8,128)} %state_hbm.1, f32[1,2048]{1,0:T(1,128)} %bitcast.22, bf16[2048,512]{1,0:T(8,128)(2,1)} %w_drive_hbm.1, f32[32,64]{1,0:T(8,128)} %lam_real_hbm.1, f32[32,64]{1,0:T(8,128)} %lam_imag_hbm.1, ...), custom_call_target="tpu_custom_call" | custom-call | flops 8000000000 | bytes 20000000 | tf_op jit(solution)/shard_map/pallas_call | solution.py:849
  63.1 0.6 copy.30
  63.7 0.7 %copy.31 = f32[2,16,2048]{2,1,0:T(8,128)} copy(f32[2,16,2048]{2,1,0:T(8,128)S(1)} %get-tuple-element.5) | data formatting | bytes 524288

commit v5 on v4

--- a/solution.py
+++ b/solution.py
@@ -13,7 +13,9 @@
 MESH = pl.DeviceIdType.MESH
 ORDERS = (("x", "y", "z"), ("y", "z", "x"), ("z", "x", "y"))
 COLS = ((0, 640), (640, 640), (1280, 768))
-RATE, DELAY, AHEAD, STEP = 46700.0, 2.0, 1.0, 0.36
+RATE, DELAY, STEP = 46700.0, 2.9, 0.36
+GATHER_AHEAD, SCATTER_AHEAD = (1.0, 0.3), (0.6, 0.3)
+SLACK = 0.4
 
 
 def sign_of(offset):
@@ -59,10 +61,21 @@
                 continue
             what = key
         out.append((kind, *what))
-    return out
-
-
-def simulate(first, react, rank):
+    merged, place = [], {}
+    since = 0
+    for step in out:
+        if not step[0].startswith("send"):
+            since = len(merged)
+        elif place.get(step[1:], -1) >= since:
+            merged[place[step[1:]]] = ("send", *step[1:])
+            continue
+        else:
+            place[step[1:]] = len(merged)
+        merged.append(step)
+    return merged
+
+
+def simulate(first, react, rank, aheads):
     queue, waiting, free, count = [], {}, {}, 0
     sent, came, ready = {}, {}, {}
 
@@ -96,7 +109,8 @@
                 push(free[k], "free", k)
                 push(free[k] + (DELAY + 0.8 if m[1] == ("m1", 2) else DELAY), "came", m)
     steps = [(t, 0, "receive", m) for m, t in came.items()]
-    steps += [(max(ready[m], t - AHEAD), 1, "send", m) for m, t in sent.items()]
+    for core, ahead in enumerate(aheads):
+        steps += [(max(ready[m], t - ahead), 1, "send%d" % core, m) for m, t in sent.items()]
     return steps, sent
 
 
@@ -123,8 +137,8 @@
     for c in range(3):
         start += present(c, 0, 0)
     rank = {"m1": 0, "m2": 1, "f2": 1, "m3": 2, "f3": 3}
-    steps, sent = simulate([(0.0, start)], react, lambda item: rank[item[1][0]])
-    return grouped(steps, gather_group), sent
+    steps, sent = simulate([(0.0, start)], react, lambda item: rank[item[1][0]], GATHER_AHEAD)
+    return with_tasks(grouped(steps, gather_group)), sent
 
 
 def plan_scatter(sent):
@@ -179,8 +193,50 @@
                     if sign_of(q) == s:
                         seen[c, ("m3", o, q, s)] = 1
     last = max(sent.values())
-    steps, _ = simulate(first, react, lambda item: last - sent[item])
+    steps, _ = simulate(first, react, lambda item: last - sent[item], SCATTER_AHEAD)
     return grouped(steps + products, scatter_group)
+
+
+def with_tasks(steps):
+    free, came, out, waiting, arrived = {}, {}, [], [], {}
+    t, done = 0.0, 0
+    sends = sum(step[0] in ("send", "send0") for step in steps)
+    held = [(("ids",), 0.5)] + [(("rows", z), 0.15) for z in range(4)] + [(("choices",), 0.4)]
+    for step in steps:
+        kind, c, m = step
+        if kind != "receive":
+            if kind != "send1":
+                k = queue_of(c, m)
+                free[k] = max(t, free.get(k, 0.0)) + bytes_of(c, m) / RATE
+                key = (c, gather_group(m)[0])
+                came[key] = max(came.get(key, 0.0), free[k] + DELAY)
+                sends -= 1
+            out.append(step)
+            continue
+        if done >= 84:
+            waiting += held
+            held = []
+        while waiting and (sends == 0 or t + waiting[0][1] <= came[c, m] + SLACK):
+            task, cost = waiting.pop(0)
+            out.append(("task", task, None))
+            t += cost
+        t = max(t, came[c, m])
+        out.append(step)
+        size = gather_size(m)
+        done += size
+        k = 2 if m[0] == "f3" else (3 if m[-1] == 1 else 1) if m[0] == "m3" else 0
+        arrived[c, k] = arrived.get((c, k), 1 if k == 0 else 0) + size
+        if arrived[c, k] == 16:
+            held += [(("hidden", c, k), 0.25), (("pick", c, k), 0.3)]
+            if k == 2:
+                held.append((("columns", c), 0.5))
+    return out + [("task", task, None) for task, _ in waiting + held]
+
+
+def gather_size(name):
+    if name[0] == "f3":
+        return 16
+    return 8 if name[0] == "m3" and len(name) == 2 else 1
 
 
 def numbered(group):
@@ -300,6 +356,15 @@
     for peer in [*peers.values(), partner]:
         pl.semaphore_signal(barrier, inc=1, device_id=(peer,), device_id_type=MESH)
 
+    def send(action, copy):
+        if action == "send":
+            copy.start()
+            return
+
+        @pl.when(core == int(action[-1]))
+        def _():
+            copy.start()
+
     def await_bytes(ref, semaphore):
         pltpu.make_async_copy(ref, ref, semaphore).wait()
 
@@ -366,7 +431,10 @@
 
     for ref in (input_re, input_im, readout_re, readout_im):
         ref[...] = jnp.zeros((4, 128, 512), BF16)
-    loaded(0, 3)
+    loaded(0, 6)
+    pl.semaphore_wait(barrier, 10)
+    for copy in swaps[:7]:
+        copy.start()
     square = lax.broadcasted_iota(jnp.int32, (32, 32), 0) == lax.broadcasted_iota(
         jnp.int32, (32, 32), 1
     )
@@ -396,15 +464,10 @@
         decay_rows[pl.ds(0, 1), lane] = decay_re[g : g + 1]
         decay_rows[pl.ds(1, 1), lane] = decay_im[g : g + 1]
 
-    pl.semaphore_wait(barrier, 10)
-    for copy in swaps[:7]:
-        copy.start()
-
     def rms_scale(values, gain):
         mean = jnp.mean(values * values, axis=1, keepdims=True)
         return (values * lax.rsqrt(mean + EPS) * gain).astype(BF16)
 
-    loaded(3, 6)
     tokens = tokens_ref[...].astype(F32)
     drive = dot(rms_scale(tokens, norms_ref[0]), w_drive_ref[...]).astype(BF16)
     loaded(6, 8)
@@ -493,7 +556,7 @@
         )
 
     def gather_wait(colour, name):
-        size = {("f3",): 16}.get(name, 8 if len(name) == 2 and name[0] == "m3" else 1)
+        size = gather_size(name)
         cols = whole(colour)
         ref = {16: x.at[0, :, :, :, cols], 8: x.at[0, pl.ds(0, 2), :, :, cols]}.get(
             size, x.at[0, 0, 0, :, cols]
@@ -593,14 +656,19 @@
             taken = jnp.where(hit, 1.0, taken)
         tables["taken"] = taken
 
-    def use_slab(colour, k):
-        start, width = COLS[colour]
-        cols = pl.ds(start, width)
+    def slab_rows(colour, k):
+        return slab_of(x, ORDERS[colour][2], k, whole(colour)).reshape(256, COLS[colour][1])
+
+    def use_hidden(colour, k):
         d = ORDERS[colour][2]
-        values = slab_of(x, d, k, cols).reshape(256, width)
         every = pl.ds(0, 256)
-        total = slab_of(sums, d, k, every).reshape(256, 256) + dot_nt(values, w_in[:, cols])
+        total = slab_of(sums, d, k, every).reshape(256, 256)
+        total = total + dot_nt(slab_rows(colour, k), w_in[:, whole(colour)])
         slab_store(sums, d, k, every, total)
+
+    def use_pick(colour, k):
+        d = ORDERS[colour][2]
+        cols = whole(colour)
         lane = lax.broadcasted_iota(jnp.int32, (1, 256), 1)
         a, b, r = lane // 64, lax.rem(lane // 16, 4), lax.rem(lane, 16)
         i = near[d][k]
@@ -612,7 +680,7 @@
             sender = a * 16 + b * 4 + i
         number = (sender * 16 + r).astype(F32)
         hot = jnp.where(tables["code"] == number, 1.0, 0.0).astype(BF16)
-        rows = dot(hot, values)
+        rows = dot(hot, slab_rows(colour, k))
         if k == 0:
             picking[:, cols] = rows
         else:
@@ -641,46 +709,44 @@
     scatter_steps = plan_scatter(gather_sent)
     ids_send(0)
     done = 0
-    ready = []
-    arrived = {}
     tasks = [
         (6, lambda: (ids_receive(0), ids_send(1))),
         (40, lambda: (ids_receive(1), ids_send(2))),
-        (84, lambda: (ids_receive(2), read_ids(), weights_wait(0))),
-        (88, lambda: slots_by_rows(0)),
-        (92, lambda: slots_by_rows(1)),
-        (96, lambda: slots_by_rows(2)),
-        (100, lambda: slots_by_rows(3)),
-        (104, read_choices),
     ]
     more = swaps[7:]
     for action, c, m in gather_steps:
-        if action == "send":
-            gather_copy(c, m).start()
+        if action == "task":
+            name, *what = c
+            if name == "ids":
+                ids_receive(2)
+                read_ids()
+                weights_wait(0)
+            elif name == "rows":
+                slots_by_rows(*what)
+            elif name == "choices":
+                read_choices()
+            elif name == "hidden":
+                use_hidden(*what)
+            elif name == "pick":
+                use_pick(*what)
+            else:
+                if not experts_in:
+                    weights_wait(1)
+                    weights_wait(2)
+                use_columns(*what)
+            continue
+        if action != "receive":
+            send(action, gather_copy(c, m))
             continue
         while tasks and done >= tasks[0][0]:
             tasks.pop(0)[1]()
         if more and done >= 12 * (8 - len(more)):
             more.pop(0).start()
-        size = gather_wait(c, m)
-        done += size
-        k = 2 if m[0] == "f3" else (3 if m[-1] == 1 else 1) if m[0] == "m3" else 0
-        arrived[c, k] = arrived.get((c, k), 1 if k == 0 else 0) + size
-        if arrived[c, k] == 16:
-            ready.append((c, k))
-        while ready and done >= 88:
-            c, k = ready.pop(0)
-            if k == 2 and not experts_in:
-                weights_wait(1)
-                weights_wait(2)
-            use_slab(c, k)
-            if k == 2:
-                use_columns(c)
+        done += gather_wait(c, m)
     weights_wait(3)
 
 
-    @pl.loop(0, 4)
-    def _(zi):
+    for zi in range(4):
         products = sums[zi].reshape(256, 256)
         words = jnp.broadcast_to(ids_all[zi], (4, 4, 16, 128)).reshape(256, 128)
         lane = lax.broadcasted_iota(jnp.int32, (256, 128), 1)
@@ -778,8 +844,8 @@
             product(*what)
             continue
         c, m = what
-        if action == "send":
-            scatter_copy(c, m).start()
+        if action != "receive":
+            send(action, scatter_copy(c, m))
             continue
         done += 1
         scatter_wait(c, m)
@@ -814,6 +880,31 @@
         for i in range(3):
             await_bytes(sent[i], ag_send.at[c, i])
             await_bytes(sent[i], rs_send.at[c, i])
+
+
+def finish_kernel(rows_ref, state_ref, rows_out, state_out, sem):
+    copies = (
+        pltpu.make_async_copy(rows_ref, rows_out, sem.at[0]),
+        pltpu.make_async_copy(state_ref, state_out, sem.at[1]),
+    )
+    for copy in copies:
+        copy.start()
+    for copy in copies:
+        copy.wait()
+
+
+def finish(rows, state):
+    return pl.pallas_call(
+        finish_kernel,
+        out_shape=(
+            jax.ShapeDtypeStruct(rows.shape, rows.dtype),
+            jax.ShapeDtypeStruct(state.shape, state.dtype),
+        ),
+        in_specs=[pl.BlockSpec(memory_space=pltpu.VMEM)] * 2,
+        out_specs=[pl.BlockSpec(memory_space=pl.ANY)] * 2,
+        scratch_shapes=[pltpu.SemaphoreType.DMA((2,))],
+        compiler_params=pltpu.CompilerParams(vmem_limit_bytes=4 * 1024 * 1024),
+    )(rows, state)
 
 
 def on_device(
@@ -846,7 +937,7 @@
 ):
     vmem = pl.BlockSpec(memory_space=pltpu.VMEM)
     hbm = pl.BlockSpec(memory_space=pltpu.HBM)
-    return pl.pallas_call(
+    rows, new_state = pl.pallas_call(
         layer_kernel,
         out_shape=(
             jax.ShapeDtypeStruct((16, 2048), BF16),
@@ -936,6 +1027,7 @@
         expert_up[0],
         expert_down[0],
     )])
+    return finish(rows, new_state)
 
 
 def solution(mesh):

time: 64.6 us -> 60 us (0.929)
  Pallas kernels: 62.4 us -> 59 us
  local copies, waits for them, and re-layouts: 1.33 us -> 0 us
    pallas_call x1, Pallas kernels: 62.4 us -> 58.2 us  [on_device(): pl.pallas_call(layer_kernel, out_shape=(jax.ShapeDtypeStruct((16, 2048),...]
    unnamed x2 -> x0, local copies, waits for them, and re-layouts: 1.33 us -> none
    pallas_call x0 -> x1, Pallas kernels: none -> 0.74 us  [finish(): pl.pallas_call(finish_kernel, out_shape=(jax.ShapeDtypeStruct(rows.shape,...]
where the time goes in v5:
time: 60 us; the launch traced here: 59.8 us
  Pallas kernels  59 us (98%)
  between operations  0.81 us (1%)
    pallas_call x1, Pallas kernels, on_device(): pl.pallas_call(layer_kernel, out_shape=(jax.ShapeDtypeStruct((16, 2048),...  58.2 us

profile of v5, /device:TPU:0, one launch (start us, length us, event | category | flops | bytes accessed | tf_op | source)
XLA Modules:
  0.0 59.8 jit_solution(11385395534618841991)
XLA Ops:
  0.6 58.2 %shard_map.257 = (bf16[16,2048]{1,0:T(8,128)(2,1)S(1)}, f32[2,16,2048]{2,1,0:T(8,128)S(1)}) custom-call(bf16[16,2048]{1,0:T(8,128)(2,1)} %tokens_hbm.1, f32[2,16,2048]{2,1,0:T(8,128)} %state_hbm.1, f32[1,2048]{1,0:T(1,128)} %bitcast.22, bf16[2048,512]{1,0:T(8,128)(2,1)} %w_drive_hbm.1, f32[32,64]{1,0:T(8,128)} %lam_real_hbm.1, f32[32,64]{1,0:T(8,128)} %lam_imag_hbm.1, ...), custom_call_target="tpu_custom_call" | custom-call | flops 8000000000 | bytes 20000000 | tf_op jit(solution)/shard_map/pallas_call | solution.py:940
  58.9 0.7 %shard_map.258 = (bf16[16,2048]{1,0:T(8,128)(2,1)}, f32[2,16,2048]{2,1,0:T(8,128)}) custom-call(bf16[16,2048]{1,0:T(8,128)(2,1)S(1)} %get-tuple-element.4.rows_ref, f32[2,16,2048]{2,1,0:T(8,128)S(1)} %get-tuple-element.5.state_ref), custom_call_target="tpu_custom_call" | custom-call | tf_op jit(solution)/shard_map/pallas_call | solution.py:897

commit v6 on v5

--- a/solution.py
+++ b/solution.py
@@ -201,7 +201,7 @@
     free, came, out, waiting, arrived = {}, {}, [], [], {}
     t, done = 0.0, 0
     sends = sum(step[0] in ("send", "send0") for step in steps)
-    held = [(("ids",), 0.5)] + [(("rows", z), 0.15) for z in range(4)] + [(("choices",), 0.4)]
+    held = [(("ids",), 0.3)] + [(("rows", z), 0.1) for z in range(4)]
     for step in steps:
         kind, c, m = step
         if kind != "receive":
@@ -227,9 +227,10 @@
         k = 2 if m[0] == "f3" else (3 if m[-1] == 1 else 1) if m[0] == "m3" else 0
         arrived[c, k] = arrived.get((c, k), 1 if k == 0 else 0) + size
         if arrived[c, k] == 16:
-            held += [(("hidden", c, k), 0.25), (("pick", c, k), 0.3)]
+            waiting.append((("hidden", c, k), 0.3))
+            held.append((("pick", c, k), 0.3))
             if k == 2:
-                held.append((("columns", c), 0.5))
+                held.append((("columns", c), 0.8))
     return out + [("task", task, None) for task, _ in waiting + held]
 
 
@@ -320,7 +321,7 @@
     sums,
     hc,
     picking,
-    group_rows,
+    w_turned,
     p,
     r1,
     r2,
@@ -499,33 +500,55 @@
 
     own[...] = normed
 
-    ids = ids_ref[...].astype(F32)
-    lanes = lax.broadcasted_iota(jnp.int32, (16, 128), 1)
-    down = lax.broadcasted_iota(jnp.int32, (16, 128), 0)
-    this = lax.broadcasted_iota(jnp.int32, (16, 16), 0)
-    that = lax.broadcasted_iota(jnp.int32, (16, 16), 1)
-    columns = [
-        jnp.sum(jnp.where(this == that, ids[t : t + 1], 0.0), axis=1, keepdims=True)
-        for t in range(6)
-    ]
-    chosen = jnp.zeros((16, 128), F32)
-    for column in columns:
-        chosen = chosen + jnp.where(column == lanes.astype(F32), 1.0, 0.0)
-    earlier = jnp.where(that < this, 1.0, 0.0)
-    ordinal = dot(earlier.astype(BF16), chosen.astype(BF16))
-    branch = jax.nn.sigmoid(
-        jnp.sum(normed.astype(F32) * norms_ref[2], axis=1, keepdims=True)
-    )
-    words = jnp.where(lanes == 96 + down, branch, 0.0)
-    for t, column in enumerate(columns):
-        rank = jnp.sum(
-            jnp.where(column == lanes.astype(F32), ordinal, 0.0), axis=1, keepdims=True
+    x[pos["z"], pos["y"], pos["x"]] = normed
+
+    def write_words():
+        normed = own[...]
+        ids = ids_ref[...].astype(F32)
+        lanes = lax.broadcasted_iota(jnp.int32, (16, 128), 1)
+        down = lax.broadcasted_iota(jnp.int32, (16, 128), 0)
+        this = lax.broadcasted_iota(jnp.int32, (16, 16), 0)
+        that = lax.broadcasted_iota(jnp.int32, (16, 16), 1)
+        hits = []
+        columns = []
+        for t in range(6):
+            column = jnp.sum(jnp.where(this == that, ids[t : t + 1], 0.0), axis=1, keepdims=True)
+            columns.append(column)
+            hits.append(column == lanes.astype(F32))
+        chosen = jnp.zeros((16, 128), F32)
+        for hit in hits:
+            chosen = chosen + jnp.where(hit, 1.0, 0.0)
+        earlier = jnp.where(that < this, 1.0, 0.0)
+        ordinal = dot(earlier.astype(BF16), chosen.astype(BF16))
+        branch = jax.nn.sigmoid(
+            jnp.sum(normed.astype(F32) * norms_ref[2], axis=1, keepdims=True)
         )
-        words = words + jnp.where(lanes == 16 * t + down, column + 128.0 * rank, 0.0)
-    words = jnp.sum(words, axis=0, keepdims=True)
-    ids_own[...] = words
-    ids_all[pos["z"], pos["y"], pos["x"]] = words
-    x[pos["z"], pos["y"], pos["x"]] = normed
+        group_exp = jnp.exp(dot_nt(normed, group_ref[...]))
+        group_prob = group_exp / jnp.sum(group_exp, axis=1, keepdims=True)
+        inner_exp = jnp.exp(dot(normed, router_ref[...]))
+        inner_sum = jnp.zeros((16, 128), F32)
+        outer = jnp.zeros((16, 128), F32)
+        for g in range(4):
+            inside = lanes // 32 == g
+            total = jnp.sum(jnp.where(inside, inner_exp, 0.0), axis=1, keepdims=True)
+            inner_sum = jnp.where(inside, total, inner_sum)
+            outer = jnp.where(inside, group_prob[:, g : g + 1], outer)
+        inner = inner_exp / inner_sum
+        joint = outer * inner
+        divisor = jnp.sum(jnp.where(chosen > 0.0, inner, 0.0), axis=1, keepdims=True)
+        words = jnp.where(lanes == 96 + down, branch, 0.0)
+        gates = jnp.zeros((16, 128), F32)
+        for t in range(6):
+            place = lanes == 16 * t + down
+            rank = jnp.sum(jnp.where(hits[t], ordinal, 0.0), axis=1, keepdims=True)
+            gate = jnp.sum(jnp.where(hits[t], joint, 0.0), axis=1, keepdims=True) / divisor
+            words = words + jnp.where(place, columns[t] + 128.0 * rank, 0.0)
+            gates = gates + jnp.where(place, gate, 0.0)
+        words = jnp.sum(words, axis=0, keepdims=True)
+        gates = jnp.sum(gates, axis=0, keepdims=True)
+        for ref in (ids_own, ids_all.at[pos["z"], pos["y"], pos["x"]]):
+            ref[pl.ds(0, 1), :] = words
+            ref[pl.ds(1, 1), :] = gates
 
     def view(ref, colour, offsets, cols):
         at = {}
@@ -609,18 +632,21 @@
     tables = {}
 
     def read_ids():
-        table = ids_all[...].reshape(64, 128)
+        table = ids_all[:, :, :, pl.ds(0, 1), :].reshape(64, 128)
+        all_gates = ids_all[:, :, :, pl.ds(1, 1), :].reshape(64, 128)
         lane = lax.broadcasted_iota(jnp.int32, (64, 128), 1)
         sender = lax.broadcasted_iota(jnp.int32, (64, 128), 0)
-        found = []
+        found, gates = [], []
         for e in range(2):
             for k in range(2):
                 wanted = (first + e + 128 * k).astype(F32)
                 hit = (table == wanted) & (lane < 96)
                 row = jnp.where(hit, lax.rem(lane, 16) + 16 * sender, -1)
                 found.append(jnp.max(row.astype(F32), axis=1, keepdims=True))
+                gates.append(jnp.sum(jnp.where(hit, all_gates, 0.0), axis=1, keepdims=True))
         code = jnp.concatenate(found, axis=0)
         tables["code"] = code
+        tables["gates"] = jnp.concatenate(gates, axis=0)
         wide = jnp.broadcast_to(code, (256, 256))
         diagonal = lax.broadcasted_iota(jnp.int32, (256, 256), 0) == lax.broadcasted_iota(
             jnp.int32, (256, 256), 1
@@ -633,29 +659,6 @@
         hot = jnp.where(number.astype(F32) == tables["across"], 1.0, 0.0).astype(BF16)
         hc[z, :, :, :, pl.ds(128, 256)] = hot.reshape(4, 4, 16, 256)
 
-    def read_choices():
-        code = tables["code"]
-        table = ids_all[...].reshape(64, 128)
-        lane = lax.broadcasted_iota(jnp.int32, (64, 128), 1)
-        slot = lax.broadcasted_iota(jnp.int32, (256, 64), 0)
-        same = lax.rem(slot, 64) == lax.broadcasted_iota(jnp.int32, (256, 64), 1)
-        choices = dot(
-            jnp.where(same, 1.0, 0.0).astype(BF16), jnp.where(lane < 96, table, 0.0).astype(BF16)
-        )
-        lane = lax.broadcasted_iota(jnp.int32, (256, 128), 1)
-        within = code - 16.0 * lax.rem(
-            lax.broadcasted_iota(jnp.int32, (256, 1), 0), 64
-        ).astype(F32)
-        taken = jnp.zeros((256, 128), F32)
-        for t in range(6):
-            word = jnp.sum(
-                jnp.where(lane.astype(F32) == within + 16.0 * t, choices, 0.0), axis=1, keepdims=True
-            )
-            expert = jnp.where(word >= 128.0, word - 128.0, word)
-            hit = (expert == lane.astype(F32)) & (code >= 0.0)
-            taken = jnp.where(hit, 1.0, taken)
-        tables["taken"] = taken
-
     def slab_rows(colour, k):
         return slab_of(x, ORDERS[colour][2], k, whole(colour)).reshape(256, COLS[colour][1])
 
@@ -663,7 +666,7 @@
         d = ORDERS[colour][2]
         every = pl.ds(0, 256)
         total = slab_of(sums, d, k, every).reshape(256, 256)
-        total = total + dot_nt(slab_rows(colour, k), w_in[:, whole(colour)])
+        total = total + dot(slab_rows(colour, k), w_turned[whole(colour), :])
         slab_store(sums, d, k, every, total)
 
     def use_pick(colour, k):
@@ -686,19 +689,21 @@
         else:
             picking[:, cols] += rows
 
-    for g in range(4):
-        group_rows[pl.ds(32 * g, 32), :] = jnp.broadcast_to(
-            group_ref[pl.ds(g, 1), :].astype(F32), (32, 2048)
-        ).astype(BF16)
     sums[...] = jnp.zeros((4, 4, 4, 16, 256), F32)
 
     experts_in = {}
+
+    def turn_weights():
+        weights_wait(0)
+        for i in range(8):
+            part = pl.ds(256 * i, 256)
+            w_turned[part, :] = w_in[:, part].T
 
     def use_columns(colour):
         start, width = COLS[colour]
         cols = pl.ds(start, width)
         rows = picking[:, cols].astype(BF16)
-        parts = [dot_nt(rows, group_rows[:, cols]), dot(rows, router_ref[cols, :])]
+        parts = []
         for e in range(2):
             mine = rows[e * 128 : (e + 1) * 128]
             parts += [dot(mine, eg[e, cols, :]), dot(mine, eu[e, cols, :])]
@@ -707,11 +712,12 @@
 
     gather_steps, gather_sent = plan_gather()
     scatter_steps = plan_scatter(gather_sent)
-    ids_send(0)
     done = 0
     tasks = [
-        (6, lambda: (ids_receive(0), ids_send(1))),
-        (40, lambda: (ids_receive(1), ids_send(2))),
+        (0, lambda: (write_words(), ids_send(0))),
+        (14, lambda: (ids_receive(0), ids_send(1))),
+        (24, turn_weights),
+        (44, lambda: (ids_receive(1), ids_send(2))),
     ]
     more = swaps[7:]
     for action, c, m in gather_steps:
@@ -720,11 +726,8 @@
             if name == "ids":
                 ids_receive(2)
                 read_ids()
-                weights_wait(0)
             elif name == "rows":
                 slots_by_rows(*what)
-            elif name == "choices":
-                read_choices()
             elif name == "hidden":
                 use_hidden(*what)
             elif name == "pick":
@@ -748,7 +751,7 @@
 
     for zi in range(4):
         products = sums[zi].reshape(256, 256)
-        words = jnp.broadcast_to(ids_all[zi], (4, 4, 16, 128)).reshape(256, 128)
+        words = jnp.broadcast_to(ids_all[zi, :, :, pl.ds(0, 1), :], (4, 4, 16, 128)).reshape(256, 128)
         lane = lax.broadcasted_iota(jnp.int32, (256, 128), 1)
         row = lax.broadcasted_iota(jnp.int32, (256, 128), 0)
         own_word = lane == 96 + lax.rem(row, 16)
@@ -756,28 +759,10 @@
         hidden = (scale * jax.nn.silu(products[:, :128]) * products[:, 128:]).astype(BF16)
         hc[zi, :, :, :, pl.ds(0, 128)] = hidden.reshape(4, 4, 16, 128)
 
-    group_exp = jnp.exp(experts_in[0])
-    inner_exp = jnp.exp(experts_in[1])
-    lane = lax.broadcasted_iota(jnp.int32, (256, 128), 1)
-    row = lax.broadcasted_iota(jnp.int32, (256, 128), 0)
-    group_sum = jnp.sum(jnp.where(lax.rem(lane, 32) == 0, group_exp, 0.0), axis=1, keepdims=True)
-    inner_sum = jnp.zeros((256, 128), F32)
-    for g in range(4):
-        inside = lane // 32 == g
-        total = jnp.sum(jnp.where(inside, inner_exp, 0.0), axis=1, keepdims=True)
-        inner_sum = jnp.where(inside, total, inner_sum)
-    inner = inner_exp / inner_sum
-    joint = (group_exp / group_sum) * inner
-    mine = lane == first + row // 128
-    numerator = jnp.sum(jnp.where(mine, joint, 0.0), axis=1, keepdims=True)
-    denominator = jnp.sum(tables["taken"] * inner, axis=1, keepdims=True)
-    live = tables["code"] >= 0.0
-    gates = jnp.where(live, numerator / jnp.where(live, denominator, 1.0), 0.0)
-
     for e in range(2):
-        hidden = (jax.nn.silu(experts_in[2 + 2 * e]) * experts_in[3 + 2 * e]).astype(BF16)
+        hidden = (jax.nn.silu(experts_in[2 * e]) * experts_in[2 * e + 1]).astype(BF16)
         result = dot(hidden, ed[e])
-        weighted = result * gates[e * 128 : (e + 1) * 128]
+        weighted = result * tables["gates"][e * 128 : (e + 1) * 128]
         w_out[pl.ds(128 + e * 128, 128), :] = weighted.astype(BF16)
 
     def landing(colour, m):
@@ -972,12 +957,12 @@
             pltpu.VMEM((2, 2048, 512), BF16),
             pltpu.VMEM((2, 2048, 512), BF16),
             pltpu.VMEM((2, 512, 2048), BF16),
-            pltpu.VMEM((4, 4, 4, 1, 128), F32),
-            pltpu.VMEM((1, 128), F32),
+            pltpu.VMEM((4, 4, 4, 2, 128), F32),
+            pltpu.VMEM((2, 128), F32),
             pltpu.VMEM((4, 4, 4, 16, 256), F32),
             pltpu.VMEM((4, 4, 4, 16, 384), BF16),
             pltpu.VMEM((256, 2048), F32),
-            pltpu.VMEM((128, 2048), BF16),
+            pltpu.VMEM((2048, 256), BF16),
             pltpu.VMEM((4, 4, 4, 16, 2048), BF16),
             pltpu.VMEM((3, 3, 16, 768), BF16),
             pltpu.VMEM((3, 3, 4, 16, 768), BF16),

time: 60 us -> 59.6 us (level)
  no operation moved by 1% of the time
where the time goes in v6:
time: 59.6 us; the launch traced here: 59.4 us
  Pallas kernels  58.6 us (98%)
  between operations  0.81 us (1%)
    pallas_call x1, Pallas kernels, on_device(): pl.pallas_call(layer_kernel, out_shape=(jax.ShapeDtypeStruct((16, 2048),...  57.9 us

profile of v6, /device:TPU:0, one launch (start us, length us, event | category | flops | bytes accessed | tf_op | source)
XLA Modules:
  0.0 59.4 jit_solution(7792340057862776485)
XLA Ops:
  0.6 57.9 %shard_map.257 = (bf16[16,2048]{1,0:T(8,128)(2,1)S(1)}, f32[2,16,2048]{2,1,0:T(8,128)S(1)}) custom-call(bf16[16,2048]{1,0:T(8,128)(2,1)} %tokens_hbm.1, f32[2,16,2048]{2,1,0:T(8,128)} %state_hbm.1, f32[1,2048]{1,0:T(1,128)} %bitcast.22, bf16[2048,512]{1,0:T(8,128)(2,1)} %w_drive_hbm.1, f32[32,64]{1,0:T(8,128)} %lam_real_hbm.1, f32[32,64]{1,0:T(8,128)} %lam_imag_hbm.1, ...), custom_call_target="tpu_custom_call" | custom-call | flops 8000000000 | bytes 20000000 | tf_op jit(solution)/shard_map/pallas_call | solution.py:925
  58.5 0.7 %shard_map.258 = (bf16[16,2048]{1,0:T(8,128)(2,1)}, f32[2,16,2048]{2,1,0:T(8,128)}) custom-call(bf16[16,2048]{1,0:T(8,128)(2,1)S(1)} %get-tuple-element.4.rows_ref, f32[2,16,2048]{2,1,0:T(8,128)S(1)} %get-tuple-element.5.state_ref), custom_call_target="tpu_custom_call" | custom-call | tf_op jit(solution)/shard_map/pallas_call | solution.py:882

commit v7 on v6

--- a/solution.py
+++ b/solution.py
@@ -179,19 +179,20 @@
 
     first, products, t = [], [], 0.0
     pairs = [(o, q) for o in range(4) for q in range(4)]
-    for k in (2, 3, 1, 0):
+    for ks in ((2,), (3, 1), (0,)):
         for c in range(3):
-            products.append((t, 0, "product", (c, k)))
-            t += STEP
-            if k == 2:
+            products.append((t, 0, "product", (c, ks)))
+            t += STEP * (0.5 + 0.5 * len(ks))
+            if ks == (2,):
                 first.append((t, [(c, ("f3", o, q)) for o, q in pairs]))
-            elif k in (1, 3):
-                s = -1 if k == 1 else 1
-                free = [(c, ("m3", o, q, s)) for o, q in pairs if sign_of(q) != s]
-                first.append((t, free))
-                for o, q in pairs:
-                    if sign_of(q) == s:
-                        seen[c, ("m3", o, q, s)] = 1
+            for k in (1, 3):
+                if k in ks:
+                    s = -1 if k == 1 else 1
+                    free = [(c, ("m3", o, q, s)) for o, q in pairs if sign_of(q) != s]
+                    first.append((t, free))
+                    for o, q in pairs:
+                        if sign_of(q) == s:
+                            seen[c, ("m3", o, q, s)] = 1
     last = max(sent.values())
     steps, _ = simulate(first, react, lambda item: last - sent[item], SCATTER_AHEAD)
     return grouped(steps + products, scatter_group)
@@ -226,9 +227,10 @@
         done += size
         k = 2 if m[0] == "f3" else (3 if m[-1] == 1 else 1) if m[0] == "m3" else 0
         arrived[c, k] = arrived.get((c, k), 1 if k == 0 else 0) + size
-        if arrived[c, k] == 16:
-            waiting.append((("hidden", c, k), 0.3))
-            held.append((("pick", c, k), 0.3))
+        if arrived[c, k] == 16 and (k in (0, 2) or arrived.get((c, 4 - k)) == 16):
+            both = (1, 3) if k in (1, 3) else (k,)
+            waiting.append((("hidden", c, both), 0.3 * len(both)))
+            held.append((("pick", c, both), 0.3 * len(both)))
             if k == 2:
                 held.append((("columns", c), 0.8))
     return out + [("task", task, None) for task, _ in waiting + held]
@@ -249,8 +251,31 @@
     return {name: i for i, name in enumerate(names)}
 
 
-GATHER_SLOT = numbered(gather_group)
-SCATTER_SLOT = numbered(scatter_group)
+def receive_slots(steps):
+    names = [(c, name) for c in range(3) for name in numbered(gather_group)]
+    gather = {key: i for i, key in enumerate(names)}
+    last = {}
+    for at, (kind, c, m) in enumerate(steps):
+        if kind.startswith("send") and link_of(c, m)[1] != 2:
+            for core in (0, 1):
+                if kind in ("send", "send%d" % core):
+                    last[core, link_of(c, m)] = at
+    early = steps[: min(last.values())]
+    free = [gather[step[1:]] for step in early if step[0] == "receive"]
+    scatter, count = {}, len(gather)
+    for c in range(3):
+        for name in numbered(scatter_group):
+            if free and name[0] != "m1":
+                scatter[c, name] = free.pop()
+            else:
+                scatter[c, name] = count
+                count += 1
+    return gather, scatter, count
+
+
+GATHER_STEPS, GATHER_SENT = plan_gather()
+SCATTER_STEPS = plan_scatter(GATHER_SENT)
+GATHER_SLOT, SCATTER_SLOT, RECEIVE_SLOTS = receive_slots(GATHER_STEPS)
 
 
 def dot(a, b):
@@ -333,9 +358,8 @@
     id_send,
     id_recv,
     ag_send,
-    ag_recv,
     rs_send,
-    rs_recv,
+    receive_sem,
 ):
     me = lax.axis_index("ep")
     core = lax.rem(me, 2)
@@ -432,10 +456,7 @@
 
     for ref in (input_re, input_im, readout_re, readout_im):
         ref[...] = jnp.zeros((4, 128, 512), BF16)
-    loaded(0, 6)
-    pl.semaphore_wait(barrier, 10)
-    for copy in swaps[:7]:
-        copy.start()
+    loaded(0, 3)
     square = lax.broadcasted_iota(jnp.int32, (32, 32), 0) == lax.broadcasted_iota(
         jnp.int32, (32, 32), 1
     )
@@ -465,10 +486,16 @@
         decay_rows[pl.ds(0, 1), lane] = decay_re[g : g + 1]
         decay_rows[pl.ds(1, 1), lane] = decay_im[g : g + 1]
 
+    pl.semaphore_wait(barrier, 10)
+    for copy in swaps[:7]:
+        copy.start()
+
+
     def rms_scale(values, gain):
         mean = jnp.mean(values * values, axis=1, keepdims=True)
         return (values * lax.rsqrt(mean + EPS) * gain).astype(BF16)
 
+    loaded(3, 6)
     tokens = tokens_ref[...].astype(F32)
     drive = dot(rms_scale(tokens, norms_ref[0]), w_drive_ref[...]).astype(BF16)
     loaded(6, 8)
@@ -503,6 +530,7 @@
     x[pos["z"], pos["y"], pos["x"]] = normed
 
     def write_words():
+        sums[...] = jnp.zeros((4, 4, 4, 16, 256), F32)
         normed = own[...]
         ids = ids_ref[...].astype(F32)
         lanes = lax.broadcasted_iota(jnp.int32, (16, 128), 1)
@@ -573,7 +601,7 @@
             src_ref=own.at[:, whole(colour)] if where == (0, 0, 0) else target,
             dst_ref=target,
             send_sem=ag_send.at[colour, int(m[0][1]) - 1],
-            recv_sem=ag_recv.at[colour, GATHER_SLOT[gather_group(m)[0]]],
+            recv_sem=receive_sem.at[GATHER_SLOT[colour, gather_group(m)[0]]],
             device_id=(peers[d, s],),
             device_id_type=MESH,
         )
@@ -584,7 +612,7 @@
         ref = {16: x.at[0, :, :, :, cols], 8: x.at[0, pl.ds(0, 2), :, :, cols]}.get(
             size, x.at[0, 0, 0, :, cols]
         )
-        await_bytes(ref, ag_recv.at[colour, GATHER_SLOT[name]])
+        await_bytes(ref, receive_sem.at[GATHER_SLOT[colour, name]])
         return size
 
     def ids_send(level):
@@ -659,37 +687,42 @@
         hot = jnp.where(number.astype(F32) == tables["across"], 1.0, 0.0).astype(BF16)
         hc[z, :, :, :, pl.ds(128, 256)] = hot.reshape(4, 4, 16, 256)
 
-    def slab_rows(colour, k):
-        return slab_of(x, ORDERS[colour][2], k, whole(colour)).reshape(256, COLS[colour][1])
-
-    def use_hidden(colour, k):
+    def slab_rows(colour, ks):
+        d, cols = ORDERS[colour][2], whole(colour)
+        slabs = [slab_of(x, d, k, cols).reshape(256, COLS[colour][1]) for k in ks]
+        return jnp.concatenate(slabs, axis=0) if len(slabs) > 1 else slabs[0]
+
+    def use_hidden(colour, ks):
         d = ORDERS[colour][2]
         every = pl.ds(0, 256)
-        total = slab_of(sums, d, k, every).reshape(256, 256)
-        total = total + dot(slab_rows(colour, k), w_turned[whole(colour), :])
-        slab_store(sums, d, k, every, total)
-
-    def use_pick(colour, k):
+        products = dot(slab_rows(colour, ks), w_turned[whole(colour), :])
+        for i, k in enumerate(ks):
+            total = slab_of(sums, d, k, every).reshape(256, 256)
+            slab_store(sums, d, k, every, total + products[256 * i : 256 * i + 256])
+
+    def use_pick(colour, ks):
         d = ORDERS[colour][2]
         cols = whole(colour)
         lane = lax.broadcasted_iota(jnp.int32, (1, 256), 1)
         a, b, r = lane // 64, lax.rem(lane // 16, 4), lax.rem(lane, 16)
-        i = near[d][k]
-        if d == "z":
-            sender = i * 16 + a * 4 + b
-        elif d == "y":
-            sender = a * 16 + i * 4 + b
-        else:
-            sender = a * 16 + b * 4 + i
-        number = (sender * 16 + r).astype(F32)
-        hot = jnp.where(tables["code"] == number, 1.0, 0.0).astype(BF16)
-        rows = dot(hot, slab_rows(colour, k))
-        if k == 0:
+        hots = []
+        for k in ks:
+            i = near[d][k]
+            if d == "z":
+                sender = i * 16 + a * 4 + b
+            elif d == "y":
+                sender = a * 16 + i * 4 + b
+            else:
+                sender = a * 16 + b * 4 + i
+            number = (sender * 16 + r).astype(F32)
+            hots.append(jnp.where(tables["code"] == number, 1.0, 0.0).astype(BF16))
+        hot = jnp.concatenate(hots, axis=1) if len(hots) > 1 else hots[0]
+        rows = dot(hot, slab_rows(colour, ks))
+        if ks == (0,):
             picking[:, cols] = rows
         else:
             picking[:, cols] += rows
 
-    sums[...] = jnp.zeros((4, 4, 4, 16, 256), F32)
 
     experts_in = {}
 
@@ -710,8 +743,6 @@
         for i, part in enumerate(parts):
             experts_in[i] = experts_in[i] + part if i in experts_in else part
 
-    gather_steps, gather_sent = plan_gather()
-    scatter_steps = plan_scatter(gather_sent)
     done = 0
     tasks = [
         (0, lambda: (write_words(), ids_send(0))),
@@ -720,7 +751,7 @@
         (44, lambda: (ids_receive(1), ids_send(2))),
     ]
     more = swaps[7:]
-    for action, c, m in gather_steps:
+    for action, c, m in GATHER_STEPS:
         if action == "task":
             name, *what = c
             if name == "ids":
@@ -791,7 +822,7 @@
             src_ref=view(p, colour, where, whole(colour)),
             dst_ref=landing(colour, m),
             send_sem=rs_send.at[colour, int(m[0][1]) - 1],
-            recv_sem=rs_recv.at[colour, SCATTER_SLOT[scatter_group(m)[0]]],
+            recv_sem=receive_sem.at[SCATTER_SLOT[colour, scatter_group(m)[0]]],
             device_id=(peers[d, s if s == 2 else -s],),
             device_id_type=MESH,
         )
@@ -807,14 +838,15 @@
             ref = r3.at[colour, two, name[1], name[2], :, cols]
         else:
             ref = landing(colour, name)
-        await_bytes(ref, rs_recv.at[colour, SCATTER_SLOT[name]])
-
-    def product(colour, k):
-        start, width = COLS[colour]
-        cols = pl.ds(start, width)
-        d = ORDERS[colour][2]
-        left = slab_of(hc, d, k, pl.ds(0, 384)).reshape(256, 384)
-        slab_store(p, d, k, cols, dot(left, w_out[:, cols]).astype(BF16))
+        await_bytes(ref, receive_sem.at[SCATTER_SLOT[colour, name]])
+
+    def product(colour, ks):
+        d, cols = ORDERS[colour][2], whole(colour)
+        left = [slab_of(hc, d, k, pl.ds(0, 384)).reshape(256, 384) for k in ks]
+        left = jnp.concatenate(left, axis=0) if len(left) > 1 else left[0]
+        values = dot(left, w_out[:, cols]).astype(BF16)
+        for i, k in enumerate(ks):
+            slab_store(p, d, k, cols, values[256 * i : 256 * i + 256])
 
     def add(colour, where, *messages):
         ref = view(p, colour, where, whole(colour))
@@ -824,7 +856,7 @@
         ref[...] = total.astype(BF16)
 
     done = 0
-    for action, *what in scatter_steps:
+    for action, *what in SCATTER_STEPS:
         if action == "product":
             product(*what)
             continue
@@ -974,9 +1006,8 @@
             pltpu.SemaphoreType.DMA((3,)),
             pltpu.SemaphoreType.DMA((3,)),
             pltpu.SemaphoreType.DMA((3, 3)),
-            pltpu.SemaphoreType.DMA((3, len(GATHER_SLOT))),
             pltpu.SemaphoreType.DMA((3, 3)),
-            pltpu.SemaphoreType.DMA((3, len(SCATTER_SLOT))),
+            pltpu.SemaphoreType.DMA((RECEIVE_SLOTS,)),
         ],
         compiler_params=pltpu.CompilerParams(
             collective_id=0, has_side_effects=True, vmem_limit_bytes=47 * 1024 * 1024

time: 59.6 us -> 57.5 us (0.965)
  Pallas kernels: 58.6 us -> 56.5 us
    pallas_call x1, Pallas kernels: 57.9 us -> 55.8 us  [on_device(): pl.pallas_call(layer_kernel, out_shape=(jax.ShapeDtypeStruct((16, 2048),...]
where the time goes in v7:
time: 57.5 us; the launch traced here: 57.3 us
  Pallas kernels  56.5 us (98%)
  between operations  0.81 us (1%)
    pallas_call x1, Pallas kernels, on_device(): pl.pallas_call(layer_kernel, out_shape=(jax.ShapeDtypeStruct((16, 2048),...  55.8 us

profile of v7, /device:TPU:0, one launch (start us, length us, event | category | flops | bytes accessed | tf_op | source)
XLA Modules:
  0.0 57.3 jit_solution(14242542716701775118)
XLA Ops:
  0.6 55.8 %shard_map.257 = (bf16[16,2048]{1,0:T(8,128)(2,1)S(1)}, f32[2,16,2048]{2,1,0:T(8,128)S(1)}) custom-call(bf16[16,2048]{1,0:T(8,128)(2,1)} %tokens_hbm.1, f32[2,16,2048]{2,1,0:T(8,128)} %state_hbm.1, f32[1,2048]{1,0:T(1,128)} %bitcast.22, bf16[2048,512]{1,0:T(8,128)(2,1)} %w_drive_hbm.1, f32[32,64]{1,0:T(8,128)} %lam_real_hbm.1, f32[32,64]{1,0:T(8,128)} %lam_imag_hbm.1, ...), custom_call_target="tpu_custom_call" | custom-call | flops 8000000000 | bytes 20000000 | tf_op jit(solution)/shard_map/pallas_call | solution.py:957
  56.4 0.7 %shard_map.258 = (bf16[16,2048]{1,0:T(8,128)(2,1)}, f32[2,16,2048]{2,1,0:T(8,128)}) custom-call(bf16[16,2048]{1,0:T(8,128)(2,1)S(1)} %get-tuple-element.4.rows_ref, f32[2,16,2048]{2,1,0:T(8,128)S(1)} %get-tuple-element.5.state_ref), custom_call_target="tpu_custom_call" | custom-call | tf_op jit(solution)/shard_map/pallas_call | solution.py:914

commit v8 on v7

--- a/solution.py
+++ b/solution.py
@@ -260,16 +260,25 @@
             for core in (0, 1):
                 if kind in ("send", "send%d" % core):
                     last[core, link_of(c, m)] = at
-    early = steps[: min(last.values())]
-    free = [gather[step[1:]] for step in early if step[0] == "receive"]
-    scatter, count = {}, len(gather)
+    waited = [(at, gather[step[1:]]) for at, step in enumerate(steps) if step[0] == "receive"]
+    limits = []
     for c in range(3):
         for name in numbered(scatter_group):
-            if free and name[0] != "m1":
-                scatter[c, name] = free.pop()
-            else:
-                scatter[c, name] = count
-                count += 1
+            if name[0] == "m1":
+                limits.append((-1, c, name))
+                continue
+            d = ORDERS[c][int(name[0][1]) - 1]
+            ways = (sign_of(name[-1]),) if name[0] in ("f2", "f3") else (1, -1)
+            limits.append((min(last[core, (d, s)] for core in (0, 1) for s in ways), c, name))
+    scatter, count = {}, len(gather)
+    for limit, c, name in sorted(limits):
+        fit = [pair for pair in waited if pair[0] < limit]
+        if fit:
+            waited.remove(fit[-1])
+            scatter[c, name] = fit[-1][1]
+        else:
+            scatter[c, name] = count
+            count += 1
     return gather, scatter, count
 
 

time: 57.5 us -> 57.4 us (level)
  no operation moved by 1% of the time
where the time goes in v8:
time: 57.4 us; the launch traced here: 57.2 us
  Pallas kernels  56.4 us (98%)
  between operations  0.81 us (1%)
    pallas_call x1, Pallas kernels, on_device(): pl.pallas_call(layer_kernel, out_shape=(jax.ShapeDtypeStruct((16, 2048),...  55.6 us

profile of v8, /device:TPU:0, one launch (start us, length us, event | category | flops | bytes accessed | tf_op | source)
XLA Modules:
  0.0 57.2 jit_solution(699562104148961569)
XLA Ops:
  0.6 55.6 %shard_map.257 = (bf16[16,2048]{1,0:T(8,128)(2,1)S(1)}, f32[2,16,2048]{2,1,0:T(8,128)S(1)}) custom-call(bf16[16,2048]{1,0:T(8,128)(2,1)} %tokens_hbm.1, f32[2,16,2048]{2,1,0:T(8,128)} %state_hbm.1, f32[1,2048]{1,0:T(1,128)} %bitcast.22, bf16[2048,512]{1,0:T(8,128)(2,1)} %w_drive_hbm.1, f32[32,64]{1,0:T(8,128)} %lam_real_hbm.1, f32[32,64]{1,0:T(8,128)} %lam_imag_hbm.1, ...), custom_call_target="tpu_custom_call" | custom-call | flops 8000000000 | bytes 20000000 | tf_op jit(solution)/shard_map/pallas_call | solution.py:966
  56.3 0.7 %shard_map.258 = (bf16[16,2048]{1,0:T(8,128)(2,1)}, f32[2,16,2048]{2,1,0:T(8,128)}) custom-call(bf16[16,2048]{1,0:T(8,128)(2,1)S(1)} %get-tuple-element.4.rows_ref, f32[2,16,2048]{2,1,0:T(8,128)S(1)} %get-tuple-element.5.state_ref), custom_call_target="tpu_custom_call" | custom-call | tf_op jit(solution)/shard_map/pallas_call | solution.py:923
